TPU v7x, 512 devices: a whole 4x4x16 slice. The times are simulated.
512 devices in a mesh: ep: 128 (over z, x, core), tp: 4 (over y).
Axes of the slice: x: 4, y: 4, z: 16, core: 2. Of those that a mesh axis runs over, the one named last changes fastest.
Arguments:
- hidden_in: bfloat16 [2048, 2048], P('ep'), may hold values from -6 to 6
- state_in: float32 [2048, 16, 64, 64], P('ep', 'tp'), may hold values from -6 to 6
- receptance: bfloat16 [2048, 1024], P('ep', 'tp'), may hold values from -6 to 6
- key_in: bfloat16 [2048, 1024], P('ep', 'tp'), may hold values from -1.5 to 1.5
- value_in: bfloat16 [2048, 1024], P('ep', 'tp'), may hold values from -6 to 6
- learn_in: bfloat16 [2048, 1024], P('ep', 'tp'), may hold values from -8 to 8
- decay_in: float32 [2048, 1024], P('ep', 'tp'), may hold values from -6 to 6
- decay_base: float32 [1024], P('tp'), may hold values from -3 to 1
- norm_gain: float32 [1024], P('tp'), may hold values from 0.1 to 1.9
- out_weight: bfloat16 [1024, 2048], P('tp'), may hold values from -0.1875 to 0.1875
- routed_gain: float32 [2048], replicated, may hold values from 0.1 to 1.9
- expert_gate: bfloat16 [128, 2048, 512], P('ep', None, 'tp'), may hold values from -0.125 to 0.125
- expert_up: bfloat16 [128, 2048, 512], P('ep', None, 'tp'), may hold values from -0.125 to 0.125
- expert_down: bfloat16 [128, 512, 2048], P('ep', 'tp'), may hold values from -0.25 to 0.25
- route_ids: int32 [2048, 6], P('ep'), may hold values from 0 to 127, all different within a row; in each aligned block of 16 rows (0 to 15, 16 to 31, ...) at most 2 rows name the same one
- route_weights: float32 [2048, 6], P('ep'), may hold values from 0.05 to 0.5
Outputs:
- hidden_out: bfloat16 [2048, 2048], P('ep')
- state_out: float32 [2048, 16, 64, 64], P('ep', 'tp')
Inputs may be any that keep to these rules, and one draw needn't show every extreme that they name: `route_ids`: each row names 6 different experts. Among the rows of one index of ep no expert is named more than 2 times, a bound that some block reaches.
All inputs are finite; a program needn't handle non-finite values.
Results may differ from a plain program's by a relative error of at most 0.014.
Values may be sent and summed in bfloat16 or wider, within the bound.
No kernel may reach another device: no remote copies, remote signals or barrier semaphores. Data moves between devices by JAX's collectives and lax.ppermute only.
A program may use at most 128 MiB of HBM per device.

v0:
```python
import jax
import jax.numpy as jnp
from jax import lax
from jax.sharding import PartitionSpec as P

EPSILON = 1e-06
GROUP_EPSILON = 0.00064


def sent_to_all(shard, axis):
    copies = jnp.broadcast_to(shard, (lax.axis_size(axis), *shard.shape))
    return lax.all_to_all(copies, axis, split_axis=0, concat_axis=0, tiled=True)


def taken_together(shard, axis):
    return sent_to_all(shard, axis).astype(jnp.float32).sum(axis=0)


def in_order(pieces, dim):
    shape = list(pieces.shape[1:])
    shape[dim] *= pieces.shape[0]
    return jnp.moveaxis(pieces, 0, dim).reshape(shape)


def gathered_copies(shard, axis, dim):
    return in_order(sent_to_all(shard, axis), dim)


def cut_along(shard, dim, length):
    before, after = (shard.shape[:dim], shard.shape[dim + 1 :])
    return jnp.moveaxis(shard.reshape(*before, length, -1, *after), dim, 0)


def sum_at_owner(shard, axis, dim):
    pieces = cut_along(shard, dim, lax.axis_size(axis))
    arrived = lax.all_to_all(pieces, axis, split_axis=0, concat_axis=0, tiled=True)
    return arrived.astype(jnp.float32).sum(axis=0)


def heads_update(state_in, receptance, key_in, value_in, learn_in, decay_in, decay_base, norm_gain):
    seq_count = receptance.shape[0]
    head_count = state_in.shape[1]
    head_size = state_in.shape[3]

    def to_heads(values):
        return values.astype(jnp.float32).reshape(seq_count, head_count, head_size)

    reading = to_heads(receptance)
    keys = to_heads(key_in)
    values = to_heads(value_in)
    learning = jax.nn.sigmoid(to_heads(learn_in))
    log_rate = -jax.nn.softplus(-(decay_base[None, :] + decay_in)) - 0.5
    decay = to_heads(jnp.exp(-jnp.exp(log_rate)))
    unit_key = keys * lax.rsqrt(jnp.sum(keys * keys, axis=-1, keepdims=True) + EPSILON)
    carried = jnp.einsum("shij,shj->shi", state_in, unit_key)
    new_state = (
        state_in * decay[:, :, None, :]
        - carried[..., None] * (unit_key * learning)[:, :, None, :]
        + values[..., None] * keys[:, :, None, :]
    )
    output = jnp.einsum("shij,shj->shi", new_state, reading)
    center = jnp.mean(output, axis=-1, keepdims=True)
    spread = jnp.mean(jnp.square(output - center), axis=-1, keepdims=True)
    gain = norm_gain.reshape(head_count, head_size)
    normed = (output - center) * lax.rsqrt(spread + GROUP_EPSILON) * gain[None]
    return (normed.reshape(seq_count, head_count * head_size).astype(jnp.bfloat16), new_state)


def slot_table(route_ids, expert_count, capacity):
    seq_count, top_count = route_ids.shape
    flat_ids = route_ids.reshape(-1)
    hit = (flat_ids[:, None] == jnp.arange(expert_count, dtype=jnp.int32)[None, :]).astype(
        jnp.int32
    )
    before = jnp.cumsum(hit, axis=0) - hit
    slot = jnp.sum(before * hit, axis=1)
    within = (slot[:, None] == jnp.arange(capacity, dtype=jnp.int32)[None, :]).astype(jnp.int32)
    place = hit[:, :, None] * within[:, None, :]
    return place.reshape(seq_count, top_count, expert_count, capacity).astype(jnp.bfloat16)


def expert_partial(arrived, expert_gate, expert_up, expert_down):
    senders, slots, width = arrived.shape
    flat = arrived.reshape(senders * slots, width)
    gate = jnp.dot(flat, expert_gate[0], preferred_element_type=jnp.float32)
    upward = jnp.dot(flat, expert_up[0], preferred_element_type=jnp.float32)
    hidden = (jax.nn.silu(gate) * upward).astype(jnp.bfloat16)
    partial_value = jnp.dot(hidden, expert_down[0], preferred_element_type=jnp.float32)
    rounded = lax.optimization_barrier(partial_value.astype(jnp.bfloat16)).astype(jnp.float32)
    return rounded.reshape(senders, slots, width)


def on_device(
    hidden_in,
    state_in,
    receptance,
    key_in,
    value_in,
    learn_in,
    decay_in,
    decay_base,
    norm_gain,
    out_weight,
    routed_gain,
    expert_gate,
    expert_up,
    expert_down,
    route_ids,
    route_weights,
):
    mixed, new_state = heads_update(
        state_in, receptance, key_in, value_in, learn_in, decay_in, decay_base, norm_gain
    )
    product = jnp.dot(mixed, out_weight, preferred_element_type=jnp.float32)
    partial_value = lax.optimization_barrier(product.astype(jnp.bfloat16)).astype(jnp.float32)
    attention = (
        taken_together(partial_value.astype(jnp.bfloat16), "tp")
        .astype(jnp.float32)
        .astype(jnp.bfloat16)
    )
    residual = hidden_in.astype(jnp.float32) + attention.astype(jnp.float32)
    scale = lax.rsqrt(jnp.mean(residual * residual, axis=-1, keepdims=True) + EPSILON)
    normed = (residual * scale * routed_gain[None, :]).astype(jnp.bfloat16)
    seq_count, top_count = route_ids.shape
    expert_count = lax.axis_size("ep") * expert_gate.shape[0]
    capacity = min(seq_count, max(2, 2 * seq_count * top_count // expert_count))
    place = slot_table(route_ids, expert_count, capacity)
    outgoing = jnp.einsum("skec,sd->ecd", place, normed, preferred_element_type=jnp.float32).astype(
        jnp.bfloat16
    )
    width = outgoing.shape[2] // lax.axis_size("tp")
    member = lax.axis_index("tp")
    portion = lax.dynamic_slice_in_dim(outgoing, member * width, width, 2)
    whole = gathered_copies(
        lax.all_to_all(portion, "ep", split_axis=0, concat_axis=0, tiled=True), "tp", 2
    )
    partial_out = expert_partial(whole, expert_gate, expert_up, expert_down)
    share = sum_at_owner(partial_out.astype(jnp.bfloat16), "tp", 2).astype(jnp.bfloat16)
    returned = lax.all_to_all(share, "ep", split_axis=0, concat_axis=0, tiled=True)
    incoming = gathered_copies(returned, "tp", 2)
    picked = jnp.einsum("skec,ecd->skd", place, incoming, preferred_element_type=jnp.float32)
    routed = jnp.sum(route_weights[:, :, None] * picked, axis=1)
    return ((residual + routed).astype(jnp.bfloat16), new_state)


def solution(mesh):
    in_specs = (
        P("ep", None),
        P("ep", "tp", None, None),
        P("ep", "tp"),
        P("ep", "tp"),
        P("ep", "tp"),
        P("ep", "tp"),
        P("ep", "tp"),
        P("tp"),
        P("tp"),
        P("tp", None),
        P(),
        P("ep", None, "tp"),
        P("ep", None, "tp"),
        P("ep", "tp", None),
        P("ep", None),
        P("ep", None),
    )
    out_specs = (P("ep", None), P("ep", "tp", None, None))
    return jax.shard_map(
        on_device, mesh=mesh, in_specs=in_specs, out_specs=out_specs, check_vma=False
    )
```

profile of v0, /device:TPU:1, one launch (start us, length us, event | category | flops | bytes accessed | tf_op | source)
XLA Modules:
  0.0 157.0 jit_solution(16114269728003424552)
XLA Ops:
  0.7 0.9 mul.152
  1.6 0.7 add_divide_fusion
  2.4 0.8 fusion.27
  3.2 0.8 reshape.128
  4.0 0.1 multiply_reduce_fusion.2
  4.1 0.8 reshape.138
  4.9 0.8 reshape.129
  5.7 0.1 fusion.29
  5.8 2.2 %fusion.30 = f32[16,4,1,64]{3,2,1,0:T(1,128)S(1)} fusion(f32[16,4,64,1]{2,3,1,0:T(1,128)S(1)} %bitcast.57, f32[16,4,64,64]{3,2,1,0:T(8,128)} %param.17), kind=kOutput, calls=%fused_computation.55 | convolution fusion | flops 524288 | bytes 1081344 | tf_op jit(solution)/shard_map/shij,shj->shi/dot_general | solution.py:55
  8.0 1.4 multiply_add_fusion
  9.4 1.3 copy-done.2
  10.7 0.6 fusion.31
  11.4 0.1 reduce_sum.88
  11.5 0.2 multiply_reduce_fusion.1
  11.7 0.1 multiply_convert_fusion.3
  11.8 0.1 convert_element_type.73
  11.9 0.2 convolution_convert_fusion.1
  12.1 0.7 broadcast_in_dim.6
  12.9 5.0 %all-to-all-start = ((bf16[4,16,2048]{2,1,0:T(8,128)(2,1)}), bf16[4,16,2048]{2,1,0:T(8,128)(2,1)S(1)}, u32[]{:S(2)}, u32[]{:S(2)}) async-start(bf16[4,16,2048]{2,1,0:T(8,128)(2,1)} %broadcast_in_dim.6), calls=%async_computation | async-start | bytes 524288 | tf_op jit(solution)/shard_map/all_to_all | solution.py:12
  17.9 0.1 copy.44
  18.0 0.1 eq.47
  18.1 0.1 fusion.20
  18.2 0.1 reduce_window_sum.11
  18.3 0.2 select_reduce_fusion
  18.6 0.1 copy.45
  18.7 0.1 convert_reduce_fusion
  18.8 4.6 %all-to-all-done = bf16[4,16,2048]{2,1,0:T(8,128)(2,1)S(1)} async-done(((bf16[4,16,2048]{2,1,0:T(8,128)(2,1)}), bf16[4,16,2048]{2,1,0:T(8,128)(2,1)S(1)}, u32[]{:S(2)}, u32[]{:S(2)}) %all-to-all-start) | async-done | bytes 262176 | tf_op jit(solution)/shard_map/all_to_all | solution.py:12
  23.4 0.1 multiply_reduce_fusion
  23.6 0.5 fusion.14
  24.1 0.3 copy.46
  24.4 41.2 %all_to_all.30 = bf16[128,2,512]{2,1,0:T(2,128)(2,1)S(1)} all-to-all(bf16[128,2,512]{2,1,0:T(2,128)(2,1)S(1)} %copy.46), channel_id=1, replica_groups=mesh['ep'=128,'tp'=4] {'ep'}, dimensions={0} | all-to-all | bytes 524288 | tf_op jit(solution)/shard_map/all_to_all | solution.py:135
  65.6 0.5 broadcast_in_dim.7
  66.2 17.1 %all_to_all.31 = bf16[4,128,2,512]{3,2,1,0:T(2,128)(2,1)S(1)} all-to-all(bf16[4,128,2,512]{3,2,1,0:T(2,128)(2,1)S(1)} %broadcast_in_dim.7), channel_id=1, replica_groups=mesh['ep'=128,'tp'=4] {'tp'}, dimensions={0} | all-to-all | bytes 2097152 | tf_op jit(solution)/shard_map/all_to_all | solution.py:12
  83.3 1.4 copy.47
  84.6 0.3 copy.60
  84.9 0.4 fusion.6
  85.4 2.0 %convolution_convert_fusion = bf16[256,2048]{1,0:T(8,128)(2,1)S(1)} fusion(bf16[256,2048]{1,0:T(8,128)(2,1)S(1)} %bitcast.48, bf16[1,128,2048]{2,1,0:T(8,128)(2,1)} %param.29, bf16[1,2048,128]{2,1,0:T(8,128)(2,1)} %param.28, f32[256,128]{1,0:T(8,128)S(1)} %fusion.6), kind=kOutput, calls=%fused_computation | convolution fusion | flops 269156352 | bytes 3276800 | tf_op jit(solution)/shard_map/dot_general | solution.py:88
  87.3 0.8 convert_element_type.85
  88.1 0.8 copy.64
  89.0 16.0 %all_to_all.32 = bf16[4,128,2,512]{3,2,1,0:T(2,128)(2,1)S(1)} all-to-all(bf16[4,128,2,512]{3,2,1,0:T(2,128)(2,1)S(1)} %bitcast.51), channel_id=1, replica_groups=mesh['ep'=128,'tp'=4] {'tp'}, dimensions={0} | all-to-all | bytes 2097152 | tf_op jit(solution)/shard_map/all_to_all | solution.py:36
  104.9 1.5 reduce_sum.94
  106.4 30.7 %all_to_all.33 = bf16[128,2,512]{2,1,0:T(2,128)(2,1)S(1)} all-to-all(bf16[128,2,512]{2,1,0:T(2,128)(2,1)S(1)} %reduce_sum.94), channel_id=1, replica_groups=mesh['ep'=128,'tp'=4] {'ep'}, dimensions={0} | all-to-all | bytes 524288 | tf_op jit(solution)/shard_map/all_to_all | solution.py:139
  137.1 0.1 broadcast_in_dim.8
  137.2 17.1 %all_to_all.34 = bf16[4,128,2,512]{3,1,2,0:T(8,128)(2,1)S(1)} all-to-all(bf16[4,128,2,512]{3,1,2,0:T(8,128)(2,1)S(1)} %broadcast_in_dim.8), channel_id=1, replica_groups=mesh['ep'=128,'tp'=4] {'tp'}, dimensions={0} | all-to-all | bytes 2097152 | tf_op jit(solution)/shard_map/all_to_all | solution.py:12
  154.3 0.8 copy.51
  155.2 0.8 reshape.135
  156.0 0.4 fusion.1
  156.3 0.7 add_convert_fusion
  (27 shorter events, 0.5 us)
Async XLA Ops:
  0.6 11.3 %copy-start = (bf16[256,2048]{1,0:T(8,128)(2,1)S(1)}, bf16[256,2048]{1,0:T(8,128)(2,1)}, u32[]{:S(2)}) copy-start(bf16[256,2048]{1,0:T(8,128)(2,1)} %param.25) | copy-start | bytes 3145732
  0.6 7.4 %copy-start.1 = (f32[16,4,64,64]{3,2,1,0:T(8,128)S(1)}, f32[16,4,64,64]{3,2,1,0:T(8,128)}, u32[]{:S(2)}) copy-start(f32[16,4,64,64]{3,2,1,0:T(8,128)} %param.17) | copy-start | bytes 3145732
  9.4 1.3 copy-start.2
  10.7 7.1 %copy-start.5 = (s32[16,6]{0,1:T(8,128)S(1)}, s32[16,6]{0,1:T(8,128)}, u32[]{:S(2)}) copy-start(s32[16,6]{0,1:T(8,128)} %param.30) | copy-start | bytes 1156
  10.7 12.7 %copy-start.3 = (bf16[16,2048]{1,0:T(8,128)(2,1)S(1)}, bf16[16,2048]{1,0:T(8,128)(2,1)}, u32[]{:S(2)}) copy-start(bf16[16,2048]{1,0:T(8,128)(2,1)} %param.16) | copy-start | bytes 196612
  10.7 12.8 %copy-start.6 = (f32[2048]{0:T(1024)S(1)}, f32[2048]{0:T(1024)}, u32[]{:S(2)}) copy-start(f32[2048]{0:T(1024)} %param.26) | copy-start | bytes 24580
  12.9 10.5 %all-to-all-start = ((bf16[4,16,2048]{2,1,0:T(8,128)(2,1)}), bf16[4,16,2048]{2,1,0:T(8,128)(2,1)S(1)}, u32[]{:S(2)}, u32[]{:S(2)}) async-start(bf16[4,16,2048]{2,1,0:T(8,128)(2,1)} %broadcast_in_dim.6), calls=%async_computation | async-start | bytes 524288 | tf_op jit(solution)/shard_map/all_to_all | solution.py:12
  83.3 1.6 %copy-start.4 = (bf16[1,2048,128]{2,1,0:T(8,128)(2,1)S(1)}, bf16[1,2048,128]{2,1,0:T(8,128)(2,1)}, u32[]{:S(2)}) copy-start(bf16[1,2048,128]{2,1,0:T(8,128)(2,1)} %param.27) | copy-start | bytes 1572868
  154.3 1.6 %copy-start.7 = (f32[16,6]{0,1:T(8,128)S(1)}, f32[16,6]{0,1:T(8,128)}, u32[]{:S(2)}) copy-start(f32[16,6]{0,1:T(8,128)} %param.31) | copy-start | bytes 1156
where the time goes:
time: 159 us; the launch traced here: 157 us
  blocking collectives  122 us (77%)
  local copies, waits for them, and re-layouts  11.7 us (7%)
  other arithmetic  6.32 us (4%)
  matrix products  6.32 us (4%)
  starting transfers between devices  5 us (3%)
  waiting for transfers between devices  4.57 us (3%)
    all_to_all x1, blocking collectives, on_device(): lax.all_to_all(portion, 'ep', split_axis=0, concat_axis=0, tiled=True)  41.2 us
    all_to_all x2, blocking collectives, sent_to_all(): return lax.all_to_all(copies, axis, split_axis=0, concat_axis=0, tiled=True)  34.2 us
    all_to_all x1, blocking collectives, on_device(): lax.all_to_all(share, 'ep', split_axis=0, concat_axis=0, tiled=True)  30.7 us
    all_to_all x1, blocking collectives, sum_at_owner(): lax.all_to_all(pieces, axis, split_axis=0, concat_axis=0, tiled=True)  16 us
    all_to_all x1, starting transfers between devices, sent_to_all(): return lax.all_to_all(copies, axis, split_axis=0, concat_axis=0, tiled=True)  5 us
    all_to_all x1, waiting for transfers between devices, sent_to_all(): return lax.all_to_all(copies, axis, split_axis=0, concat_axis=0, tiled=True)  4.57 us
  transfers between devices with their start and end apart: 1, of which 1 were waited for; matrix products, arithmetic and copies ran while one was open for 1% of the time, Pallas kernels for 0%

commit v1 on v0

v1 whole, which is shorter than its diff:
```python
import jax
import jax.numpy as jnp
import numpy as np
from jax import lax
from jax.sharding import Mesh, PartitionSpec as P

EPSILON = 1e-06
GROUP_EPSILON = 0.00064
Z_AXES = ("zq", "zp")
NEAR_AXES = ("zp", "x", "c", "y")
EP = ("zq", "zp", "x", "c")


def exchange(pieces, axes):
    return lax.all_to_all(pieces, axes, split_axis=0, concat_axis=0, tiled=True)


def heads_update(state_in, receptance, key_in, value_in, learn_in, decay_in, decay_base, norm_gain):
    seq_count = receptance.shape[0]
    head_count = state_in.shape[1]
    head_size = state_in.shape[3]

    def to_heads(values):
        return values.astype(jnp.float32).reshape(seq_count, head_count, head_size)

    reading = to_heads(receptance)
    keys = to_heads(key_in)
    values = to_heads(value_in)
    learning = jax.nn.sigmoid(to_heads(learn_in))
    log_rate = -jax.nn.softplus(-(decay_base[None, :] + decay_in)) - 0.5
    decay = to_heads(jnp.exp(-jnp.exp(log_rate)))
    unit_key = keys * lax.rsqrt(jnp.sum(keys * keys, axis=-1, keepdims=True) + EPSILON)
    carried = jnp.einsum("shij,shj->shi", state_in, unit_key)
    new_state = (
        state_in * decay[:, :, None, :]
        - carried[..., None] * (unit_key * learning)[:, :, None, :]
        + values[..., None] * keys[:, :, None, :]
    )
    output = jnp.einsum("shij,shj->shi", new_state, reading)
    center = jnp.mean(output, axis=-1, keepdims=True)
    spread = jnp.mean(jnp.square(output - center), axis=-1, keepdims=True)
    gain = norm_gain.reshape(head_count, head_size)
    normed = (output - center) * lax.rsqrt(spread + GROUP_EPSILON) * gain[None]
    return (normed.reshape(seq_count, head_count * head_size).astype(jnp.bfloat16), new_state)


def split_weights(weights):
    high = weights.astype(jnp.bfloat16)
    low = (weights - high.astype(jnp.float32)).astype(jnp.bfloat16)
    return high, low


def selection(routing, first_expert, experts, slots):
    tokens = routing.shape[0]
    senders = lax.axis_size(Z_AXES)
    per_sender = tokens // senders
    wide = routing.astype(jnp.float32)
    named = first_expert + jnp.arange(experts, dtype=jnp.int32)
    ids = wide[:, 0:6].astype(jnp.int32)
    hit = ids[:, :, None] == named[None, None, :]
    member = jnp.any(hit, axis=1).astype(jnp.float32)
    high = jnp.sum(jnp.where(hit, wide[:, 6:12, None], 0.0), axis=1)
    low = jnp.sum(jnp.where(hit, wide[:, 12:18, None], 0.0), axis=1)
    at = np.arange(tokens)
    earlier = (at[:, None] // per_sender == at[None, :] // per_sender) & (at[:, None] < at[None, :])
    rank = jnp.einsum("te,tu->eu", member.astype(jnp.bfloat16), jnp.asarray(earlier, jnp.bfloat16), preferred_element_type=jnp.float32)
    sender = jnp.asarray(at // per_sender, jnp.float32)
    row = jnp.where(member.T > 0, sender[None, :] * slots + rank, -1.0)
    choice = row[:, None, :] == jnp.arange(senders * slots, dtype=jnp.float32)[None, :, None]
    weights = [jnp.where(choice, part.T[:, None, :], 0.0).astype(jnp.bfloat16).reshape(-1, tokens) for part in (high, low)]
    return choice.astype(jnp.bfloat16).reshape(-1, tokens), weights


def on_device(
    hidden_in,
    state_in,
    receptance,
    key_in,
    value_in,
    learn_in,
    decay_in,
    decay_base,
    norm_gain,
    out_weight,
    routed_gain,
    expert_gate,
    expert_up,
    expert_down,
    route_ids,
    route_weights,
):
    bf16, f32 = jnp.bfloat16, jnp.float32
    n_y, n_z, n_zp = lax.axis_size("y"), lax.axis_size(Z_AXES), lax.axis_size("zp")
    near = lax.axis_size(("zp", "x", "c"))
    seqs, width = hidden_in.shape
    quarter = width // n_y
    piece = quarter // n_zp
    slots = 2
    y = lax.axis_index("y")

    mixed, new_state = heads_update(
        state_in, receptance, key_in, value_in, learn_in, decay_in, decay_base, norm_gain
    )
    product = jnp.dot(mixed, out_weight, preferred_element_type=f32).astype(bf16)
    arrived = exchange(jnp.broadcast_to(product, (n_y, seqs, width)), "y")
    attention = arrived.astype(f32).sum(axis=0).astype(bf16)
    residual = hidden_in.astype(f32) + attention.astype(f32)
    scale = lax.rsqrt(jnp.mean(residual * residual, axis=-1, keepdims=True) + EPSILON)
    normed = (residual * scale * routed_gain[None, :]).astype(bf16)
    own = lax.dynamic_slice_in_dim(normed, y * quarter, quarter, 1)
    own_residual = lax.dynamic_slice_in_dim(residual, y * quarter, quarter, 1)

    high, low = split_weights(route_weights)
    routing = jnp.concatenate([route_ids.astype(bf16), high, low], axis=1)
    routing = jnp.pad(routing, ((0, 0), (0, 128 - routing.shape[1])))
    halves = own.reshape(seqs, n_zp, piece).transpose(1, 0, 2)
    parcel = jnp.concatenate([halves, jnp.broadcast_to(routing, (n_zp, seqs, 128))], axis=2)
    parcels = jnp.broadcast_to(parcel, (n_z // n_zp, *parcel.shape)).reshape(n_z, seqs, piece + 128)
    rows = exchange(parcels, Z_AXES).reshape(n_z * seqs, piece + 128)

    choice, (weight_high, weight_low) = selection(rows[:, piece:], lax.axis_index("zq") * near, near, slots)
    chosen = jnp.dot(choice, rows[:, :piece], preferred_element_type=f32).astype(bf16)
    per_expert = n_z * slots
    chosen = chosen.reshape(near, 1, per_expert, piece)
    outgoing = jnp.broadcast_to(chosen, (near, n_y, per_expert, piece)).reshape(near * n_y, per_expert, piece)
    got = exchange(outgoing, NEAR_AXES)

    n_xc = near // n_zp
    flat = got.reshape(n_zp, n_xc, n_y, per_expert, piece).transpose(1, 3, 2, 0, 4).reshape(n_xc * per_expert, width)
    gate = jnp.dot(flat, expert_gate[0], preferred_element_type=f32)
    upward = jnp.dot(flat, expert_up[0], preferred_element_type=f32)
    hidden = (jax.nn.silu(gate) * upward).astype(bf16)
    partial_out = jnp.dot(hidden, expert_down[0], preferred_element_type=f32).astype(bf16)
    back = partial_out.reshape(n_xc, per_expert, n_y, n_zp, piece).transpose(3, 0, 2, 1, 4)
    returned = exchange(back.reshape(near * n_y, per_expert, piece), NEAR_AXES)

    summed = returned.reshape(near, n_y, per_expert, piece).astype(f32).sum(axis=1).astype(bf16)
    summed = summed.reshape(near * per_expert, piece)

    def weighed(weight):
        return lax.dot_general(weight, summed, (((0,), (0,)), ((), ())), preferred_element_type=f32)

    combined = (weighed(weight_high) + weighed(weight_low)).astype(bf16)
    parts = exchange(combined.reshape(n_z, seqs, piece), Z_AXES)
    routed = parts.reshape(n_z // n_zp, n_zp, seqs, piece).astype(f32).sum(axis=0)
    routed = routed.transpose(1, 0, 2).reshape(seqs, quarter)
    result = (own_residual + routed).astype(bf16)
    spread = exchange(jnp.broadcast_to(result, (n_y, seqs, quarter)), "y")
    return (spread.transpose(1, 0, 2).reshape(seqs, width), new_state)


def solution(mesh):
    near_mesh = Mesh(mesh.devices.reshape(8, 2, 4, 2, 4), ("zq", "zp", "x", "c", "y"))
    in_specs = (
        P(EP, None),
        P(EP, "y", None, None),
        P(EP, "y"),
        P(EP, "y"),
        P(EP, "y"),
        P(EP, "y"),
        P(EP, "y"),
        P("y"),
        P("y"),
        P("y", None),
        P(),
        P(EP, None, "y"),
        P(EP, None, "y"),
        P(EP, "y", None),
        P(EP, None),
        P(EP, None),
    )
    out_specs = (P(EP, None), P(EP, "y", None, None))
    return jax.shard_map(
        on_device, mesh=near_mesh, in_specs=in_specs, out_specs=out_specs, check_vma=False
    )
```

time: 159 us -> 140 us (0.88)
  blocking collectives: 122 us -> 53.2 us
  waiting for transfers between devices: 4.57 us -> 34.4 us
  starting transfers between devices: 5 us -> 25 us
  other arithmetic: 6.32 us -> 4.31 us
    all_to_all x5 -> x3, blocking collectives: 122 us -> 53.2 us  [exchange(): return lax.all_to_all(pieces, axes, split_axis=0, concat_axis=0, tiled=True)]
    all_to_all x1 -> x3, waiting for transfers between devices: 4.57 us -> 34.4 us  [exchange(): return lax.all_to_all(pieces, axes, split_axis=0, concat_axis=0, tiled=True)]
    all_to_all x1 -> x3, starting transfers between devices: 5 us -> 25 us  [exchange(): return lax.all_to_all(pieces, axes, split_axis=0, concat_axis=0, tiled=True)]
    reshape x1 -> x6, local copies, waits for them, and re-layouts: 0.81 us -> 3.52 us  [the longest x2 2.04 us: on_device(): partial_out.reshape(n_xc, per_expert, n_y, n_zp, piece)]
    convert_element_type x3 -> x0, local copies, waits for them, and re-layouts: 1.63 us -> none  [the longest x2 1.61 us: on_device(): partial_out.astype(jnp.bfloat16)]
    dot_general x5 -> x7, matrix products: 3.47 us -> 4.61 us  [the longest x1 1.97 us: on_device(): jnp.dot(hidden, expert_down[0], preferred_element_type=f32).astype(bf16)]
  transfers between devices with their start and end apart: 1 -> 3, of which waited for: 1 -> 3; matrix products, arithmetic and copies ran while one was open for 1% -> 1% of each run, Pallas kernels for 0% -> 0%
where the time goes in v1:
time: 140 us; the launch traced here: 137 us
  blocking collectives  53.2 us (38%)
  waiting for transfers between devices  34.4 us (25%)
  starting transfers between devices  25 us (18%)
  local copies, waits for them, and re-layouts  12.1 us (9%)
  matrix products  7.47 us (5%)
  other arithmetic  4.31 us (3%)
    all_to_all x3, blocking collectives, exchange(): return lax.all_to_all(pieces, axes, split_axis=0, concat_axis=0, tiled=True)  53.2 us
    all_to_all x3, waiting for transfers between devices, exchange(): return lax.all_to_all(pieces, axes, split_axis=0, concat_axis=0, tiled=True)  34.4 us
    all_to_all x3, starting transfers between devices, exchange(): return lax.all_to_all(pieces, axes, split_axis=0, concat_axis=0, tiled=True)  25 us
  transfers between devices with their start and end apart: 3, of which 3 were waited for; matrix products, arithmetic and copies ran while one was open for 1% of the time, Pallas kernels for 0%

profile of v1, /device:TPU:1, one launch (start us, length us, event | category | flops | bytes accessed | tf_op | source)
XLA Modules:
  0.0 137.5 jit_solution(8642445264013049832)
XLA Ops:
  0.7 0.9 mul.138
  1.6 0.7 add_divide_fusion
  2.4 0.8 fusion.28
  3.2 0.8 reshape.144
  4.0 0.1 multiply_reduce_fusion.2
  4.1 0.8 reshape.154
  4.9 0.8 reshape.145
  5.7 0.1 fusion.33
  5.8 2.2 %fusion.35 = f32[16,4,1,64]{3,2,1,0:T(1,128)S(1)} fusion(f32[16,4,64,1]{2,3,1,0:T(1,128)S(1)} %bitcast.78, f32[16,4,64,64]{3,2,1,0:T(8,128)} %param.19), kind=kOutput, calls=%fused_computation.72 | convolution fusion | flops 524288 | bytes 1081344 | tf_op jit(solution)/shard_map/shij,shj->shi/dot_general | solution.py:33
  8.0 1.4 %multiply_add_fusion = f32[16,4,64,64]{3,2,1,0:T(8,128)S(1)} fusion(f32[16,4,64,64]{3,2,1,0:T(8,128)S(1)} %copy-done.1, f32[16,4,64]{2,1,0:T(4,128)S(1)} %reshape.144, f32[16,4,64]{2,1,0:T(4,128)S(1)} %reshape.145, f32[16,4,64]{2,1,0:T(4,128)S(1)} %get-tuple-element.4, f32[16,4,64]{2,1,0:T(4,128)S(1)} %bitcast.77, f32[16,4,64]{2,1,0:T(4,128)S(1)} %mul.121), kind=kLoop, calls=%fused_computation.2 | loop fusion | flops 1310720 | bytes 2179072 | tf_op jit(solution)/shard_map/add | solution.py:35
  9.4 1.3 copy-done.2
  10.8 0.6 fusion.36
  11.4 0.1 reduce_sum.88
  11.6 0.2 multiply_reduce_fusion.1
  11.7 0.1 multiply_convert_fusion.1
  11.8 0.1 convert_element_type.87
  11.9 0.2 convolution_convert_fusion.1
  12.2 0.7 broadcast_in_dim.76
  12.9 5.0 %all-to-all-start = ((bf16[4,16,2048]{2,1,0:T(8,128)(2,1)}), bf16[4,16,2048]{2,1,0:T(8,128)(2,1)S(1)}, u32[]{:S(2)}, u32[]{:S(2)}) async-start(bf16[4,16,2048]{2,1,0:T(8,128)(2,1)} %broadcast_in_dim.76), calls=%async_computation | async-start | bytes 524288 | tf_op jit(solution)/shard_map/all_to_all | solution.py:15
  18.0 0.1 copy.75
  18.0 0.8 dynamic-slice
  18.8 4.6 %all-to-all-done = bf16[4,16,2048]{2,1,0:T(8,128)(2,1)S(1)} async-done(((bf16[4,16,2048]{2,1,0:T(8,128)(2,1)}), bf16[4,16,2048]{2,1,0:T(8,128)(2,1)S(1)}, u32[]{:S(2)}, u32[]{:S(2)}) %all-to-all-start) | async-done | bytes 262176 | tf_op jit(solution)/shard_map/all_to_all | solution.py:15
  23.5 0.1 multiply_reduce_fusion
  23.8 0.7 broadcast_in_dim.78
  24.5 14.9 %all-to-all-start.1 = ((bf16[16,16,384]{2,1,0:T(8,128)(2,1)}), bf16[16,16,384]{2,1,0:T(8,128)(2,1)S(1)}, u32[]{:S(2)}, u32[]{:S(2)}) async-start(bf16[16,16,384]{2,1,0:T(8,128)(2,1)} %bitcast.7), calls=%async_computation.1 | async-start | bytes 393216 | tf_op jit(solution)/shard_map/all_to_all | solution.py:15
  39.5 12.2 %all-to-all-done.1 = bf16[16,16,384]{2,1,0:T(8,128)(2,1)S(1)} async-done(((bf16[16,16,384]{2,1,0:T(8,128)(2,1)}), bf16[16,16,384]{2,1,0:T(8,128)(2,1)S(1)}, u32[]{:S(2)}, u32[]{:S(2)}) %all-to-all-start.1) | async-done | bytes 196640 | tf_op jit(solution)/shard_map/all_to_all | solution.py:15
  51.7 0.1 copy.74
  51.9 0.1 compare_reduce_fusion
  52.0 0.1 fusion.3
  52.1 0.2 bitcast_compare_fusion
  52.3 0.2 convolution_convert_fusion.2
  52.5 0.1 broadcast_in_dim.85
  52.7 29.2 %all_to_all.30 = bf16[64,32,256]{2,1,0:T(8,128)(2,1)S(1)} all-to-all(bf16[64,32,256]{2,1,0:T(8,128)(2,1)S(1)} %bitcast.67), channel_id=1, replica_groups=mesh['zq'=8,'zp'=2,'x'=4,'c'=2,'y'=4] {'zp','x','c','y'}, dimensions={0} | all-to-all | bytes 2097152 | tf_op jit(solution)/shard_map/all_to_all | solution.py:15
  81.9 1.1 copy.64
  83.0 0.8 reshape.136
  83.8 1.5 %fusion.7 = f32[256,128]{1,0:T(8,128)S(1)} fusion(bf16[256,2048]{1,0:T(8,128)(2,1)S(1)} %reshape.136, bf16[1,2048,128]{2,1,0:T(8,128)(2,1)} %param.29), kind=kOutput, calls=%fused_computation.15 | convolution fusion | flops 134217728 | bytes 1703936 | tf_op jit(solution)/shard_map/dot_general | solution.py:130
  85.3 2.0 %convolution_convert_fusion = bf16[256,2048]{1,0:T(8,128)(2,1)S(1)} fusion(bf16[256,2048]{1,0:T(8,128)(2,1)S(1)} %reshape.136, bf16[1,128,2048]{2,1,0:T(8,128)(2,1)} %param.31, bf16[1,2048,128]{2,1,0:T(8,128)(2,1)} %param.30, f32[256,128]{1,0:T(8,128)S(1)} %fusion.7), kind=kOutput, calls=%fused_computation | convolution fusion | flops 269156352 | bytes 3276800 | tf_op jit(solution)/shard_map/dot_general | solution.py:133
  87.3 0.8 reshape.137
  88.1 1.2 copy.65
  89.3 5.1 %all-to-all-start.3 = ((bf16[64,32,256]{2,1,0:T(8,128)(2,1)}), bf16[64,32,256]{2,1,0:T(8,128)(2,1)S(1)}, u32[]{:S(2)}, u32[]{:S(2)}) async-start(bf16[64,32,256]{2,1,0:T(8,128)(2,1)} %bitcast.20), calls=%async_computation.3 | async-start | bytes 2097152 | tf_op jit(solution)/shard_map/all_to_all | solution.py:15
  94.4 0.1 fusion.21
  94.5 17.6 %all-to-all-done.3 = bf16[64,32,256]{2,1,0:T(8,128)(2,1)S(1)} async-done(((bf16[64,32,256]{2,1,0:T(8,128)(2,1)}), bf16[64,32,256]{2,1,0:T(8,128)(2,1)S(1)}, u32[]{:S(2)}, u32[]{:S(2)}) %all-to-all-start.3) | async-done | bytes 1048608 | tf_op jit(solution)/shard_map/all_to_all | solution.py:15
  112.1 0.2 bitcast_reduce_fusion
  112.2 0.3 convolution_bitcast_fusion
  112.5 0.3 fusion.1
  112.8 15.8 %all_to_all.31 = bf16[16,16,256]{2,1,0:T(8,128)(2,1)S(1)} all-to-all(bf16[16,16,256]{2,1,0:T(8,128)(2,1)S(1)} %bitcast.80), channel_id=1, replica_groups=mesh['zq'=8,'zp'=2,'x'=4,'c'=2,'y'=4] {'zq','zp'}, dimensions={0} | all-to-all | bytes 262144 | tf_op jit(solution)/shard_map/all_to_all | solution.py:15
  128.7 8.1 %all_to_all.32 = bf16[4,16,512]{2,1,0:T(8,128)(2,1)S(1)} all-to-all(bf16[4,16,512]{2,1,0:T(8,128)(2,1)S(1)} %broadcast_in_dim.88), channel_id=1, replica_groups=mesh['zq'=8,'zp'=2,'x'=4,'c'=2,'y'=4] {'y'}, dimensions={0} | all-to-all | bytes 131072 | tf_op jit(solution)/shard_map/all_to_all | solution.py:15
  136.8 0.6 copy.77
  (41 shorter events, 0.6 us)
Async XLA Ops:
  0.6 11.3 %copy-start = (bf16[256,2048]{1,0:T(8,128)(2,1)S(1)}, bf16[256,2048]{1,0:T(8,128)(2,1)}, u32[]{:S(2)}) copy-start(bf16[256,2048]{1,0:T(8,128)(2,1)} %param.27) | copy-start | bytes 3145732
  0.6 7.4 %copy-start.1 = (f32[16,4,64,64]{3,2,1,0:T(8,128)S(1)}, f32[16,4,64,64]{3,2,1,0:T(8,128)}, u32[]{:S(2)}) copy-start(f32[16,4,64,64]{3,2,1,0:T(8,128)} %param.19) | copy-start | bytes 3145732
  9.4 1.3 copy-start.2
  10.8 7.1 %copy-start.6 = (f32[16,6]{0,1:T(8,128)S(1)}, f32[16,6]{0,1:T(8,128)}, u32[]{:S(2)}) copy-start(f32[16,6]{0,1:T(8,128)} %param.33) | copy-start | bytes 1156
  10.8 7.2 %copy-start.5 = (s32[16,6]{0,1:T(8,128)S(1)}, s32[16,6]{0,1:T(8,128)}, u32[]{:S(2)}) copy-start(s32[16,6]{0,1:T(8,128)} %param.32) | copy-start | bytes 1156
  10.8 12.7 %copy-start.4 = (bf16[16,2048]{1,0:T(8,128)(2,1)S(1)}, bf16[16,2048]{1,0:T(8,128)(2,1)}, u32[]{:S(2)}) copy-start(bf16[16,2048]{1,0:T(8,128)(2,1)} %param.18) | copy-start | bytes 196612
  11.5 40.5 %copy-start.3 = (bf16[256,256]{1,0:T(8,128)(2,1)S(1)}, bf16[256,256]{1,0:T(8,128)(2,1)}, u32[]{:S(2)}) copy-start(bf16[256,256]{1,0:T(8,128)(2,1)} %constant.56.clone) | copy-start | bytes 393220
  11.5 40.4 %copy-start.7 = (f32[256]{0:T(256)S(1)}, f32[256]{0:T(256)}, u32[]{:S(2)}) copy-start(f32[256]{0:T(256)} %constant.72) | copy-start | bytes 3076
  12.9 10.5 %all-to-all-start = ((bf16[4,16,2048]{2,1,0:T(8,128)(2,1)}), bf16[4,16,2048]{2,1,0:T(8,128)(2,1)S(1)}, u32[]{:S(2)}, u32[]{:S(2)}) async-start(bf16[4,16,2048]{2,1,0:T(8,128)(2,1)} %broadcast_in_dim.76), calls=%async_computation | async-start | bytes 524288 | tf_op jit(solution)/shard_map/all_to_all | solution.py:15
  24.5 27.2 %all-to-all-start.1 = ((bf16[16,16,384]{2,1,0:T(8,128)(2,1)}), bf16[16,16,384]{2,1,0:T(8,128)(2,1)S(1)}, u32[]{:S(2)}, u32[]{:S(2)}) async-start(bf16[16,16,384]{2,1,0:T(8,128)(2,1)} %bitcast.7), calls=%async_computation.1 | async-start | bytes 393216 | tf_op jit(solution)/shard_map/all_to_all | solution.py:15
  89.3 22.7 %all-to-all-start.3 = ((bf16[64,32,256]{2,1,0:T(8,128)(2,1)}), bf16[64,32,256]{2,1,0:T(8,128)(2,1)S(1)}, u32[]{:S(2)}, u32[]{:S(2)}) async-start(bf16[64,32,256]{2,1,0:T(8,128)(2,1)} %bitcast.20), calls=%async_computation.3 | async-start | bytes 2097152 | tf_op jit(solution)/shard_map/all_to_all | solution.py:15

commit v2 on v1

--- a/solution.py
+++ b/solution.py
@@ -1,11 +1,16 @@
+import functools
+import math
 import jax
 import jax.numpy as jnp
 import numpy as np
 from jax import lax
+from jax.experimental import pallas as pl
+from jax.experimental.pallas import tpu as pltpu
 from jax.sharding import Mesh, PartitionSpec as P
 
 EPSILON = 1e-06
 GROUP_EPSILON = 0.00064
+SEQ_STEP = 4
 Z_AXES = ("zq", "zp")
 NEAR_AXES = ("zp", "x", "c", "y")
 EP = ("zq", "zp", "x", "c")
@@ -15,33 +20,163 @@
     return lax.all_to_all(pieces, axes, split_axis=0, concat_axis=0, tiled=True)
 
 
-def heads_update(state_in, receptance, key_in, value_in, learn_in, decay_in, decay_base, norm_gain):
-    seq_count = receptance.shape[0]
-    head_count = state_in.shape[1]
-    head_size = state_in.shape[3]
-
-    def to_heads(values):
-        return values.astype(jnp.float32).reshape(seq_count, head_count, head_size)
-
-    reading = to_heads(receptance)
-    keys = to_heads(key_in)
-    values = to_heads(value_in)
-    learning = jax.nn.sigmoid(to_heads(learn_in))
-    log_rate = -jax.nn.softplus(-(decay_base[None, :] + decay_in)) - 0.5
-    decay = to_heads(jnp.exp(-jnp.exp(log_rate)))
-    unit_key = keys * lax.rsqrt(jnp.sum(keys * keys, axis=-1, keepdims=True) + EPSILON)
-    carried = jnp.einsum("shij,shj->shi", state_in, unit_key)
-    new_state = (
-        state_in * decay[:, :, None, :]
-        - carried[..., None] * (unit_key * learning)[:, :, None, :]
-        + values[..., None] * keys[:, :, None, :]
-    )
-    output = jnp.einsum("shij,shj->shi", new_state, reading)
-    center = jnp.mean(output, axis=-1, keepdims=True)
-    spread = jnp.mean(jnp.square(output - center), axis=-1, keepdims=True)
-    gain = norm_gain.reshape(head_count, head_size)
-    normed = (output - center) * lax.rsqrt(spread + GROUP_EPSILON) * gain[None]
-    return (normed.reshape(seq_count, head_count * head_size).astype(jnp.bfloat16), new_state)
+def heads_kernel(
+    copies,
+    state_ref,
+    reading_ref,
+    key_ref,
+    value_ref,
+    learn_ref,
+    decay_ref,
+    base_ref,
+    gain_ref,
+    weight_ref,
+    new_state_ref,
+    out_ref,
+    rows,
+    values_across,
+    read,
+):
+    f32 = jnp.float32
+    step = pl.program_id(0)
+    seqs = reading_ref.shape[0]
+    per_step, heads, size, _ = state_ref.shape
+    lanes = lax.broadcasted_iota(jnp.int32, (size, 128), 1)
+
+    @pl.when(step == 0)
+    def _():
+        keys = key_ref[...].astype(f32)
+        values = value_ref[...].astype(f32)
+        learning = jax.nn.sigmoid(learn_ref[...].astype(f32))
+        decay = jnp.exp(-math.exp(-0.5) * jax.nn.sigmoid(base_ref[...] + decay_ref[...]))
+        reading = reading_ref[...].astype(f32)
+        values_across[...] = jnp.zeros_like(values_across)
+        read[...] = jnp.zeros_like(read)
+        for head in range(heads):
+            at = slice(head * size, (head + 1) * size)
+            key = keys[:, at]
+            unit = key * lax.rsqrt(jnp.sum(key * key, axis=1, keepdims=True) + EPSILON)
+            rows[0, head] = unit
+            rows[1, head] = decay[:, at]
+            rows[2, head] = unit * learning[:, at]
+            rows[3, head] = key
+            rows[4, head] = reading[:, at]
+            values_across[head * seqs : (head + 1) * seqs, 0:size] = values[:, at]
+        values_across[...] = values_across[...].T
+
+    shifted = pltpu.roll(values_across[0:size, :], 128 - step * per_step, 1)
+    found = jnp.zeros((size, 128), f32)
+    for local in range(per_step):
+        seq = step * per_step + local
+        for head in range(heads):
+            column = head * seqs + local
+            state = state_ref[local, head]
+
+            def row(which):
+                return rows[which, head, pl.ds(seq, 1), :]
+
+            carried = jnp.sum(state * row(0), axis=1, keepdims=True)
+            new = (
+                state * row(1)
+                - carried * row(2)
+                + shifted[:, column : column + 1] * row(3)
+            )
+            new_state_ref[local, head] = new
+            found = jnp.where(lanes == column, jnp.sum(new * row(4), axis=1, keepdims=True), found)
+    read[0:size, :] += pltpu.roll(found, step * per_step, 1)
+
+    @pl.when(step == pl.num_programs(0) - 1)
+    def _():
+        output = read[...]
+        live = output[0:size]
+        center = jnp.mean(live, axis=0, keepdims=True)
+        spread = jnp.mean(jnp.square(live - center), axis=0, keepdims=True)
+        read[...] = (output - center) * lax.rsqrt(spread + GROUP_EPSILON)
+        across = read[...].T
+        gain = gain_ref[...]
+        mixed = jnp.concatenate(
+            [
+                across[head * seqs : (head + 1) * seqs, 0:size]
+                * gain[:, head * size : (head + 1) * size]
+                for head in range(heads)
+            ],
+            axis=1,
+        ).astype(jnp.bfloat16)
+        product = jnp.dot(mixed, weight_ref[...], preferred_element_type=f32).astype(jnp.bfloat16)
+        for copy in range(copies):
+            out_ref[copy] = product
+
+
+def heads_update(copies, state_in, receptance, key_in, value_in, learn_in, decay_in, decay_base, norm_gain, out_weight):
+    seqs, heads, size, _ = state_in.shape
+    width = out_weight.shape[1]
+    channels = heads * size
+    block = pl.BlockSpec((SEQ_STEP, heads, size, size), lambda s: (s, 0, 0, 0))
+
+    def whole(shape):
+        return pl.BlockSpec(shape, lambda s: (0,) * len(shape))
+
+    tall = whole((seqs, channels))
+    flat = whole((1, channels))
+    new_state, product = pl.pallas_call(
+        functools.partial(heads_kernel, copies),
+        grid=(seqs // SEQ_STEP,),
+        in_specs=[block, tall, tall, tall, tall, tall, flat, flat, whole((channels, width))],
+        out_specs=[block, whole((copies, seqs, width))],
+        out_shape=[
+            jax.ShapeDtypeStruct(state_in.shape, jnp.float32),
+            jax.ShapeDtypeStruct((copies, seqs, width), jnp.bfloat16),
+        ],
+        scratch_shapes=[
+            pltpu.VMEM((5, heads, seqs, size), jnp.float32),
+            pltpu.VMEM((128, 128), jnp.float32),
+            pltpu.VMEM((128, 128), jnp.float32),
+        ],
+        cost_estimate=pl.CostEstimate(flops=20_000_000, bytes_accessed=5_000_000, transcendentals=20_000),
+    )(
+        state_in,
+        receptance,
+        key_in,
+        value_in,
+        learn_in,
+        decay_in,
+        decay_base.reshape(1, channels),
+        norm_gain.reshape(1, channels),
+        out_weight,
+    )
+    return product, new_state
+
+
+def expert_kernel(got_ref, gate_ref, up_ref, down_ref, out_ref, flat):
+    f32 = jnp.float32
+    n_zp, n_xc, n_y, rows, piece = got_ref.shape
+    total = n_xc * rows
+    for y in range(n_y):
+        for zp in range(n_zp):
+            at = (y * n_zp + zp) * piece
+            flat[:, at : at + piece] = got_ref[zp, :, y].reshape(total, piece)
+    arrived = flat[...]
+    gate = jnp.dot(arrived, gate_ref[0], preferred_element_type=f32)
+    upward = jnp.dot(arrived, up_ref[0], preferred_element_type=f32)
+    hidden = (gate * jax.nn.sigmoid(gate) * upward).astype(jnp.bfloat16)
+    for y in range(n_y):
+        for zp in range(n_zp):
+            at = (y * n_zp + zp) * piece
+            partial = jnp.dot(hidden, down_ref[0, :, at : at + piece], preferred_element_type=f32)
+            out_ref[zp, :, y] = partial.astype(jnp.bfloat16).reshape(n_xc, rows, piece)
+
+
+def experts(got, expert_gate, expert_up, expert_down):
+    n_zp, n_xc, n_y, rows, piece = got.shape
+    vmem = pl.BlockSpec(memory_space=pltpu.VMEM)
+    return pl.pallas_call(
+        expert_kernel,
+        in_specs=[vmem] * 4,
+        out_specs=vmem,
+        out_shape=jax.ShapeDtypeStruct(got.shape, jnp.bfloat16),
+        scratch_shapes=[pltpu.VMEM((n_xc * rows, n_zp * n_y * piece), jnp.bfloat16)],
+        cost_estimate=pl.CostEstimate(flops=400_000_000, bytes_accessed=4_000_000, transcendentals=40_000),
+    )(got, expert_gate, expert_up, expert_down)
 
 
 def split_weights(weights):
@@ -98,11 +233,10 @@
     slots = 2
     y = lax.axis_index("y")
 
-    mixed, new_state = heads_update(
-        state_in, receptance, key_in, value_in, learn_in, decay_in, decay_base, norm_gain
-    )
-    product = jnp.dot(mixed, out_weight, preferred_element_type=f32).astype(bf16)
-    arrived = exchange(jnp.broadcast_to(product, (n_y, seqs, width)), "y")
+    product, new_state = heads_update(
+        n_y, state_in, receptance, key_in, value_in, learn_in, decay_in, decay_base, norm_gain, out_weight
+    )
+    arrived = exchange(product, "y")
     attention = arrived.astype(f32).sum(axis=0).astype(bf16)
     residual = hidden_in.astype(f32) + attention.astype(f32)
     scale = lax.rsqrt(jnp.mean(residual * residual, axis=-1, keepdims=True) + EPSILON)
@@ -126,12 +260,9 @@
     got = exchange(outgoing, NEAR_AXES)
 
     n_xc = near // n_zp
-    flat = got.reshape(n_zp, n_xc, n_y, per_expert, piece).transpose(1, 3, 2, 0, 4).reshape(n_xc * per_expert, width)
-    gate = jnp.dot(flat, expert_gate[0], preferred_element_type=f32)
-    upward = jnp.dot(flat, expert_up[0], preferred_element_type=f32)
-    hidden = (jax.nn.silu(gate) * upward).astype(bf16)
-    partial_out = jnp.dot(hidden, expert_down[0], preferred_element_type=f32).astype(bf16)
-    back = partial_out.reshape(n_xc, per_expert, n_y, n_zp, piece).transpose(3, 0, 2, 1, 4)
+    back = experts(
+        got.reshape(n_zp, n_xc, n_y, per_expert, piece), expert_gate, expert_up, expert_down
+    )
     returned = exchange(back.reshape(near * n_y, per_expert, piece), NEAR_AXES)
 
     summed = returned.reshape(near, n_y, per_expert, piece).astype(f32).sum(axis=1).astype(bf16)

time: 140 us -> 134 us (0.957)
  Pallas kernels: 0 us -> 13.4 us
  local copies, waits for them, and re-layouts: 12.1 us -> 2.57 us
  matrix products: 7.47 us -> 0.93 us
  other arithmetic: 4.31 us -> 0.87 us
    pallas_call x0 -> x2, Pallas kernels: none -> 13.4 us  [the longest x1 9.66 us: heads_update(): pl.pallas_call(functools.partial(heads_kernel, copies), grid=(seqs // SEQ...]
    dot_general x5 -> x0, matrix products: 6.54 us -> none  [the longest x1 2.22 us: heads_update(): carried = jnp.einsum('shij,shj->shi', state_in, unit_key)]
    reshape x5 -> x0, local copies, waits for them, and re-layouts: 4.43 us -> none  [the longest x2 2.04 us: on_device(): partial_out.reshape(n_xc, per_expert, n_y, n_zp, piece)]
    mul x3 -> x0, local copies, waits for them, and re-layouts: 1.78 us -> none  [the longest x1 0.91 us: heads_update(): normed = (output - center) * lax.rsqrt(spread + GROUP_EPSILON) * gain[None]]
where the time goes in v2:
time: 134 us; the launch traced here: 131 us
  blocking collectives  53.3 us (40%)
  waiting for transfers between devices  34.4 us (26%)
  starting transfers between devices  25 us (19%)
  Pallas kernels  13.4 us (10%)
  local copies, waits for them, and re-layouts  2.57 us (2%)
    all_to_all x3, blocking collectives, exchange(): return lax.all_to_all(pieces, axes, split_axis=0, concat_axis=0, tiled=True)  53.3 us
    all_to_all x3, waiting for transfers between devices, exchange(): return lax.all_to_all(pieces, axes, split_axis=0, concat_axis=0, tiled=True)  34.4 us
    all_to_all x3, starting transfers between devices, exchange(): return lax.all_to_all(pieces, axes, split_axis=0, concat_axis=0, tiled=True)  25 us
    pallas_call x1, Pallas kernels, heads_update(): pl.pallas_call(functools.partial(heads_kernel, copies), grid=(seqs // SEQ...  9.66 us
    pallas_call x1, Pallas kernels, experts(): pl.pallas_call(expert_kernel, in_specs=[vmem] * 4, out_specs=vmem, out_sh...  3.76 us
  transfers between devices with their start and end apart: 3, of which 3 were waited for; matrix products, arithmetic and copies ran while one was open for 1% of the time, Pallas kernels for 0%

profile of v2, /device:TPU:1, one launch (start us, length us, event | category | flops | bytes accessed | tf_op | source)
XLA Modules:
  0.0 131.4 jit_solution(10198914529212809295)
XLA Ops:
  0.6 0.0 copy-start.3
  0.6 0.0 copy-start.2
  0.7 0.0 copy-start.1
  0.7 0.0 copy-start
  0.7 0.0 copy-start.4
  0.7 9.7 %shard_map.185 = (f32[16,4,64,64]{3,2,1,0:T(8,128)}, bf16[4,16,2048]{2,1,0:T(8,128)(2,1)}) custom-call(f32[16,4,64,64]{3,2,1,0:T(8,128)} %state_ref.1, bf16[16,256]{1,0:T(8,128)(2,1)} %reading_ref.1, bf16[16,256]{1,0:T(8,128)(2,1)} %key_ref.1, bf16[16,256]{1,0:T(8,128)(2,1)} %value_ref.1, bf16[16,256]{1,0:T(8,128)(2,1)} %learn_ref.1, f32[16,256]{1,0:T(8,128)} %decay_ref.1, ...), custom_call_target="tpu_custom_call" | custom-call | flops 20000000 | bytes 5000000 | tf_op jit(solution)/shard_map/pallas_call | solution.py:121
  10.3 5.0 %all-to-all-start = ((bf16[4,16,2048]{2,1,0:T(8,128)(2,1)}), bf16[4,16,2048]{2,1,0:T(8,128)(2,1)S(1)}, u32[]{:S(2)}, u32[]{:S(2)}) async-start(bf16[4,16,2048]{2,1,0:T(8,128)(2,1)} %get-tuple-element.4), calls=%async_computation | async-start | bytes 524288 | tf_op jit(solution)/shard_map/all_to_all | solution.py:20
  15.4 0.0 copy-done.3
  15.4 0.0 copy-done.2
  15.4 0.1 copy.46
  15.5 0.8 dynamic-slice
  16.3 4.6 %all-to-all-done = bf16[4,16,2048]{2,1,0:T(8,128)(2,1)S(1)} async-done(((bf16[4,16,2048]{2,1,0:T(8,128)(2,1)}), bf16[4,16,2048]{2,1,0:T(8,128)(2,1)S(1)}, u32[]{:S(2)}, u32[]{:S(2)}) %all-to-all-start) | async-done | bytes 262176 | tf_op jit(solution)/shard_map/all_to_all | solution.py:20
  20.9 0.0 copy-done.1
  20.9 0.1 multiply_reduce_fusion
  21.1 0.1 multiply_convert_fusion
  21.2 0.7 broadcast_in_dim.68
  21.9 14.9 %all-to-all-start.1 = ((bf16[16,16,384]{2,1,0:T(8,128)(2,1)}), bf16[16,16,384]{2,1,0:T(8,128)(2,1)S(1)}, u32[]{:S(2)}, u32[]{:S(2)}) async-start(bf16[16,16,384]{2,1,0:T(8,128)(2,1)} %bitcast.3), calls=%async_computation.1 | async-start | bytes 393216 | tf_op jit(solution)/shard_map/all_to_all | solution.py:20
  36.9 0.1 eq.45
  37.0 12.2 %all-to-all-done.1 = bf16[16,16,384]{2,1,0:T(8,128)(2,1)S(1)} async-done(((bf16[16,16,384]{2,1,0:T(8,128)(2,1)}), bf16[16,16,384]{2,1,0:T(8,128)(2,1)S(1)}, u32[]{:S(2)}, u32[]{:S(2)}) %all-to-all-start.1) | async-done | bytes 196640 | tf_op jit(solution)/shard_map/all_to_all | solution.py:20
  49.2 0.1 copy.45
  49.3 0.1 compare_reduce_fusion
  49.4 0.0 copy-done
  49.4 0.0 copy-done.4
  49.4 0.1 fusion.2
  49.6 0.2 bitcast_compare_fusion
  49.7 0.2 convolution_convert_fusion
  50.0 0.1 broadcast_in_dim.75
  50.1 29.3 %all_to_all.30 = bf16[64,32,256]{2,1,0:T(8,128)(2,1)} all-to-all(bf16[64,32,256]{2,1,0:T(8,128)(2,1)S(1)} %bitcast.42), channel_id=1, replica_groups=mesh['zq'=8,'zp'=2,'x'=4,'c'=2,'y'=4] {'zp','x','c','y'}, dimensions={0} | all-to-all | bytes 2097152 | tf_op jit(solution)/shard_map/all_to_all | solution.py:20
  79.5 3.8 %shard_map.186 = bf16[2,8,4,32,256]{4,3,2,1,0:T(8,128)(2,1)} custom-call(bf16[2,8,4,32,256]{4,3,2,1,0:T(8,128)(2,1)} %bitcast.41, bf16[1,2048,128]{2,1,0:T(8,128)(2,1)} %gate_ref.1, bf16[1,2048,128]{2,1,0:T(8,128)(2,1)} %up_ref.1, bf16[1,128,2048]{2,1,0:T(8,128)(2,1)} %down_ref.1), custom_call_target="tpu_custom_call" | custom-call | flops 400000000 | bytes 4000000 | tf_op jit(solution)/shard_map/pallas_call | solution.py:172
  83.2 5.1 %all-to-all-start.3 = ((bf16[64,32,256]{2,1,0:T(8,128)(2,1)}), bf16[64,32,256]{2,1,0:T(8,128)(2,1)S(1)}, u32[]{:S(2)}, u32[]{:S(2)}) async-start(bf16[64,32,256]{2,1,0:T(8,128)(2,1)} %bitcast.40), calls=%async_computation.3 | async-start | bytes 2097152 | tf_op jit(solution)/shard_map/all_to_all | solution.py:20
  88.3 0.1 fusion.10
  88.4 17.6 %all-to-all-done.3 = bf16[64,32,256]{2,1,0:T(8,128)(2,1)S(1)} async-done(((bf16[64,32,256]{2,1,0:T(8,128)(2,1)}), bf16[64,32,256]{2,1,0:T(8,128)(2,1)S(1)}, u32[]{:S(2)}, u32[]{:S(2)}) %all-to-all-start.3) | async-done | bytes 1048608 | tf_op jit(solution)/shard_map/all_to_all | solution.py:20
  106.0 0.2 bitcast_reduce_fusion
  106.1 0.3 convolution_bitcast_fusion
  106.4 0.3 fusion.1
  106.7 15.8 %all_to_all.31 = bf16[16,16,256]{2,1,0:T(8,128)(2,1)S(1)} all-to-all(bf16[16,16,256]{2,1,0:T(8,128)(2,1)S(1)} %bitcast.49), channel_id=1, replica_groups=mesh['zq'=8,'zp'=2,'x'=4,'c'=2,'y'=4] {'zq','zp'}, dimensions={0} | all-to-all | bytes 262144 | tf_op jit(solution)/shard_map/all_to_all | solution.py:20
  122.6 8.1 %all_to_all.32 = bf16[4,16,512]{2,1,0:T(8,128)(2,1)S(1)} all-to-all(bf16[4,16,512]{2,1,0:T(8,128)(2,1)S(1)} %broadcast_in_dim.78), channel_id=1, replica_groups=mesh['zq'=8,'zp'=2,'x'=4,'c'=2,'y'=4] {'y'}, dimensions={0} | all-to-all | bytes 131072 | tf_op jit(solution)/shard_map/all_to_all | solution.py:20
  130.7 0.6 copy.48
  (19 shorter events, 0.2 us)
Async XLA Ops:
  0.6 14.7 %copy-start.3 = (f32[16,6]{0,1:T(8,128)S(1)}, f32[16,6]{0,1:T(8,128)}, u32[]{:S(2)}) copy-start(f32[16,6]{0,1:T(8,128)} %param.33) | copy-start | bytes 1156
  0.6 14.7 %copy-start.2 = (s32[16,6]{0,1:T(8,128)S(1)}, s32[16,6]{0,1:T(8,128)}, u32[]{:S(2)}) copy-start(s32[16,6]{0,1:T(8,128)} %param.32) | copy-start | bytes 1156
  0.7 20.3 %copy-start.1 = (bf16[16,2048]{1,0:T(8,128)(2,1)S(1)}, bf16[16,2048]{1,0:T(8,128)(2,1)}, u32[]{:S(2)}) copy-start(bf16[16,2048]{1,0:T(8,128)(2,1)} %param.18) | copy-start | bytes 196612
  0.7 48.8 %copy-start = (bf16[256,256]{1,0:T(8,128)(2,1)S(1)}, bf16[256,256]{1,0:T(8,128)(2,1)}, u32[]{:S(2)}) copy-start(bf16[256,256]{1,0:T(8,128)(2,1)} %constant.40.clone) | copy-start | bytes 393220
  0.7 48.8 %copy-start.4 = (f32[256]{0:T(256)S(1)}, f32[256]{0:T(256)}, u32[]{:S(2)}) copy-start(f32[256]{0:T(256)} %constant.56) | copy-start | bytes 3076
  10.3 10.5 %all-to-all-start = ((bf16[4,16,2048]{2,1,0:T(8,128)(2,1)}), bf16[4,16,2048]{2,1,0:T(8,128)(2,1)S(1)}, u32[]{:S(2)}, u32[]{:S(2)}) async-start(bf16[4,16,2048]{2,1,0:T(8,128)(2,1)} %get-tuple-element.4), calls=%async_computation | async-start | bytes 524288 | tf_op jit(solution)/shard_map/all_to_all | solution.py:20
  21.9 27.2 %all-to-all-start.1 = ((bf16[16,16,384]{2,1,0:T(8,128)(2,1)}), bf16[16,16,384]{2,1,0:T(8,128)(2,1)S(1)}, u32[]{:S(2)}, u32[]{:S(2)}) async-start(bf16[16,16,384]{2,1,0:T(8,128)(2,1)} %bitcast.3), calls=%async_computation.1 | async-start | bytes 393216 | tf_op jit(solution)/shard_map/all_to_all | solution.py:20
  83.2 22.7 %all-to-all-start.3 = ((bf16[64,32,256]{2,1,0:T(8,128)(2,1)}), bf16[64,32,256]{2,1,0:T(8,128)(2,1)S(1)}, u32[]{:S(2)}, u32[]{:S(2)}) async-start(bf16[64,32,256]{2,1,0:T(8,128)(2,1)} %bitcast.40), calls=%async_computation.3 | async-start | bytes 2097152 | tf_op jit(solution)/shard_map/all_to_all | solution.py:20

commit v3 on v2

v3 whole, which is shorter than its diff:
```python
import functools
import math
import jax
import jax.numpy as jnp
import numpy as np
from jax import lax
from jax.experimental import pallas as pl
from jax.experimental.pallas import tpu as pltpu
from jax.sharding import Mesh, PartitionSpec as P

EPSILON = 1e-06
GROUP_EPSILON = 0.00064
SEQ_STEP = 4
SLOTS = 2
Z_AXES = ("zq", "zp")
NEAR_AXES = ("zp", "x", "c", "y")
EP = ("zq", "zp", "x", "c")


def exchange(pieces, axes):
    return lax.all_to_all(pieces, axes, split_axis=0, concat_axis=0, tiled=True)


def split_dot(product, ones, contract):
    high = product.astype(jnp.bfloat16)
    low = (product - high.astype(jnp.float32)).astype(jnp.bfloat16)
    return contract(high, ones) + contract(low, ones)


def sum_across(product, ones):
    return jnp.dot(product, ones, preferred_element_type=jnp.float32)


def sum_to_row(product, ones):
    return lax.dot_general(
        ones, product, (((1,), (1,)), ((), ())), preferred_element_type=jnp.float32
    )


def heads_kernel(
    copies,
    state_ref,
    reading_ref,
    key_ref,
    value_ref,
    learn_ref,
    decay_ref,
    base_ref,
    gain_ref,
    weight_ref,
    new_state_ref,
    out_ref,
    rows,
    read,
):
    f32, bf16 = jnp.float32, jnp.bfloat16
    step = pl.program_id(0)
    seqs, channels = reading_ref.shape
    per_step, heads, size, _ = state_ref.shape

    @pl.when(step == 0)
    def _():
        keys = key_ref[...].astype(f32)
        values = value_ref[...].astype(f32)
        learning = jax.nn.sigmoid(learn_ref[...].astype(f32))
        decay = jnp.exp(-math.exp(-0.5) * jax.nn.sigmoid(base_ref[...] + decay_ref[...]))
        reading = reading_ref[...].astype(f32)
        read[...] = jnp.zeros_like(read)
        for head in range(heads):
            at = slice(head * size, (head + 1) * size)
            key = keys[:, at]
            unit = key * lax.rsqrt(jnp.sum(key * key, axis=1, keepdims=True) + EPSILON)
            rows[0, head] = unit
            rows[1, head] = decay[:, at]
            rows[2, head] = unit * learning[:, at]
            rows[3, head] = key
            rows[4, head] = reading[:, at]
            rows[5, head] = values[:, at]

    square = (size, size)
    diagonal = lax.broadcasted_iota(jnp.int32, square, 0) == lax.broadcasted_iota(jnp.int32, square, 1)
    ones = jnp.ones(square, bf16)
    tall_ones = jnp.ones((seqs, size), bf16)
    seq_of = lax.broadcasted_iota(jnp.int32, (seqs, channels), 0)
    found = read[...]
    for local in range(per_step):
        seq = step * per_step + local

        def row(which, head):
            return rows[which, head, pl.ds(seq, 1), :]

        carried = split_dot(
            jnp.concatenate([state_ref[local, head] * row(0, head) for head in range(heads)], axis=0),
            ones,
            sum_across,
        )
        value = sum_across(
            jnp.concatenate(
                [jnp.where(diagonal, row(5, head), 0.0).astype(bf16) for head in range(heads)], axis=0
            ),
            ones,
        )
        news = []
        for head in range(heads):
            at = slice(head * size, (head + 1) * size)
            new = (
                state_ref[local, head] * row(1, head)
                - carried[at] * row(2, head)
                + value[at] * row(3, head)
            )
            new_state_ref[local, head] = new
            news.append(new * row(4, head))
        found = jnp.where(
            seq_of == seq, split_dot(jnp.concatenate(news, axis=0), tall_ones, sum_to_row), found
        )
    read[...] = found

    @pl.when(step == pl.num_programs(0) - 1)
    def _():
        output = read[...]
        gain = gain_ref[...]
        mixed = []
        for head in range(heads):
            at = slice(head * size, (head + 1) * size)
            live = output[:, at]
            live = live - jnp.mean(live, axis=1, keepdims=True)
            spread = jnp.mean(jnp.square(live), axis=1, keepdims=True)
            mixed.append(live * lax.rsqrt(spread + GROUP_EPSILON) * gain[:, at])
        mixed = jnp.concatenate(mixed, axis=1).astype(bf16)
        product = jnp.dot(mixed, weight_ref[...], preferred_element_type=f32).astype(bf16)
        for copy in range(copies):
            out_ref[copy] = product


def heads_update(copies, state_in, receptance, key_in, value_in, learn_in, decay_in, decay_base, norm_gain, out_weight):
    seqs, heads, size, _ = state_in.shape
    width = out_weight.shape[1]
    channels = heads * size
    block = pl.BlockSpec((SEQ_STEP, heads, size, size), lambda s: (s, 0, 0, 0))

    def whole(shape):
        return pl.BlockSpec(shape, lambda s: (0,) * len(shape))

    tall = whole((seqs, channels))
    flat = whole((1, channels))
    new_state, product = pl.pallas_call(
        functools.partial(heads_kernel, copies),
        grid=(seqs // SEQ_STEP,),
        in_specs=[block, tall, tall, tall, tall, tall, flat, flat, whole((channels, width))],
        out_specs=[block, whole((copies, seqs, width))],
        out_shape=[
            jax.ShapeDtypeStruct(state_in.shape, jnp.float32),
            jax.ShapeDtypeStruct((copies, seqs, width), jnp.bfloat16),
        ],
        scratch_shapes=[
            pltpu.VMEM((6, heads, seqs, size), jnp.float32),
            pltpu.VMEM((seqs, channels), jnp.float32),
        ],
        compiler_params=pltpu.CompilerParams(vmem_limit_bytes=60 << 20),
        cost_estimate=pl.CostEstimate(flops=20_000_000, bytes_accessed=5_000_000, transcendentals=20_000),
    )(
        state_in,
        receptance,
        key_in,
        value_in,
        learn_in,
        decay_in,
        decay_base.reshape(1, channels),
        norm_gain.reshape(1, channels),
        out_weight,
    )
    return product, new_state


def expert_kernel(got_ref, gate_ref, up_ref, down_ref, out_ref, flat):
    f32 = jnp.float32
    n_zp, n_xc, n_y, rows, piece = got_ref.shape
    total = n_xc * rows
    for y in range(n_y):
        for zp in range(n_zp):
            at = (y * n_zp + zp) * piece
            flat[:, at : at + piece] = got_ref[zp, :, y].reshape(total, piece)
    arrived = flat[...]
    gate = jnp.dot(arrived, gate_ref[0], preferred_element_type=f32)
    upward = jnp.dot(arrived, up_ref[0], preferred_element_type=f32)
    hidden = (gate * jax.nn.sigmoid(gate) * upward).astype(jnp.bfloat16)
    for y in range(n_y):
        for zp in range(n_zp):
            at = (y * n_zp + zp) * piece
            partial = jnp.dot(hidden, down_ref[0, :, at : at + piece], preferred_element_type=f32)
            out_ref[zp, :, y] = partial.astype(jnp.bfloat16).reshape(n_xc, rows, piece)


def experts(got, expert_gate, expert_up, expert_down):
    n_zp, n_xc, n_y, rows, piece = got.shape
    vmem = pl.BlockSpec(memory_space=pltpu.VMEM)
    return pl.pallas_call(
        expert_kernel,
        in_specs=[vmem] * 4,
        out_specs=vmem,
        out_shape=jax.ShapeDtypeStruct(got.shape, jnp.bfloat16),
        scratch_shapes=[pltpu.VMEM((n_xc * rows, n_zp * n_y * piece), jnp.bfloat16)],
        compiler_params=pltpu.CompilerParams(vmem_limit_bytes=12 << 20),
        cost_estimate=pl.CostEstimate(flops=400_000_000, bytes_accessed=4_000_000, transcendentals=40_000),
    )(got, expert_gate, expert_up, expert_down)


def pack_kernel(
    n_zp, arrived_ref, hidden_ref, gain_ref, ids_ref, weights_ref, parcels_ref, own_ref
):
    f32, bf16 = jnp.float32, jnp.bfloat16
    seqs, width = hidden_ref.shape
    quarter = own_ref.shape[1]
    top = ids_ref.shape[0]
    attention = jnp.sum(arrived_ref[...].astype(f32), axis=0).astype(bf16)
    residual = hidden_ref[...].astype(f32) + attention.astype(f32)
    scale = lax.rsqrt(jnp.mean(residual * residual, axis=1, keepdims=True) + EPSILON)
    at = pl.ds(pl.multiple_of(lax.axis_index("y") * quarter, quarter), quarter)
    attention = jnp.sum(arrived_ref[:, :, at].astype(f32), axis=0).astype(bf16)
    residual = hidden_ref[:, at].astype(f32) + attention.astype(f32)
    own_ref[...] = residual
    normed = (residual * scale * gain_ref[:, at]).astype(bf16)

    weights = weights_ref[...]
    routing = jnp.zeros((8, 128), f32)
    parts = [ids_ref[...].astype(f32)]
    for _ in range(3):
        part = weights.astype(bf16).astype(f32)
        parts.append(part)
        weights = weights - part
    routing = jnp.concatenate(
        [jnp.pad(part, ((0, 8 - top), (0, 0))) for part in parts]
        + [jnp.zeros((8, 128 - len(parts) * seqs), f32)],
        axis=1,
    ).astype(bf16)
    n_z = parcels_ref.shape[0]
    chunks = quarter // n_zp // 128
    for z in range(n_z):
        first = (z % n_zp) * chunks
        for chunk in range(chunks):
            lanes = slice((first + chunk) * 128, (first + chunk + 1) * 128)
            parcels_ref[z, chunk * seqs : (chunk + 1) * seqs, :] = normed[:, lanes]
        parcels_ref[z, chunks * seqs : chunks * seqs + 8, :] = routing


def pack(arrived, hidden_in, routed_gain, route_ids, route_weights, n_z, n_zp):
    n_y, seqs, width = arrived.shape
    quarter = width // n_y
    vmem = pl.BlockSpec(memory_space=pltpu.VMEM)
    return pl.pallas_call(
        functools.partial(pack_kernel, n_zp),
        in_specs=[vmem] * 5,
        out_specs=[vmem] * 2,
        out_shape=[
            jax.ShapeDtypeStruct((n_z, quarter // n_zp // 128 * seqs + 8, 128), jnp.bfloat16),
            jax.ShapeDtypeStruct((seqs, quarter), jnp.float32),
        ],
        compiler_params=pltpu.CompilerParams(vmem_limit_bytes=8 << 20),
    )(arrived, hidden_in, routed_gain.reshape(1, width), route_ids.T, route_weights.T)


def choose_kernel(top, slots, rows_ref, chosen_ref, place_ref, weight_ref, flat, choice):
    f32, bf16 = jnp.float32, jnp.bfloat16
    n_z = rows_ref.shape[0]
    seqs = flat.shape[0] // n_z
    near, n_y, per_expert, piece = chosen_ref.shape
    tokens = n_z * seqs
    chunks = piece // 128
    sender_of = lax.broadcasted_iota(jnp.int32, (8, 128), 1) // seqs
    groups = tokens // 128
    per_group = 128 // seqs
    spread = [[jnp.zeros((8, 128), f32) for _ in range(groups)] for _ in range(4)]
    for z in range(n_z):
        for chunk in range(chunks):
            flat[z * seqs : (z + 1) * seqs, chunk * 128 : (chunk + 1) * 128] = rows_ref[
                z, chunk * seqs : (chunk + 1) * seqs, :
            ]
        routing = rows_ref[z, chunks * seqs : chunks * seqs + 8, :].astype(f32)
        group, place = divmod(z, per_group)
        for which in range(4):
            turn = (place - which) * seqs % 128
            moved = routing if turn == 0 else pltpu.roll(routing, turn, 1)
            spread[which][group] = jnp.where(sender_of == place, moved, spread[which][group])
    ids, high, middle, low = [jnp.concatenate(part, axis=1) for part in spread]
    weights = high + middle + low
    named = (
        lax.axis_index("zq") * near + lax.broadcasted_iota(jnp.int32, (near, tokens), 0)
    ).astype(f32)
    member = jnp.zeros((near, tokens), f32)
    weight = jnp.zeros((near, tokens), f32)
    for k in range(top):
        hit = named == ids[k : k + 1, :]
        member = jnp.where(hit, 1.0, member)
        weight = jnp.where(hit, weights[k : k + 1, :], weight)
    token = lax.broadcasted_iota(jnp.int32, (tokens, tokens), 0)
    other = lax.broadcasted_iota(jnp.int32, (tokens, tokens), 1)
    earlier = (token // seqs == other // seqs) & (token < other)
    rank = jnp.dot(member.astype(bf16), jnp.where(earlier, 1.0, 0.0).astype(bf16), preferred_element_type=f32)
    sender = (lax.broadcasted_iota(jnp.int32, (near, tokens), 1) // seqs * slots).astype(f32)
    place = jnp.where(member > 0, sender + rank, -1.0)
    place_ref[...] = place
    weight_ref[...] = weight
    row = lax.broadcasted_iota(jnp.int32, (per_expert, tokens), 0).astype(f32)
    for expert in range(near):
        choice[expert * per_expert : (expert + 1) * per_expert, :] = jnp.where(
            row == place[expert : expert + 1, :], 1.0, 0.0
        ).astype(bf16)
    chosen = jnp.dot(choice[...], flat[...], preferred_element_type=f32).astype(bf16)
    chosen = chosen.reshape(near, per_expert, piece)
    for y in range(n_y):
        chosen_ref[:, y] = chosen


def choose(rows, near, n_y, slots, top, seqs):
    n_z, depth, _ = rows.shape
    piece = (depth - 8) // seqs * 128
    tokens = n_z * seqs
    vmem = pl.BlockSpec(memory_space=pltpu.VMEM)
    return pl.pallas_call(
        functools.partial(choose_kernel, top, slots),
        in_specs=[vmem],
        out_specs=[vmem] * 3,
        out_shape=[
            jax.ShapeDtypeStruct((near, n_y, n_z * slots, piece), jnp.bfloat16),
            jax.ShapeDtypeStruct((near, tokens), jnp.float32),
            jax.ShapeDtypeStruct((near, tokens), jnp.float32),
        ],
        scratch_shapes=[
            pltpu.VMEM((tokens, piece), jnp.bfloat16),
            pltpu.VMEM((near * n_z * slots, tokens), jnp.bfloat16),
        ],
        compiler_params=pltpu.CompilerParams(vmem_limit_bytes=12 << 20),
    )(rows)


def combine_kernel(returned_ref, place_ref, weight_ref, out_ref, summed, choice):
    f32, bf16 = jnp.float32, jnp.bfloat16
    near, n_y, per_expert, piece = returned_ref.shape
    n_z, seqs, _ = out_ref.shape
    tokens = n_z * seqs
    total = near * per_expert
    row = lax.broadcasted_iota(jnp.int32, (per_expert, tokens), 0).astype(f32)
    for expert in range(near):
        at = slice(expert * per_expert, (expert + 1) * per_expert)
        result = jnp.sum(returned_ref[expert].astype(f32), axis=0).astype(bf16)
        summed[at, :] = result
        summed[total + expert * per_expert : total + (expert + 1) * per_expert, :] = result
        weight = jnp.where(
            row == place_ref[expert : expert + 1, :], weight_ref[expert : expert + 1, :], 0.0
        )
        high = weight.astype(bf16)
        choice[at, :] = high
        choice[total + expert * per_expert : total + (expert + 1) * per_expert, :] = (
            weight - high.astype(f32)
        ).astype(bf16)
    combined = lax.dot_general(
        choice[...], summed[...], (((0,), (0,)), ((), ())), preferred_element_type=f32
    )
    out_ref[...] = combined.astype(bf16).reshape(n_z, seqs, piece)


def combine(returned, place, weight, n_z):
    near, n_y, per_expert, piece = returned.shape
    tokens = place.shape[1]
    vmem = pl.BlockSpec(memory_space=pltpu.VMEM)
    return pl.pallas_call(
        combine_kernel,
        in_specs=[vmem] * 3,
        out_specs=vmem,
        out_shape=jax.ShapeDtypeStruct((n_z, tokens // n_z, piece), jnp.bfloat16),
        scratch_shapes=[
            pltpu.VMEM((2 * near * per_expert, piece), jnp.bfloat16),
            pltpu.VMEM((2 * near * per_expert, tokens), jnp.bfloat16),
        ],
        compiler_params=pltpu.CompilerParams(vmem_limit_bytes=12 << 20),
    )(returned, place, weight)


def on_device(
    hidden_in,
    state_in,
    receptance,
    key_in,
    value_in,
    learn_in,
    decay_in,
    decay_base,
    norm_gain,
    out_weight,
    routed_gain,
    expert_gate,
    expert_up,
    expert_down,
    route_ids,
    route_weights,
):
    n_y, n_z, n_zp = lax.axis_size("y"), lax.axis_size(Z_AXES), lax.axis_size("zp")
    near = lax.axis_size(("zp", "x", "c"))
    seqs, width = hidden_in.shape
    quarter = width // n_y
    piece = quarter // n_zp
    per_expert = n_z * SLOTS

    product, new_state = heads_update(
        n_y, state_in, receptance, key_in, value_in, learn_in, decay_in, decay_base, norm_gain, out_weight
    )
    arrived = exchange(product, "y")
    parcels, own_residual = pack(arrived, hidden_in, routed_gain, route_ids, route_weights, n_z, n_zp)
    rows = exchange(parcels, Z_AXES)
    chosen, place, weight = choose(rows, near, n_y, SLOTS, route_ids.shape[1], seqs)
    got = exchange(chosen.reshape(near * n_y, per_expert, piece), NEAR_AXES)
    got = got.reshape(n_zp, near // n_zp, n_y, per_expert, piece)
    back = experts(got, expert_gate, expert_up, expert_down)
    returned = exchange(back.reshape(near * n_y, per_expert, piece), NEAR_AXES)
    combined = combine(returned.reshape(near, n_y, per_expert, piece), place, weight, n_z)
    parts = exchange(combined, Z_AXES)
    routed = parts.reshape(n_z // n_zp, n_zp, seqs, piece).astype(jnp.float32).sum(axis=0)
    routed = routed.transpose(1, 0, 2).reshape(seqs, quarter)
    result = (own_residual + routed).astype(jnp.bfloat16)
    spread = exchange(jnp.broadcast_to(result, (n_y, seqs, quarter)), "y")
    return (spread.transpose(1, 0, 2).reshape(seqs, width), new_state)


def solution(mesh):
    near_mesh = Mesh(mesh.devices.reshape(8, 2, 4, 2, 4), ("zq", "zp", "x", "c", "y"))
    in_specs = (
        P(EP, None),
        P(EP, "y", None, None),
        P(EP, "y"),
        P(EP, "y"),
        P(EP, "y"),
        P(EP, "y"),
        P(EP, "y"),
        P("y"),
        P("y"),
        P("y", None),
        P(),
        P(EP, None, "y"),
        P(EP, None, "y"),
        P(EP, "y", None),
        P(EP, None),
        P(EP, None),
    )
    out_specs = (P(EP, None), P(EP, "y", None, None))
    return jax.shard_map(
        on_device, mesh=near_mesh, in_specs=in_specs, out_specs=out_specs, check_vma=False
    )
```

time: 134 us -> 125 us (0.933)
  blocking collectives: 53.3 us -> 112 us
  waiting for transfers between devices: 34.4 us -> 0 us
  starting transfers between devices: 25 us -> 0 us
  Pallas kernels: 13.4 us -> 9.56 us
  local copies, waits for them, and re-layouts: 2.57 us -> 0.68 us
    all_to_all x3 -> x6, blocking collectives: 53.3 us -> 112 us  [exchange(): return lax.all_to_all(pieces, axes, split_axis=0, concat_axis=0, tiled=True)]
    all_to_all x3 -> x0, waiting for transfers between devices: 34.4 us -> none  [exchange(): return lax.all_to_all(pieces, axes, split_axis=0, concat_axis=0, tiled=True)]
    all_to_all x3 -> x0, starting transfers between devices: 25 us -> none  [exchange(): return lax.all_to_all(pieces, axes, split_axis=0, concat_axis=0, tiled=True)]
    pallas_call x1, Pallas kernels: 3.76 us -> 1.04 us  [experts(): pl.pallas_call(expert_kernel, in_specs=[vmem] * 4, out_specs=vmem, out_sh...]
    pallas_call x1, Pallas kernels: 9.66 us -> 7.49 us  [heads_update(): pl.pallas_call(functools.partial(heads_kernel, copies), grid=(seqs // SEQ...]
  transfers between devices with their start and end apart: 3 -> 0, of which waited for: 3 -> 0; matrix products, arithmetic and copies ran while one was open for 1% -> 0% of each run, Pallas kernels for 0% -> 0%
where the time goes in v3:
time: 125 us; the launch traced here: 123 us
  blocking collectives  112 us (90%)
  Pallas kernels  9.56 us (8%)
    all_to_all x6, blocking collectives, exchange(): return lax.all_to_all(pieces, axes, split_axis=0, concat_axis=0, tiled=True)  112 us
    pallas_call x1, Pallas kernels, heads_update(): pl.pallas_call(functools.partial(heads_kernel, copies), grid=(seqs // SEQ...  7.49 us

profile of v3, /device:TPU:1, one launch (start us, length us, event | category | flops | bytes accessed | tf_op | source)
XLA Modules:
  0.0 122.9 jit_solution(9675329128640814346)
XLA Ops:
  0.6 0.0 copy-start.6
  0.6 0.0 copy-start.5
  0.7 0.0 copy-start.4
  0.7 0.0 copy-start.3
  0.7 7.5 %shard_map.167 = (f32[16,4,64,64]{3,2,1,0:T(8,128)}, bf16[4,16,2048]{2,1,0:T(8,128)(2,1)}) custom-call(f32[16,4,64,64]{3,2,1,0:T(8,128)} %state_ref.1, bf16[16,256]{1,0:T(8,128)(2,1)} %reading_ref.1, bf16[16,256]{1,0:T(8,128)(2,1)} %key_ref.1, bf16[16,256]{1,0:T(8,128)(2,1)} %value_ref.1, bf16[16,256]{1,0:T(8,128)(2,1)} %learn_ref.1, f32[16,256]{1,0:T(8,128)} %decay_ref.1, ...), custom_call_target="tpu_custom_call" | custom-call | flops 20000000 | bytes 5000000 | tf_op jit(solution)/shard_map/pallas_call | solution.py:146
  8.2 0.0 copy-start
  8.2 0.0 copy-start.1
  8.2 0.0 copy-start.2
  8.2 10.7 %all_to_all.30.arrived_ref = bf16[4,16,2048]{2,1,0:T(8,128)(2,1)S(1)} all-to-all(bf16[4,16,2048]{2,1,0:T(8,128)(2,1)} %get-tuple-element.9), channel_id=1, replica_groups=mesh['zq'=8,'zp'=2,'x'=4,'c'=2,'y'=4] {'y'}, dimensions={0} | all-to-all | bytes 524288 | tf_op jit(solution)/shard_map/all_to_all | solution.py:21
  18.9 0.0 copy-done.6
  18.9 0.0 copy-done.5
  18.9 0.0 copy-done.4
  18.9 0.0 copy-done.3
  18.9 0.2 shard_map.168
  19.1 26.9 %all_to_all.31.rows_ref = bf16[16,40,128]{2,1,0:T(8,128)(2,1)S(1)} all-to-all(bf16[16,40,128]{2,1,0:T(8,128)(2,1)S(1)} %get-tuple-element.11), channel_id=1, replica_groups=mesh['zq'=8,'zp'=2,'x'=4,'c'=2,'y'=4] {'zq','zp'}, dimensions={0} | all-to-all | bytes 327680 | tf_op jit(solution)/shard_map/all_to_all | solution.py:21
  45.9 0.4 shard_map.169
  46.4 28.2 %all_to_all.32 = bf16[64,32,256]{2,1,0:T(8,128)(2,1)S(1)} all-to-all(bf16[64,32,256]{2,1,0:T(8,128)(2,1)S(1)} %bitcast.20), channel_id=1, replica_groups=mesh['zq'=8,'zp'=2,'x'=4,'c'=2,'y'=4] {'zp','x','c','y'}, dimensions={0} | all-to-all | bytes 2097152 | tf_op jit(solution)/shard_map/all_to_all | solution.py:21
  74.5 0.0 copy-done
  74.5 0.0 copy-done.1
  74.6 0.0 copy-done.2
  74.6 1.0 shard_map.170
  75.6 22.4 %all_to_all.33 = bf16[64,32,256]{2,1,0:T(8,128)(2,1)S(1)} all-to-all(bf16[64,32,256]{2,1,0:T(8,128)(2,1)S(1)} %bitcast.18), channel_id=1, replica_groups=mesh['zq'=8,'zp'=2,'x'=4,'c'=2,'y'=4] {'zp','x','c','y'}, dimensions={0} | all-to-all | bytes 2097152 | tf_op jit(solution)/shard_map/all_to_all | solution.py:21
  98.0 0.4 shard_map.171
  98.4 15.7 %all_to_all.34 = bf16[16,16,256]{2,1,0:T(8,128)(2,1)S(1)} all-to-all(bf16[16,16,256]{2,1,0:T(8,128)(2,1)S(1)} %shard_map.171), channel_id=1, replica_groups=mesh['zq'=8,'zp'=2,'x'=4,'c'=2,'y'=4] {'zq','zp'}, dimensions={0} | all-to-all | bytes 262144 | tf_op jit(solution)/shard_map/all_to_all | solution.py:21
  114.1 8.1 %all_to_all.35 = bf16[4,16,512]{2,1,0:T(8,128)(2,1)S(1)} all-to-all(bf16[4,16,512]{2,1,0:T(8,128)(2,1)S(1)} %broadcast_in_dim.3), channel_id=1, replica_groups=mesh['zq'=8,'zp'=2,'x'=4,'c'=2,'y'=4] {'y'}, dimensions={0} | all-to-all | bytes 131072 | tf_op jit(solution)/shard_map/all_to_all | solution.py:21
  122.3 0.6 copy.22
  (4 shorter events, 0.0 us)
Async XLA Ops:
  0.6 18.2 %copy-start.6 = (f32[16,6]{0,1:T(8,128)S(1)}, f32[16,6]{0,1:T(8,128)}, u32[]{:S(2)}) copy-start(f32[16,6]{0,1:T(8,128)} %param.31) | copy-start | bytes 1156
  0.6 18.2 %copy-start.5 = (s32[16,6]{0,1:T(8,128)S(1)}, s32[16,6]{0,1:T(8,128)}, u32[]{:S(2)}) copy-start(s32[16,6]{0,1:T(8,128)} %param.30) | copy-start | bytes 1156
  0.7 18.2 %copy-start.4 = (f32[2048]{0:T(1024)S(1)}, f32[2048]{0:T(1024)}, u32[]{:S(2)}) copy-start(f32[2048]{0:T(1024)} %param.26) | copy-start | bytes 24580
  0.7 18.2 %copy-start.3 = (bf16[16,2048]{1,0:T(8,128)(2,1)S(1)}, bf16[16,2048]{1,0:T(8,128)(2,1)}, u32[]{:S(2)}) copy-start(bf16[16,2048]{1,0:T(8,128)(2,1)} %hidden_ref.1) | copy-start | bytes 196612
  8.2 66.4 %copy-start = (bf16[1,2048,128]{2,1,0:T(8,128)(2,1)S(1)}, bf16[1,2048,128]{2,1,0:T(8,128)(2,1)}, u32[]{:S(2)}) copy-start(bf16[1,2048,128]{2,1,0:T(8,128)(2,1)} %gate_ref.1) | copy-start | bytes 1572868
  8.2 66.4 %copy-start.1 = (bf16[1,2048,128]{2,1,0:T(8,128)(2,1)S(1)}, bf16[1,2048,128]{2,1,0:T(8,128)(2,1)}, u32[]{:S(2)}) copy-start(bf16[1,2048,128]{2,1,0:T(8,128)(2,1)} %up_ref.1) | copy-start | bytes 1572868
  8.2 66.4 %copy-start.2 = (bf16[1,128,2048]{2,1,0:T(8,128)(2,1)S(1)}, bf16[1,128,2048]{2,1,0:T(8,128)(2,1)}, u32[]{:S(2)}) copy-start(bf16[1,128,2048]{2,1,0:T(8,128)(2,1)} %down_ref.1) | copy-start | bytes 1572868

commit v4 on v3

--- a/solution.py
+++ b/solution.py
@@ -10,9 +10,8 @@
 
 EPSILON = 1e-06
 GROUP_EPSILON = 0.00064
-SEQ_STEP = 4
+SEQ_STEP = 8
 SLOTS = 2
-Z_AXES = ("zq", "zp")
 NEAR_AXES = ("zp", "x", "c", "y")
 EP = ("zq", "zp", "x", "c")
 
@@ -21,20 +20,9 @@
     return lax.all_to_all(pieces, axes, split_axis=0, concat_axis=0, tiled=True)
 
 
-def split_dot(product, ones, contract):
-    high = product.astype(jnp.bfloat16)
-    low = (product - high.astype(jnp.float32)).astype(jnp.bfloat16)
-    return contract(high, ones) + contract(low, ones)
-
-
-def sum_across(product, ones):
-    return jnp.dot(product, ones, preferred_element_type=jnp.float32)
-
-
-def sum_to_row(product, ones):
-    return lax.dot_general(
-        ones, product, (((1,), (1,)), ((), ())), preferred_element_type=jnp.float32
-    )
+def two_parts(values):
+    high = values.astype(jnp.bfloat16)
+    return high, (values - high.astype(jnp.float32)).astype(jnp.bfloat16)
 
 
 def heads_kernel(
@@ -52,80 +40,99 @@
     out_ref,
     rows,
     read,
+    joined,
+    parts,
+    sums,
 ):
     f32, bf16 = jnp.float32, jnp.bfloat16
     step = pl.program_id(0)
     seqs, channels = reading_ref.shape
     per_step, heads, size, _ = state_ref.shape
+    pairs = heads // 2
+    pair_width = 2 * size
+    square = (pair_width, pair_width)
+    same_head = (
+        lax.broadcasted_iota(jnp.int32, square, 0) // size
+        == lax.broadcasted_iota(jnp.int32, square, 1) // size
+    )
+    ones = jnp.where(same_head, 1.0, 0.0).astype(bf16)
+
+    def head_sums(values):
+        return sum(jnp.dot(part, ones, preferred_element_type=f32) for part in two_parts(values))
 
     @pl.when(step == 0)
     def _():
-        keys = key_ref[...].astype(f32)
-        values = value_ref[...].astype(f32)
         learning = jax.nn.sigmoid(learn_ref[...].astype(f32))
         decay = jnp.exp(-math.exp(-0.5) * jax.nn.sigmoid(base_ref[...] + decay_ref[...]))
-        reading = reading_ref[...].astype(f32)
+        keys = key_ref[...].astype(f32)
         read[...] = jnp.zeros_like(read)
-        for head in range(heads):
-            at = slice(head * size, (head + 1) * size)
+        for pair in range(pairs):
+            at = slice(pair * pair_width, (pair + 1) * pair_width)
             key = keys[:, at]
-            unit = key * lax.rsqrt(jnp.sum(key * key, axis=1, keepdims=True) + EPSILON)
-            rows[0, head] = unit
-            rows[1, head] = decay[:, at]
-            rows[2, head] = unit * learning[:, at]
-            rows[3, head] = key
-            rows[4, head] = reading[:, at]
-            rows[5, head] = values[:, at]
-
-    square = (size, size)
-    diagonal = lax.broadcasted_iota(jnp.int32, square, 0) == lax.broadcasted_iota(jnp.int32, square, 1)
-    ones = jnp.ones(square, bf16)
-    tall_ones = jnp.ones((seqs, size), bf16)
-    seq_of = lax.broadcasted_iota(jnp.int32, (seqs, channels), 0)
-    found = read[...]
-    for local in range(per_step):
-        seq = step * per_step + local
-
-        def row(which, head):
-            return rows[which, head, pl.ds(seq, 1), :]
-
-        carried = split_dot(
-            jnp.concatenate([state_ref[local, head] * row(0, head) for head in range(heads)], axis=0),
-            ones,
-            sum_across,
+            unit = key * lax.rsqrt(head_sums(key * key) + EPSILON)
+            rows[0, pair] = unit
+            rows[1, pair] = decay[:, at]
+            rows[2, pair] = unit * learning[:, at]
+            rows[3, pair] = key
+            rows[4, pair] = reading_ref[:, at].astype(f32)
+            rows[5, pair] = value_ref[:, at].astype(f32)
+
+    blocks = [
+        (local, pair, slice((local * pairs + pair) * size, (local * pairs + pair + 1) * size))
+        for local in range(per_step)
+        for pair in range(pairs)
+    ]
+
+    def row(which, local, pair):
+        return rows[which, pair, pl.ds(step * per_step + local, 1), :]
+
+    on_diagonal = lax.broadcasted_iota(jnp.int32, (size, pair_width), 0) == (
+        lax.broadcasted_iota(jnp.int32, (size, pair_width), 1) % size
+    )
+    for local, pair, at in blocks:
+        state = jnp.concatenate([state_ref[local, 2 * pair], state_ref[local, 2 * pair + 1]], axis=1)
+        joined[at, :] = state
+        parts[0, at, :], parts[1, at, :] = two_parts(state * row(0, local, pair))
+        parts[2, at, :] = jnp.where(on_diagonal, row(5, local, pair), 0.0).astype(bf16)
+    sums[0] = jnp.dot(parts[0], ones, preferred_element_type=f32) + jnp.dot(
+        parts[1], ones, preferred_element_type=f32
+    )
+    sums[1] = jnp.dot(parts[2], ones, preferred_element_type=f32)
+    for local, pair, at in blocks:
+        new = (
+            joined[at, :] * row(1, local, pair)
+            - sums[0, at, :] * row(2, local, pair)
+            + sums[1, at, :] * row(3, local, pair)
         )
-        value = sum_across(
-            jnp.concatenate(
-                [jnp.where(diagonal, row(5, head), 0.0).astype(bf16) for head in range(heads)], axis=0
-            ),
-            ones,
-        )
-        news = []
-        for head in range(heads):
-            at = slice(head * size, (head + 1) * size)
-            new = (
-                state_ref[local, head] * row(1, head)
-                - carried[at] * row(2, head)
-                + value[at] * row(3, head)
-            )
-            new_state_ref[local, head] = new
-            news.append(new * row(4, head))
-        found = jnp.where(
-            seq_of == seq, split_dot(jnp.concatenate(news, axis=0), tall_ones, sum_to_row), found
-        )
-    read[...] = found
+        new_state_ref[local, 2 * pair] = new[:, 0:size]
+        new_state_ref[local, 2 * pair + 1] = new[:, size:pair_width]
+        parts[0, at, :], parts[1, at, :] = two_parts(new * row(4, local, pair))
+    head_of = lax.broadcasted_iota(jnp.int32, (2 * 8, pair_width), 0) // 8
+    pick = jnp.where(
+        head_of == lax.broadcasted_iota(jnp.int32, (2 * 8, pair_width), 1) // size, 1.0, 0.0
+    ).astype(bf16)
+    dims = (((1,), (1,)), ((), ()))
+    found = lax.dot_general(pick, parts[0], dims, preferred_element_type=f32) + lax.dot_general(
+        pick, parts[1], dims, preferred_element_type=f32
+    )
+    seq_of = lax.broadcasted_iota(jnp.int32, (seqs, pairs * size), 0)
+    for which in range(2):
+        latest = read[which]
+        for local in range(per_step):
+            line = found[which * 8 : which * 8 + 1, local * pairs * size : (local + 1) * pairs * size]
+            latest = jnp.where(seq_of == step * per_step + local, line, latest)
+        read[which] = latest
 
     @pl.when(step == pl.num_programs(0) - 1)
     def _():
-        output = read[...]
-        gain = gain_ref[...]
         mixed = []
-        for head in range(heads):
-            at = slice(head * size, (head + 1) * size)
-            live = output[:, at]
-            live = live - jnp.mean(live, axis=1, keepdims=True)
-            spread = jnp.mean(jnp.square(live), axis=1, keepdims=True)
-            mixed.append(live * lax.rsqrt(spread + GROUP_EPSILON) * gain[:, at])
+        for pair in range(pairs):
+            at = slice(pair * size, (pair + 1) * size)
+            live = jnp.concatenate([read[0, :, at], read[1, :, at]], axis=1)
+            live = live - head_sums(live) * (1.0 / size)
+            spread = head_sums(jnp.square(live)) * (1.0 / size)
+            gain = gain_ref[:, pair * pair_width : (pair + 1) * pair_width]
+            mixed.append(live * lax.rsqrt(spread + GROUP_EPSILON) * gain)
         mixed = jnp.concatenate(mixed, axis=1).astype(bf16)
         product = jnp.dot(mixed, weight_ref[...], preferred_element_type=f32).astype(bf16)
         for copy in range(copies):
@@ -150,11 +157,14 @@
         out_specs=[block, whole((copies, seqs, width))],
         out_shape=[
             jax.ShapeDtypeStruct(state_in.shape, jnp.float32),
-            jax.ShapeDtypeStruct((copies, seqs, width), jnp.bfloat16),
+            pltpu.VMEM((copies, seqs, width), jnp.bfloat16),
         ],
         scratch_shapes=[
-            pltpu.VMEM((6, heads, seqs, size), jnp.float32),
-            pltpu.VMEM((seqs, channels), jnp.float32),
+            pltpu.VMEM((6, heads // 2, seqs, 2 * size), jnp.float32),
+            pltpu.VMEM((2, seqs, channels // 2), jnp.float32),
+            pltpu.VMEM((SEQ_STEP * heads // 2 * size, 2 * size), jnp.float32),
+            pltpu.VMEM((3, SEQ_STEP * heads // 2 * size, 2 * size), jnp.bfloat16),
+            pltpu.VMEM((2, SEQ_STEP * heads // 2 * size, 2 * size), jnp.float32),
         ],
         compiler_params=pltpu.CompilerParams(vmem_limit_bytes=60 << 20),
         cost_estimate=pl.CostEstimate(flops=20_000_000, bytes_accessed=5_000_000, transcendentals=20_000),
@@ -174,39 +184,36 @@
 
 def expert_kernel(got_ref, gate_ref, up_ref, down_ref, out_ref, flat):
     f32 = jnp.float32
-    n_zp, n_xc, n_y, rows, piece = got_ref.shape
-    total = n_xc * rows
+    senders, n_y, rows, quarter = got_ref.shape
     for y in range(n_y):
-        for zp in range(n_zp):
-            at = (y * n_zp + zp) * piece
-            flat[:, at : at + piece] = got_ref[zp, :, y].reshape(total, piece)
+        flat[:, y * quarter : (y + 1) * quarter] = got_ref[:, y].reshape(senders * rows, quarter)
     arrived = flat[...]
     gate = jnp.dot(arrived, gate_ref[0], preferred_element_type=f32)
     upward = jnp.dot(arrived, up_ref[0], preferred_element_type=f32)
     hidden = (gate * jax.nn.sigmoid(gate) * upward).astype(jnp.bfloat16)
     for y in range(n_y):
-        for zp in range(n_zp):
-            at = (y * n_zp + zp) * piece
-            partial = jnp.dot(hidden, down_ref[0, :, at : at + piece], preferred_element_type=f32)
-            out_ref[zp, :, y] = partial.astype(jnp.bfloat16).reshape(n_xc, rows, piece)
+        partial = jnp.dot(
+            hidden, down_ref[0, :, y * quarter : (y + 1) * quarter], preferred_element_type=f32
+        )
+        out_ref[:, y] = partial.astype(jnp.bfloat16).reshape(senders, rows, quarter)
 
 
 def experts(got, expert_gate, expert_up, expert_down):
-    n_zp, n_xc, n_y, rows, piece = got.shape
+    senders, n_y, rows, quarter = got.shape
     vmem = pl.BlockSpec(memory_space=pltpu.VMEM)
     return pl.pallas_call(
         expert_kernel,
         in_specs=[vmem] * 4,
         out_specs=vmem,
         out_shape=jax.ShapeDtypeStruct(got.shape, jnp.bfloat16),
-        scratch_shapes=[pltpu.VMEM((n_xc * rows, n_zp * n_y * piece), jnp.bfloat16)],
+        scratch_shapes=[pltpu.VMEM((senders * rows, n_y * quarter), jnp.bfloat16)],
         compiler_params=pltpu.CompilerParams(vmem_limit_bytes=12 << 20),
         cost_estimate=pl.CostEstimate(flops=400_000_000, bytes_accessed=4_000_000, transcendentals=40_000),
     )(got, expert_gate, expert_up, expert_down)
 
 
 def pack_kernel(
-    n_zp, arrived_ref, hidden_ref, gain_ref, ids_ref, weights_ref, parcels_ref, own_ref
+    arrived_ref, hidden_ref, gain_ref, ids_ref, weights_ref, parcels_ref, own_ref
 ):
     f32, bf16 = jnp.float32, jnp.bfloat16
     seqs, width = hidden_ref.shape
@@ -233,26 +240,25 @@
         + [jnp.zeros((8, 128 - len(parts) * seqs), f32)],
         axis=1,
     ).astype(bf16)
-    n_z = parcels_ref.shape[0]
-    chunks = quarter // n_zp // 128
-    for z in range(n_z):
-        first = (z % n_zp) * chunks
+    chunks = quarter // 128
+    for z in range(parcels_ref.shape[0]):
         for chunk in range(chunks):
-            lanes = slice((first + chunk) * 128, (first + chunk + 1) * 128)
-            parcels_ref[z, chunk * seqs : (chunk + 1) * seqs, :] = normed[:, lanes]
+            parcels_ref[z, chunk * seqs : (chunk + 1) * seqs, :] = normed[
+                :, chunk * 128 : (chunk + 1) * 128
+            ]
         parcels_ref[z, chunks * seqs : chunks * seqs + 8, :] = routing
 
 
-def pack(arrived, hidden_in, routed_gain, route_ids, route_weights, n_z, n_zp):
+def pack(arrived, hidden_in, routed_gain, route_ids, route_weights, n_z):
     n_y, seqs, width = arrived.shape
     quarter = width // n_y
     vmem = pl.BlockSpec(memory_space=pltpu.VMEM)
     return pl.pallas_call(
-        functools.partial(pack_kernel, n_zp),
+        pack_kernel,
         in_specs=[vmem] * 5,
         out_specs=[vmem] * 2,
         out_shape=[
-            jax.ShapeDtypeStruct((n_z, quarter // n_zp // 128 * seqs + 8, 128), jnp.bfloat16),
+            jax.ShapeDtypeStruct((n_z, quarter // 128 * seqs + 8, 128), jnp.bfloat16),
             jax.ShapeDtypeStruct((seqs, quarter), jnp.float32),
         ],
         compiler_params=pltpu.CompilerParams(vmem_limit_bytes=8 << 20),
@@ -394,28 +400,24 @@
     route_ids,
     route_weights,
 ):
-    n_y, n_z, n_zp = lax.axis_size("y"), lax.axis_size(Z_AXES), lax.axis_size("zp")
+    n_y, n_zq = lax.axis_size("y"), lax.axis_size("zq")
     near = lax.axis_size(("zp", "x", "c"))
     seqs, width = hidden_in.shape
     quarter = width // n_y
-    piece = quarter // n_zp
-    per_expert = n_z * SLOTS
+    per_expert = n_zq * SLOTS
 
     product, new_state = heads_update(
         n_y, state_in, receptance, key_in, value_in, learn_in, decay_in, decay_base, norm_gain, out_weight
     )
     arrived = exchange(product, "y")
-    parcels, own_residual = pack(arrived, hidden_in, routed_gain, route_ids, route_weights, n_z, n_zp)
-    rows = exchange(parcels, Z_AXES)
+    parcels, own_residual = pack(arrived, hidden_in, routed_gain, route_ids, route_weights, n_zq)
+    rows = exchange(parcels, "zq")
     chosen, place, weight = choose(rows, near, n_y, SLOTS, route_ids.shape[1], seqs)
-    got = exchange(chosen.reshape(near * n_y, per_expert, piece), NEAR_AXES)
-    got = got.reshape(n_zp, near // n_zp, n_y, per_expert, piece)
-    back = experts(got, expert_gate, expert_up, expert_down)
-    returned = exchange(back.reshape(near * n_y, per_expert, piece), NEAR_AXES)
-    combined = combine(returned.reshape(near, n_y, per_expert, piece), place, weight, n_z)
-    parts = exchange(combined, Z_AXES)
-    routed = parts.reshape(n_z // n_zp, n_zp, seqs, piece).astype(jnp.float32).sum(axis=0)
-    routed = routed.transpose(1, 0, 2).reshape(seqs, quarter)
+    got = exchange(chosen.reshape(near * n_y, per_expert, quarter), NEAR_AXES)
+    back = experts(got.reshape(near, n_y, per_expert, quarter), expert_gate, expert_up, expert_down)
+    returned = exchange(back.reshape(near * n_y, per_expert, quarter), NEAR_AXES)
+    combined = combine(returned.reshape(near, n_y, per_expert, quarter), place, weight, n_zq)
+    routed = exchange(combined, "zq").astype(jnp.float32).sum(axis=0)
     result = (own_residual + routed).astype(jnp.bfloat16)
     spread = exchange(jnp.broadcast_to(result, (n_y, seqs, quarter)), "y")
     return (spread.transpose(1, 0, 2).reshape(seqs, width), new_state)

time: 125 us -> 123 us (0.984); the launches traced: 123 us -> 122 us
  Pallas kernels: 9.56 us -> 7.44 us
    pallas_call x1, Pallas kernels: 7.49 us -> 5.43 us  [heads_update(): pl.pallas_call(functools.partial(heads_kernel, copies), grid=(seqs // SEQ...]
    all_to_all x6, blocking collectives: 112 us -> 113 us  [exchange(): return lax.all_to_all(pieces, axes, split_axis=0, concat_axis=0, tiled=True)]
where the time goes in v4:
time: 123 us; the launch traced here: 122 us
  blocking collectives  113 us (92%)
  Pallas kernels  7.44 us (6%)
    all_to_all x6, blocking collectives, exchange(): return lax.all_to_all(pieces, axes, split_axis=0, concat_axis=0, tiled=True)  113 us
    pallas_call x1, Pallas kernels, heads_update(): pl.pallas_call(functools.partial(heads_kernel, copies), grid=(seqs // SEQ...  5.43 us

profile of v4, /device:TPU:1, one launch (start us, length us, event | category | flops | bytes accessed | tf_op | source)
XLA Modules:
  0.0 122.2 jit_solution(239975857695787216)
XLA Ops:
  0.6 0.0 copy-start.6
  0.6 0.0 copy-start.5
  0.7 0.0 copy-start.4
  0.7 0.0 copy-start.3
  0.7 5.4 %shard_map.167 = (f32[16,4,64,64]{3,2,1,0:T(8,128)}, bf16[4,16,2048]{2,1,0:T(8,128)(2,1)S(1)}) custom-call(f32[16,4,64,64]{3,2,1,0:T(8,128)} %state_ref.1, bf16[16,256]{1,0:T(8,128)(2,1)} %reading_ref.1, bf16[16,256]{1,0:T(8,128)(2,1)} %key_ref.1, bf16[16,256]{1,0:T(8,128)(2,1)} %value_ref.1, bf16[16,256]{1,0:T(8,128)(2,1)} %learn_ref.1, ...), custom_call_target="tpu_custom_call" | custom-call | flops 20000000 | bytes 5000000 | tf_op jit(solution)/shard_map/pallas_call | solution.py:153
  6.1 0.0 copy-start
  6.1 0.0 copy-start.1
  6.1 0.0 copy-start.2
  6.1 10.5 %all_to_all.30.arrived_ref = bf16[4,16,2048]{2,1,0:T(8,128)(2,1)S(1)} all-to-all(bf16[4,16,2048]{2,1,0:T(8,128)(2,1)S(1)} %get-tuple-element.9), channel_id=1, replica_groups=mesh['zq'=8,'zp'=2,'x'=4,'c'=2,'y'=4] {'y'}, dimensions={0} | all-to-all | bytes 524288 | tf_op jit(solution)/shard_map/all_to_all | solution.py:20
  16.6 0.0 copy-done.6
  16.6 0.0 copy-done.5
  16.6 0.0 copy-done.4
  16.6 0.0 copy-done.3
  16.6 0.2 shard_map.168
  16.8 28.4 %all_to_all.31.rows_ref = bf16[8,72,128]{2,1,0:T(8,128)(2,1)S(1)} all-to-all(bf16[8,72,128]{2,1,0:T(8,128)(2,1)S(1)} %get-tuple-element.11), channel_id=1, replica_groups=mesh['zq'=8,'zp'=2,'x'=4,'c'=2,'y'=4] {'zq'}, dimensions={0} | all-to-all | bytes 294912 | tf_op jit(solution)/shard_map/all_to_all | solution.py:20
  45.1 0.4 shard_map.169
  45.6 26.7 %all_to_all.32 = bf16[64,16,512]{2,1,0:T(8,128)(2,1)S(1)} all-to-all(bf16[64,16,512]{2,1,0:T(8,128)(2,1)S(1)} %bitcast.15), channel_id=1, replica_groups=mesh['zq'=8,'zp'=2,'x'=4,'c'=2,'y'=4] {'zp','x','c','y'}, dimensions={0} | all-to-all | bytes 2097152 | tf_op jit(solution)/shard_map/all_to_all | solution.py:20
  72.2 0.0 copy-done
  72.2 0.0 copy-done.1
  72.2 0.0 copy-done.2
  72.2 1.1 shard_map.170
  73.3 22.3 %all_to_all.33 = bf16[64,16,512]{2,1,0:T(8,128)(2,1)S(1)} all-to-all(bf16[64,16,512]{2,1,0:T(8,128)(2,1)S(1)} %bitcast.13), channel_id=1, replica_groups=mesh['zq'=8,'zp'=2,'x'=4,'c'=2,'y'=4] {'zp','x','c','y'}, dimensions={0} | all-to-all | bytes 2097152 | tf_op jit(solution)/shard_map/all_to_all | solution.py:20
  95.6 0.4 shard_map.171
  96.0 15.5 %all_to_all.34 = bf16[8,16,512]{2,1,0:T(8,128)(2,1)S(1)} all-to-all(bf16[8,16,512]{2,1,0:T(8,128)(2,1)S(1)} %shard_map.171), channel_id=1, replica_groups=mesh['zq'=8,'zp'=2,'x'=4,'c'=2,'y'=4] {'zq'}, dimensions={0} | all-to-all | bytes 262144 | tf_op jit(solution)/shard_map/all_to_all | solution.py:20
  111.6 10.0 %all_to_all.35 = bf16[4,16,512]{2,1,0:T(8,128)(2,1)S(1)} all-to-all(bf16[4,16,512]{2,1,0:T(8,128)(2,1)S(1)} %broadcast_in_dim.3), channel_id=1, replica_groups=mesh['zq'=8,'zp'=2,'x'=4,'c'=2,'y'=4] {'y'}, dimensions={0} | all-to-all | bytes 131072 | tf_op jit(solution)/shard_map/all_to_all | solution.py:20
  121.6 0.6 copy.19
  (3 shorter events, 0.0 us)
Async XLA Ops:
  0.6 16.0 %copy-start.6 = (f32[16,6]{0,1:T(8,128)S(1)}, f32[16,6]{0,1:T(8,128)}, u32[]{:S(2)}) copy-start(f32[16,6]{0,1:T(8,128)} %param.31) | copy-start | bytes 1156
  0.6 16.0 %copy-start.5 = (s32[16,6]{0,1:T(8,128)S(1)}, s32[16,6]{0,1:T(8,128)}, u32[]{:S(2)}) copy-start(s32[16,6]{0,1:T(8,128)} %param.30) | copy-start | bytes 1156
  0.7 15.9 %copy-start.4 = (f32[2048]{0:T(1024)S(1)}, f32[2048]{0:T(1024)}, u32[]{:S(2)}) copy-start(f32[2048]{0:T(1024)} %param.26) | copy-start | bytes 24580
  0.7 15.9 %copy-start.3 = (bf16[16,2048]{1,0:T(8,128)(2,1)S(1)}, bf16[16,2048]{1,0:T(8,128)(2,1)}, u32[]{:S(2)}) copy-start(bf16[16,2048]{1,0:T(8,128)(2,1)} %hidden_ref.1) | copy-start | bytes 196612
  6.1 66.1 %copy-start = (bf16[1,2048,128]{2,1,0:T(8,128)(2,1)S(1)}, bf16[1,2048,128]{2,1,0:T(8,128)(2,1)}, u32[]{:S(2)}) copy-start(bf16[1,2048,128]{2,1,0:T(8,128)(2,1)} %gate_ref.1) | copy-start | bytes 1572868
  6.1 66.1 %copy-start.1 = (bf16[1,2048,128]{2,1,0:T(8,128)(2,1)S(1)}, bf16[1,2048,128]{2,1,0:T(8,128)(2,1)}, u32[]{:S(2)}) copy-start(bf16[1,2048,128]{2,1,0:T(8,128)(2,1)} %up_ref.1) | copy-start | bytes 1572868
  6.1 66.1 %copy-start.2 = (bf16[1,128,2048]{2,1,0:T(8,128)(2,1)S(1)}, bf16[1,128,2048]{2,1,0:T(8,128)(2,1)}, u32[]{:S(2)}) copy-start(bf16[1,128,2048]{2,1,0:T(8,128)(2,1)} %down_ref.1) | copy-start | bytes 1572868

commit v5 on v4

--- a/solution.py
+++ b/solution.py
@@ -38,18 +38,56 @@
     weight_ref,
     new_state_ref,
     out_ref,
+    state_here,
+    new_here,
+    inputs,
+    decay_here,
+    vectors,
+    weight_here,
     rows,
     read,
     joined,
     parts,
     sums,
+    arrived,
+    stored,
 ):
     f32, bf16 = jnp.float32, jnp.bfloat16
-    step = pl.program_id(0)
-    seqs, channels = reading_ref.shape
-    per_step, heads, size, _ = state_ref.shape
+    seqs, heads, size, _ = state_here.shape
+    channels = heads * size
     pairs = heads // 2
     pair_width = 2 * size
+    steps = seqs // SEQ_STEP
+
+    def state_load(step):
+        at = pl.ds(step * SEQ_STEP, SEQ_STEP)
+        return pltpu.make_async_copy(state_ref.at[at], state_here.at[at], arrived.at[step])
+
+    def state_store(step):
+        at = pl.ds(step * SEQ_STEP, SEQ_STEP)
+        return pltpu.make_async_copy(new_here.at[at], new_state_ref.at[at], stored.at[step])
+
+    small = [
+        pltpu.make_async_copy(source, target, arrived.at[steps + number])
+        for number, (source, target) in enumerate(
+            (
+                (key_ref, inputs.at[0]),
+                (learn_ref, inputs.at[1]),
+                (decay_ref, decay_here),
+                (base_ref, vectors.at[0]),
+                (reading_ref, inputs.at[2]),
+                (value_ref, inputs.at[3]),
+                (gain_ref, vectors.at[1]),
+            )
+        )
+    ]
+    weight_load = pltpu.make_async_copy(weight_ref, weight_here, arrived.at[steps + len(small)])
+    for load in small:
+        load.start()
+    for step in range(steps):
+        state_load(step).start()
+    weight_load.start()
+
     square = (pair_width, pair_width)
     same_head = (
         lax.broadcasted_iota(jnp.int32, square, 0) // size
@@ -60,111 +98,125 @@
     def head_sums(values):
         return sum(jnp.dot(part, ones, preferred_element_type=f32) for part in two_parts(values))
 
-    @pl.when(step == 0)
-    def _():
-        learning = jax.nn.sigmoid(learn_ref[...].astype(f32))
-        decay = jnp.exp(-math.exp(-0.5) * jax.nn.sigmoid(base_ref[...] + decay_ref[...]))
-        keys = key_ref[...].astype(f32)
-        read[...] = jnp.zeros_like(read)
-        for pair in range(pairs):
-            at = slice(pair * pair_width, (pair + 1) * pair_width)
-            key = keys[:, at]
-            unit = key * lax.rsqrt(head_sums(key * key) + EPSILON)
-            rows[0, pair] = unit
-            rows[1, pair] = decay[:, at]
-            rows[2, pair] = unit * learning[:, at]
-            rows[3, pair] = key
-            rows[4, pair] = reading_ref[:, at].astype(f32)
-            rows[5, pair] = value_ref[:, at].astype(f32)
+    for load in small:
+        load.wait()
+    keys = inputs[0].astype(f32)
+    learning = jax.nn.sigmoid(inputs[1].astype(f32))
+    decay = jnp.exp(-math.exp(-0.5) * jax.nn.sigmoid(vectors[0] + decay_here[...]))
+    read[...] = jnp.zeros_like(read)
+    for pair in range(pairs):
+        at = slice(pair * pair_width, (pair + 1) * pair_width)
+        key = keys[:, at]
+        unit = key * lax.rsqrt(head_sums(key * key) + EPSILON)
+        rows[0, pair] = unit
+        rows[1, pair] = decay[:, at]
+        rows[2, pair] = unit * learning[:, at]
+        rows[3, pair] = key
+        rows[4, pair] = inputs[2, :, at].astype(f32)
+        rows[5, pair] = inputs[3, :, at].astype(f32)
 
     blocks = [
         (local, pair, slice((local * pairs + pair) * size, (local * pairs + pair + 1) * size))
-        for local in range(per_step)
+        for local in range(SEQ_STEP)
         for pair in range(pairs)
     ]
-
-    def row(which, local, pair):
-        return rows[which, pair, pl.ds(step * per_step + local, 1), :]
-
     on_diagonal = lax.broadcasted_iota(jnp.int32, (size, pair_width), 0) == (
         lax.broadcasted_iota(jnp.int32, (size, pair_width), 1) % size
     )
-    for local, pair, at in blocks:
-        state = jnp.concatenate([state_ref[local, 2 * pair], state_ref[local, 2 * pair + 1]], axis=1)
-        joined[at, :] = state
-        parts[0, at, :], parts[1, at, :] = two_parts(state * row(0, local, pair))
-        parts[2, at, :] = jnp.where(on_diagonal, row(5, local, pair), 0.0).astype(bf16)
-    sums[0] = jnp.dot(parts[0], ones, preferred_element_type=f32) + jnp.dot(
-        parts[1], ones, preferred_element_type=f32
-    )
-    sums[1] = jnp.dot(parts[2], ones, preferred_element_type=f32)
-    for local, pair, at in blocks:
-        new = (
-            joined[at, :] * row(1, local, pair)
-            - sums[0, at, :] * row(2, local, pair)
-            + sums[1, at, :] * row(3, local, pair)
-        )
-        new_state_ref[local, 2 * pair] = new[:, 0:size]
-        new_state_ref[local, 2 * pair + 1] = new[:, size:pair_width]
-        parts[0, at, :], parts[1, at, :] = two_parts(new * row(4, local, pair))
     head_of = lax.broadcasted_iota(jnp.int32, (2 * 8, pair_width), 0) // 8
     pick = jnp.where(
         head_of == lax.broadcasted_iota(jnp.int32, (2 * 8, pair_width), 1) // size, 1.0, 0.0
     ).astype(bf16)
-    dims = (((1,), (1,)), ((), ()))
-    found = lax.dot_general(pick, parts[0], dims, preferred_element_type=f32) + lax.dot_general(
-        pick, parts[1], dims, preferred_element_type=f32
-    )
     seq_of = lax.broadcasted_iota(jnp.int32, (seqs, pairs * size), 0)
-    for which in range(2):
-        latest = read[which]
-        for local in range(per_step):
-            line = found[which * 8 : which * 8 + 1, local * pairs * size : (local + 1) * pairs * size]
-            latest = jnp.where(seq_of == step * per_step + local, line, latest)
-        read[which] = latest
-
-    @pl.when(step == pl.num_programs(0) - 1)
-    def _():
-        mixed = []
-        for pair in range(pairs):
-            at = slice(pair * size, (pair + 1) * size)
-            live = jnp.concatenate([read[0, :, at], read[1, :, at]], axis=1)
-            live = live - head_sums(live) * (1.0 / size)
-            spread = head_sums(jnp.square(live)) * (1.0 / size)
-            gain = gain_ref[:, pair * pair_width : (pair + 1) * pair_width]
-            mixed.append(live * lax.rsqrt(spread + GROUP_EPSILON) * gain)
-        mixed = jnp.concatenate(mixed, axis=1).astype(bf16)
-        product = jnp.dot(mixed, weight_ref[...], preferred_element_type=f32).astype(bf16)
-        for copy in range(copies):
-            out_ref[copy] = product
+
+    @pl.loop(0, steps)
+    def _(step):
+        first = step * SEQ_STEP
+
+        def row(which, local, pair):
+            return rows[which, pair, pl.ds(first + local, 1), :]
+
+        state_load(step).wait()
+        for local, pair, at in blocks:
+            parts[2, at, :] = jnp.where(on_diagonal, row(5, local, pair), 0.0).astype(bf16)
+            state = jnp.concatenate(
+                [state_here[first + local, 2 * pair], state_here[first + local, 2 * pair + 1]], axis=1
+            )
+            joined[at, :] = state
+            parts[0, at, :], parts[1, at, :] = two_parts(state * row(0, local, pair))
+        sums[0] = jnp.dot(parts[0], ones, preferred_element_type=f32) + jnp.dot(
+            parts[1], ones, preferred_element_type=f32
+        )
+        sums[1] = jnp.dot(parts[2], ones, preferred_element_type=f32)
+        for local, pair, at in blocks:
+            new = (
+                joined[at, :] * row(1, local, pair)
+                - sums[0, at, :] * row(2, local, pair)
+                + sums[1, at, :] * row(3, local, pair)
+            )
+            new_here[first + local, 2 * pair] = new[:, 0:size]
+            new_here[first + local, 2 * pair + 1] = new[:, size:pair_width]
+            parts[0, at, :], parts[1, at, :] = two_parts(new * row(4, local, pair))
+        state_store(step).start()
+        dims = (((1,), (1,)), ((), ()))
+        found = lax.dot_general(pick, parts[0], dims, preferred_element_type=f32) + lax.dot_general(
+            pick, parts[1], dims, preferred_element_type=f32
+        )
+        for which in range(2):
+            latest = read[which]
+            for local in range(SEQ_STEP):
+                line = found[
+                    which * 8 : which * 8 + 1, local * pairs * size : (local + 1) * pairs * size
+                ]
+                latest = jnp.where(seq_of == first + local, line, latest)
+            read[which] = latest
+
+    mixed = []
+    for pair in range(pairs):
+        at = slice(pair * size, (pair + 1) * size)
+        live = jnp.concatenate([read[0, :, at], read[1, :, at]], axis=1)
+        live = live - head_sums(live) * (1.0 / size)
+        spread = head_sums(jnp.square(live)) * (1.0 / size)
+        gain = vectors[1, :, pair * pair_width : (pair + 1) * pair_width]
+        mixed.append(live * lax.rsqrt(spread + GROUP_EPSILON) * gain)
+    mixed = jnp.concatenate(mixed, axis=1).astype(bf16)
+    weight_load.wait()
+    product = jnp.dot(mixed, weight_here[...], preferred_element_type=f32).astype(bf16)
+    for copy in range(copies):
+        out_ref[copy] = product
+    for step in range(steps):
+        state_store(step).wait()
 
 
 def heads_update(copies, state_in, receptance, key_in, value_in, learn_in, decay_in, decay_base, norm_gain, out_weight):
     seqs, heads, size, _ = state_in.shape
     width = out_weight.shape[1]
     channels = heads * size
-    block = pl.BlockSpec((SEQ_STEP, heads, size, size), lambda s: (s, 0, 0, 0))
-
-    def whole(shape):
-        return pl.BlockSpec(shape, lambda s: (0,) * len(shape))
-
-    tall = whole((seqs, channels))
-    flat = whole((1, channels))
+    steps = seqs // SEQ_STEP
+    step_rows = SEQ_STEP * heads // 2 * size
+    any_space = pl.BlockSpec(memory_space=pl.ANY)
     new_state, product = pl.pallas_call(
         functools.partial(heads_kernel, copies),
-        grid=(seqs // SEQ_STEP,),
-        in_specs=[block, tall, tall, tall, tall, tall, flat, flat, whole((channels, width))],
-        out_specs=[block, whole((copies, seqs, width))],
+        in_specs=[any_space] * 9,
+        out_specs=[any_space, pl.BlockSpec(memory_space=pltpu.VMEM)],
         out_shape=[
             jax.ShapeDtypeStruct(state_in.shape, jnp.float32),
             pltpu.VMEM((copies, seqs, width), jnp.bfloat16),
         ],
         scratch_shapes=[
+            pltpu.VMEM(state_in.shape, jnp.float32),
+            pltpu.VMEM(state_in.shape, jnp.float32),
+            pltpu.VMEM((4, seqs, channels), jnp.bfloat16),
+            pltpu.VMEM((seqs, channels), jnp.float32),
+            pltpu.VMEM((2, 1, channels), jnp.float32),
+            pltpu.VMEM((channels, width), jnp.bfloat16),
             pltpu.VMEM((6, heads // 2, seqs, 2 * size), jnp.float32),
             pltpu.VMEM((2, seqs, channels // 2), jnp.float32),
-            pltpu.VMEM((SEQ_STEP * heads // 2 * size, 2 * size), jnp.float32),
-            pltpu.VMEM((3, SEQ_STEP * heads // 2 * size, 2 * size), jnp.bfloat16),
-            pltpu.VMEM((2, SEQ_STEP * heads // 2 * size, 2 * size), jnp.float32),
+            pltpu.VMEM((step_rows, 2 * size), jnp.float32),
+            pltpu.VMEM((3, step_rows, 2 * size), jnp.bfloat16),
+            pltpu.VMEM((2, step_rows, 2 * size), jnp.float32),
+            pltpu.SemaphoreType.DMA((steps + 8,)),
+            pltpu.SemaphoreType.DMA((steps,)),
         ],
         compiler_params=pltpu.CompilerParams(vmem_limit_bytes=60 << 20),
         cost_estimate=pl.CostEstimate(flops=20_000_000, bytes_accessed=5_000_000, transcendentals=20_000),

time: 123 us -> 121 us (0.984)
  Pallas kernels: 7.44 us -> 6.1 us
    pallas_call x1, Pallas kernels: 5.43 us -> 4.11 us  [heads_update(): pl.pallas_call(functools.partial(heads_kernel, copies), in_specs=[any_spa...]
where the time goes in v5:
time: 121 us
  blocking collectives  113 us (93%)
  Pallas kernels  6.1 us (5%)
    all_to_all x6, blocking collectives, exchange(): return lax.all_to_all(pieces, axes, split_axis=0, concat_axis=0, tiled=True)  113 us
    pallas_call x1, Pallas kernels, heads_update(): pl.pallas_call(functools.partial(heads_kernel, copies), in_specs=[any_spa...  4.11 us

profile of v5, /device:TPU:1, one launch (start us, length us, event | category | flops | bytes accessed | tf_op | source)
XLA Modules:
  0.0 120.9 jit_solution(15091070956201540542)
XLA Ops:
  0.6 0.0 copy-start.6
  0.6 0.0 copy-start.5
  0.7 0.0 copy-start.4
  0.7 0.0 copy-start.3
  0.7 4.1 %shard_map.167 = (f32[16,4,64,64]{3,2,1,0:T(8,128)}, bf16[4,16,2048]{2,1,0:T(8,128)(2,1)S(1)}) custom-call(f32[16,4,64,64]{3,2,1,0:T(8,128)} %state_ref.1, bf16[16,256]{1,0:T(8,128)(2,1)} %reading_ref.1, bf16[16,256]{1,0:T(8,128)(2,1)} %key_ref.1, bf16[16,256]{1,0:T(8,128)(2,1)} %value_ref.1, bf16[16,256]{1,0:T(8,128)(2,1)} %learn_ref.1, ...), custom_call_target="tpu_custom_call" | custom-call | flops 20000000 | bytes 5000000 | tf_op jit(solution)/shard_map/pallas_call | solution.py:198
  4.8 0.0 copy-start
  4.8 0.0 copy-start.1
  4.8 0.0 copy-start.2
  4.8 10.5 %all_to_all.30.arrived_ref = bf16[4,16,2048]{2,1,0:T(8,128)(2,1)S(1)} all-to-all(bf16[4,16,2048]{2,1,0:T(8,128)(2,1)S(1)} %get-tuple-element.9), channel_id=1, replica_groups=mesh['zq'=8,'zp'=2,'x'=4,'c'=2,'y'=4] {'y'}, dimensions={0} | all-to-all | bytes 524288 | tf_op jit(solution)/shard_map/all_to_all | solution.py:20
  15.3 0.0 copy-done.6
  15.3 0.0 copy-done.5
  15.3 0.0 copy-done.4
  15.3 0.0 copy-done.3
  15.3 0.2 shard_map.168
  15.5 28.4 %all_to_all.31.rows_ref = bf16[8,72,128]{2,1,0:T(8,128)(2,1)S(1)} all-to-all(bf16[8,72,128]{2,1,0:T(8,128)(2,1)S(1)} %get-tuple-element.11), channel_id=1, replica_groups=mesh['zq'=8,'zp'=2,'x'=4,'c'=2,'y'=4] {'zq'}, dimensions={0} | all-to-all | bytes 294912 | tf_op jit(solution)/shard_map/all_to_all | solution.py:20
  43.8 0.4 shard_map.169
  44.3 26.7 %all_to_all.32 = bf16[64,16,512]{2,1,0:T(8,128)(2,1)S(1)} all-to-all(bf16[64,16,512]{2,1,0:T(8,128)(2,1)S(1)} %bitcast.15), channel_id=1, replica_groups=mesh['zq'=8,'zp'=2,'x'=4,'c'=2,'y'=4] {'zp','x','c','y'}, dimensions={0} | all-to-all | bytes 2097152 | tf_op jit(solution)/shard_map/all_to_all | solution.py:20
  70.9 0.0 copy-done
  70.9 0.0 copy-done.1
  70.9 0.0 copy-done.2
  70.9 1.0 shard_map.170
  72.0 22.3 %all_to_all.33 = bf16[64,16,512]{2,1,0:T(8,128)(2,1)S(1)} all-to-all(bf16[64,16,512]{2,1,0:T(8,128)(2,1)S(1)} %bitcast.13), channel_id=1, replica_groups=mesh['zq'=8,'zp'=2,'x'=4,'c'=2,'y'=4] {'zp','x','c','y'}, dimensions={0} | all-to-all | bytes 2097152 | tf_op jit(solution)/shard_map/all_to_all | solution.py:20
  94.3 0.4 shard_map.171
  94.7 15.5 %all_to_all.34 = bf16[8,16,512]{2,1,0:T(8,128)(2,1)S(1)} all-to-all(bf16[8,16,512]{2,1,0:T(8,128)(2,1)S(1)} %shard_map.171), channel_id=1, replica_groups=mesh['zq'=8,'zp'=2,'x'=4,'c'=2,'y'=4] {'zq'}, dimensions={0} | all-to-all | bytes 262144 | tf_op jit(solution)/shard_map/all_to_all | solution.py:20
  110.3 10.0 %all_to_all.35 = bf16[4,16,512]{2,1,0:T(8,128)(2,1)S(1)} all-to-all(bf16[4,16,512]{2,1,0:T(8,128)(2,1)S(1)} %broadcast_in_dim.3), channel_id=1, replica_groups=mesh['zq'=8,'zp'=2,'x'=4,'c'=2,'y'=4] {'y'}, dimensions={0} | all-to-all | bytes 131072 | tf_op jit(solution)/shard_map/all_to_all | solution.py:20
  120.3 0.6 copy.19
  (3 shorter events, 0.0 us)
Async XLA Ops:
  0.6 14.7 %copy-start.6 = (f32[16,6]{0,1:T(8,128)S(1)}, f32[16,6]{0,1:T(8,128)}, u32[]{:S(2)}) copy-start(f32[16,6]{0,1:T(8,128)} %param.31) | copy-start | bytes 1156
  0.6 14.6 %copy-start.5 = (s32[16,6]{0,1:T(8,128)S(1)}, s32[16,6]{0,1:T(8,128)}, u32[]{:S(2)}) copy-start(s32[16,6]{0,1:T(8,128)} %param.30) | copy-start | bytes 1156
  0.7 14.6 %copy-start.4 = (f32[2048]{0:T(1024)S(1)}, f32[2048]{0:T(1024)}, u32[]{:S(2)}) copy-start(f32[2048]{0:T(1024)} %param.26) | copy-start | bytes 24580
  0.7 14.6 %copy-start.3 = (bf16[16,2048]{1,0:T(8,128)(2,1)S(1)}, bf16[16,2048]{1,0:T(8,128)(2,1)}, u32[]{:S(2)}) copy-start(bf16[16,2048]{1,0:T(8,128)(2,1)} %hidden_ref.1) | copy-start | bytes 196612
  4.8 66.1 %copy-start = (bf16[1,2048,128]{2,1,0:T(8,128)(2,1)S(1)}, bf16[1,2048,128]{2,1,0:T(8,128)(2,1)}, u32[]{:S(2)}) copy-start(bf16[1,2048,128]{2,1,0:T(8,128)(2,1)} %gate_ref.1) | copy-start | bytes 1572868
  4.8 66.1 %copy-start.1 = (bf16[1,2048,128]{2,1,0:T(8,128)(2,1)S(1)}, bf16[1,2048,128]{2,1,0:T(8,128)(2,1)}, u32[]{:S(2)}) copy-start(bf16[1,2048,128]{2,1,0:T(8,128)(2,1)} %up_ref.1) | copy-start | bytes 1572868
  4.8 66.1 %copy-start.2 = (bf16[1,128,2048]{2,1,0:T(8,128)(2,1)S(1)}, bf16[1,128,2048]{2,1,0:T(8,128)(2,1)}, u32[]{:S(2)}) copy-start(bf16[1,128,2048]{2,1,0:T(8,128)(2,1)} %down_ref.1) | copy-start | bytes 1572868

commit v6 on v5

--- a/solution.py
+++ b/solution.py
@@ -103,7 +103,6 @@
     keys = inputs[0].astype(f32)
     learning = jax.nn.sigmoid(inputs[1].astype(f32))
     decay = jnp.exp(-math.exp(-0.5) * jax.nn.sigmoid(vectors[0] + decay_here[...]))
-    read[...] = jnp.zeros_like(read)
     for pair in range(pairs):
         at = slice(pair * pair_width, (pair + 1) * pair_width)
         key = keys[:, at]
@@ -127,49 +126,47 @@
     pick = jnp.where(
         head_of == lax.broadcasted_iota(jnp.int32, (2 * 8, pair_width), 1) // size, 1.0, 0.0
     ).astype(bf16)
-    seq_of = lax.broadcasted_iota(jnp.int32, (seqs, pairs * size), 0)
-
-    @pl.loop(0, steps)
-    def _(step):
+
+    for step in range(steps):
         first = step * SEQ_STEP
 
         def row(which, local, pair):
-            return rows[which, pair, pl.ds(first + local, 1), :]
+            return rows[which, pair, first + local : first + local + 1, :]
 
         state_load(step).wait()
         for local, pair, at in blocks:
-            parts[2, at, :] = jnp.where(on_diagonal, row(5, local, pair), 0.0).astype(bf16)
+            parts[step, 2, at, :] = jnp.where(on_diagonal, row(5, local, pair), 0.0).astype(bf16)
             state = jnp.concatenate(
                 [state_here[first + local, 2 * pair], state_here[first + local, 2 * pair + 1]], axis=1
             )
-            joined[at, :] = state
-            parts[0, at, :], parts[1, at, :] = two_parts(state * row(0, local, pair))
-        sums[0] = jnp.dot(parts[0], ones, preferred_element_type=f32) + jnp.dot(
-            parts[1], ones, preferred_element_type=f32
+            joined[step, at, :] = state
+            parts[step, 0, at, :], parts[step, 1, at, :] = two_parts(state * row(0, local, pair))
+        sums[step, 0] = jnp.dot(parts[step, 0], ones, preferred_element_type=f32) + jnp.dot(
+            parts[step, 1], ones, preferred_element_type=f32
         )
-        sums[1] = jnp.dot(parts[2], ones, preferred_element_type=f32)
+        sums[step, 1] = jnp.dot(parts[step, 2], ones, preferred_element_type=f32)
         for local, pair, at in blocks:
             new = (
-                joined[at, :] * row(1, local, pair)
-                - sums[0, at, :] * row(2, local, pair)
-                + sums[1, at, :] * row(3, local, pair)
+                joined[step, at, :] * row(1, local, pair)
+                - sums[step, 0, at, :] * row(2, local, pair)
+                + sums[step, 1, at, :] * row(3, local, pair)
             )
             new_here[first + local, 2 * pair] = new[:, 0:size]
             new_here[first + local, 2 * pair + 1] = new[:, size:pair_width]
-            parts[0, at, :], parts[1, at, :] = two_parts(new * row(4, local, pair))
+            parts[step, 0, at, :], parts[step, 1, at, :] = two_parts(new * row(4, local, pair))
         state_store(step).start()
-        dims = (((1,), (1,)), ((), ()))
-        found = lax.dot_general(pick, parts[0], dims, preferred_element_type=f32) + lax.dot_general(
-            pick, parts[1], dims, preferred_element_type=f32
-        )
+
+    dims = (((1,), (1,)), ((), ()))
+    lines = [[], []]
+    for step in range(steps):
+        found = lax.dot_general(pick, parts[step, 0], dims, preferred_element_type=f32)
+        found += lax.dot_general(pick, parts[step, 1], dims, preferred_element_type=f32)
         for which in range(2):
-            latest = read[which]
             for local in range(SEQ_STEP):
-                line = found[
-                    which * 8 : which * 8 + 1, local * pairs * size : (local + 1) * pairs * size
-                ]
-                latest = jnp.where(seq_of == first + local, line, latest)
-            read[which] = latest
+                at = slice(local * pairs * size, (local + 1) * pairs * size)
+                lines[which].append(found[which * 8 : which * 8 + 1, at])
+    for which in range(2):
+        read[which] = jnp.concatenate(lines[which], axis=0)
 
     mixed = []
     for pair in range(pairs):
@@ -212,9 +209,9 @@
             pltpu.VMEM((channels, width), jnp.bfloat16),
             pltpu.VMEM((6, heads // 2, seqs, 2 * size), jnp.float32),
             pltpu.VMEM((2, seqs, channels // 2), jnp.float32),
-            pltpu.VMEM((step_rows, 2 * size), jnp.float32),
-            pltpu.VMEM((3, step_rows, 2 * size), jnp.bfloat16),
-            pltpu.VMEM((2, step_rows, 2 * size), jnp.float32),
+            pltpu.VMEM((steps, step_rows, 2 * size), jnp.float32),
+            pltpu.VMEM((steps, 3, step_rows, 2 * size), jnp.bfloat16),
+            pltpu.VMEM((steps, 2, step_rows, 2 * size), jnp.float32),
             pltpu.SemaphoreType.DMA((steps + 8,)),
             pltpu.SemaphoreType.DMA((steps,)),
         ],
@@ -239,10 +236,15 @@
     senders, n_y, rows, quarter = got_ref.shape
     for y in range(n_y):
         flat[:, y * quarter : (y + 1) * quarter] = got_ref[:, y].reshape(senders * rows, quarter)
-    arrived = flat[...]
-    gate = jnp.dot(arrived, gate_ref[0], preferred_element_type=f32)
-    upward = jnp.dot(arrived, up_ref[0], preferred_element_type=f32)
-    hidden = (gate * jax.nn.sigmoid(gate) * upward).astype(jnp.bfloat16)
+    units = gate_ref.shape[2]
+    weights = jnp.concatenate([gate_ref[0], up_ref[0]], axis=1)
+    half = senders * rows // 2
+    hidden = []
+    for first in (0, half):
+        both = jnp.dot(flat[first : first + half], weights, preferred_element_type=f32)
+        gate, upward = both[:, :units], both[:, units:]
+        hidden.append((gate * jax.nn.sigmoid(gate) * upward).astype(jnp.bfloat16))
+    hidden = jnp.concatenate(hidden, axis=0)
     for y in range(n_y):
         partial = jnp.dot(
             hidden, down_ref[0, :, y * quarter : (y + 1) * quarter], preferred_element_type=f32

time: 121 us -> 121 us (level)
  no operation moved by 1% of the time
where the time goes in v6:
time: 121 us
  blocking collectives  113 us (93%)
  Pallas kernels  5.86 us (5%)
    all_to_all x6, blocking collectives, exchange(): return lax.all_to_all(pieces, axes, split_axis=0, concat_axis=0, tiled=True)  113 us
    pallas_call x1, Pallas kernels, heads_update(): pl.pallas_call(functools.partial(heads_kernel, copies), in_specs=[any_spa...  4.09 us

profile of v6, /device:TPU:1, one launch (start us, length us, event | category | flops | bytes accessed | tf_op | source)
XLA Modules:
  0.0 120.7 jit_solution(17891769473418163984)
XLA Ops:
  0.6 0.0 copy-start.6
  0.6 0.0 copy-start.5
  0.7 0.0 copy-start.4
  0.7 0.0 copy-start.3
  0.7 4.1 %shard_map.167 = (f32[16,4,64,64]{3,2,1,0:T(8,128)}, bf16[4,16,2048]{2,1,0:T(8,128)(2,1)S(1)}) custom-call(f32[16,4,64,64]{3,2,1,0:T(8,128)} %state_ref.1, bf16[16,256]{1,0:T(8,128)(2,1)} %reading_ref.1, bf16[16,256]{1,0:T(8,128)(2,1)} %key_ref.1, bf16[16,256]{1,0:T(8,128)(2,1)} %value_ref.1, bf16[16,256]{1,0:T(8,128)(2,1)} %learn_ref.1, ...), custom_call_target="tpu_custom_call" | custom-call | flops 20000000 | bytes 5000000 | tf_op jit(solution)/shard_map/pallas_call | solution.py:195
  4.8 0.0 copy-start
  4.8 0.0 copy-start.1
  4.8 0.0 copy-start.2
  4.8 10.5 %all_to_all.30.arrived_ref = bf16[4,16,2048]{2,1,0:T(8,128)(2,1)S(1)} all-to-all(bf16[4,16,2048]{2,1,0:T(8,128)(2,1)S(1)} %get-tuple-element.9), channel_id=1, replica_groups=mesh['zq'=8,'zp'=2,'x'=4,'c'=2,'y'=4] {'y'}, dimensions={0} | all-to-all | bytes 524288 | tf_op jit(solution)/shard_map/all_to_all | solution.py:20
  15.3 0.0 copy-done.6
  15.3 0.0 copy-done.5
  15.3 0.0 copy-done.4
  15.3 0.0 copy-done.3
  15.3 0.2 shard_map.168
  15.5 28.4 %all_to_all.31.rows_ref = bf16[8,72,128]{2,1,0:T(8,128)(2,1)S(1)} all-to-all(bf16[8,72,128]{2,1,0:T(8,128)(2,1)S(1)} %get-tuple-element.11), channel_id=1, replica_groups=mesh['zq'=8,'zp'=2,'x'=4,'c'=2,'y'=4] {'zq'}, dimensions={0} | all-to-all | bytes 294912 | tf_op jit(solution)/shard_map/all_to_all | solution.py:20
  43.8 0.4 shard_map.169
  44.2 26.7 %all_to_all.32 = bf16[64,16,512]{2,1,0:T(8,128)(2,1)S(1)} all-to-all(bf16[64,16,512]{2,1,0:T(8,128)(2,1)S(1)} %bitcast.15), channel_id=1, replica_groups=mesh['zq'=8,'zp'=2,'x'=4,'c'=2,'y'=4] {'zp','x','c','y'}, dimensions={0} | all-to-all | bytes 2097152 | tf_op jit(solution)/shard_map/all_to_all | solution.py:20
  70.9 0.0 copy-done
  70.9 0.0 copy-done.1
  70.9 0.0 copy-done.2
  70.9 0.8 shard_map.170
  71.7 22.4 %all_to_all.33 = bf16[64,16,512]{2,1,0:T(8,128)(2,1)S(1)} all-to-all(bf16[64,16,512]{2,1,0:T(8,128)(2,1)S(1)} %bitcast.13), channel_id=1, replica_groups=mesh['zq'=8,'zp'=2,'x'=4,'c'=2,'y'=4] {'zp','x','c','y'}, dimensions={0} | all-to-all | bytes 2097152 | tf_op jit(solution)/shard_map/all_to_all | solution.py:20
  94.1 0.4 shard_map.171
  94.5 15.5 %all_to_all.34 = bf16[8,16,512]{2,1,0:T(8,128)(2,1)S(1)} all-to-all(bf16[8,16,512]{2,1,0:T(8,128)(2,1)S(1)} %shard_map.171), channel_id=1, replica_groups=mesh['zq'=8,'zp'=2,'x'=4,'c'=2,'y'=4] {'zq'}, dimensions={0} | all-to-all | bytes 262144 | tf_op jit(solution)/shard_map/all_to_all | solution.py:20
  110.0 10.0 %all_to_all.35 = bf16[4,16,512]{2,1,0:T(8,128)(2,1)S(1)} all-to-all(bf16[4,16,512]{2,1,0:T(8,128)(2,1)S(1)} %broadcast_in_dim.3), channel_id=1, replica_groups=mesh['zq'=8,'zp'=2,'x'=4,'c'=2,'y'=4] {'y'}, dimensions={0} | all-to-all | bytes 131072 | tf_op jit(solution)/shard_map/all_to_all | solution.py:20
  120.1 0.6 copy.19
  (3 shorter events, 0.0 us)
Async XLA Ops:
  0.6 14.6 %copy-start.6 = (f32[16,6]{0,1:T(8,128)S(1)}, f32[16,6]{0,1:T(8,128)}, u32[]{:S(2)}) copy-start(f32[16,6]{0,1:T(8,128)} %param.31) | copy-start | bytes 1156
  0.6 14.6 %copy-start.5 = (s32[16,6]{0,1:T(8,128)S(1)}, s32[16,6]{0,1:T(8,128)}, u32[]{:S(2)}) copy-start(s32[16,6]{0,1:T(8,128)} %param.30) | copy-start | bytes 1156
  0.7 14.6 %copy-start.4 = (f32[2048]{0:T(1024)S(1)}, f32[2048]{0:T(1024)}, u32[]{:S(2)}) copy-start(f32[2048]{0:T(1024)} %param.26) | copy-start | bytes 24580
  0.7 14.6 %copy-start.3 = (bf16[16,2048]{1,0:T(8,128)(2,1)S(1)}, bf16[16,2048]{1,0:T(8,128)(2,1)}, u32[]{:S(2)}) copy-start(bf16[16,2048]{1,0:T(8,128)(2,1)} %hidden_ref.1) | copy-start | bytes 196612
  4.8 66.1 %copy-start = (bf16[1,2048,128]{2,1,0:T(8,128)(2,1)S(1)}, bf16[1,2048,128]{2,1,0:T(8,128)(2,1)}, u32[]{:S(2)}) copy-start(bf16[1,2048,128]{2,1,0:T(8,128)(2,1)} %gate_ref.1) | copy-start | bytes 1572868
  4.8 66.1 %copy-start.1 = (bf16[1,2048,128]{2,1,0:T(8,128)(2,1)S(1)}, bf16[1,2048,128]{2,1,0:T(8,128)(2,1)}, u32[]{:S(2)}) copy-start(bf16[1,2048,128]{2,1,0:T(8,128)(2,1)} %up_ref.1) | copy-start | bytes 1572868
  4.8 66.1 %copy-start.2 = (bf16[1,128,2048]{2,1,0:T(8,128)(2,1)S(1)}, bf16[1,128,2048]{2,1,0:T(8,128)(2,1)}, u32[]{:S(2)}) copy-start(bf16[1,128,2048]{2,1,0:T(8,128)(2,1)} %down_ref.1) | copy-start | bytes 1572868

commit v7 on v6

--- a/solution.py
+++ b/solution.py
@@ -26,7 +26,7 @@
 
 
 def heads_kernel(
-    copies,
+    owners,
     state_ref,
     reading_ref,
     key_ref,
@@ -179,13 +179,14 @@
     mixed = jnp.concatenate(mixed, axis=1).astype(bf16)
     weight_load.wait()
     product = jnp.dot(mixed, weight_here[...], preferred_element_type=f32).astype(bf16)
-    for copy in range(copies):
-        out_ref[copy] = product
+    quarter = out_ref.shape[2]
+    for owner in range(owners):
+        out_ref[owner] = product[:, owner * quarter : (owner + 1) * quarter]
     for step in range(steps):
         state_store(step).wait()
 
 
-def heads_update(copies, state_in, receptance, key_in, value_in, learn_in, decay_in, decay_base, norm_gain, out_weight):
+def heads_update(owners, state_in, receptance, key_in, value_in, learn_in, decay_in, decay_base, norm_gain, out_weight):
     seqs, heads, size, _ = state_in.shape
     width = out_weight.shape[1]
     channels = heads * size
@@ -193,12 +194,12 @@
     step_rows = SEQ_STEP * heads // 2 * size
     any_space = pl.BlockSpec(memory_space=pl.ANY)
     new_state, product = pl.pallas_call(
-        functools.partial(heads_kernel, copies),
+        functools.partial(heads_kernel, owners),
         in_specs=[any_space] * 9,
         out_specs=[any_space, pl.BlockSpec(memory_space=pltpu.VMEM)],
         out_shape=[
             jax.ShapeDtypeStruct(state_in.shape, jnp.float32),
-            pltpu.VMEM((copies, seqs, width), jnp.bfloat16),
+            pltpu.VMEM((owners, seqs, width // owners), jnp.bfloat16),
         ],
         scratch_shapes=[
             pltpu.VMEM(state_in.shape, jnp.float32),
@@ -231,17 +232,25 @@
     return product, new_state
 
 
-def expert_kernel(got_ref, gate_ref, up_ref, down_ref, out_ref, flat):
+def expert_kernel(got_ref, gain_ref, gate_ref, up_ref, down_ref, out_ref, flat):
     f32 = jnp.float32
     senders, n_y, rows, quarter = got_ref.shape
+    power = jnp.zeros((senders * rows, 128), f32)
     for y in range(n_y):
         flat[:, y * quarter : (y + 1) * quarter] = got_ref[:, y].reshape(senders * rows, quarter)
+        for first in range(y * quarter, (y + 1) * quarter, 128):
+            at = slice(first, first + 128)
+            original = flat[:, at].astype(f32) * (1.0 / gain_ref[:, at])
+            power += original * original
+    mean = jnp.sum(power, axis=1, keepdims=True) * (1.0 / (n_y * quarter))
+    scale = lax.rsqrt(mean + EPSILON)
     units = gate_ref.shape[2]
     weights = jnp.concatenate([gate_ref[0], up_ref[0]], axis=1)
     half = senders * rows // 2
     hidden = []
     for first in (0, half):
         both = jnp.dot(flat[first : first + half], weights, preferred_element_type=f32)
+        both = both * scale[first : first + half]
         gate, upward = both[:, :units], both[:, units:]
         hidden.append((gate * jax.nn.sigmoid(gate) * upward).astype(jnp.bfloat16))
     hidden = jnp.concatenate(hidden, axis=0)
@@ -252,35 +261,31 @@
         out_ref[:, y] = partial.astype(jnp.bfloat16).reshape(senders, rows, quarter)
 
 
-def experts(got, expert_gate, expert_up, expert_down):
+def experts(got, routed_gain, expert_gate, expert_up, expert_down):
     senders, n_y, rows, quarter = got.shape
     vmem = pl.BlockSpec(memory_space=pltpu.VMEM)
     return pl.pallas_call(
         expert_kernel,
-        in_specs=[vmem] * 4,
+        in_specs=[vmem] * 5,
         out_specs=vmem,
         out_shape=jax.ShapeDtypeStruct(got.shape, jnp.bfloat16),
         scratch_shapes=[pltpu.VMEM((senders * rows, n_y * quarter), jnp.bfloat16)],
         compiler_params=pltpu.CompilerParams(vmem_limit_bytes=12 << 20),
         cost_estimate=pl.CostEstimate(flops=400_000_000, bytes_accessed=4_000_000, transcendentals=40_000),
-    )(got, expert_gate, expert_up, expert_down)
+    )(got, routed_gain.reshape(1, n_y * quarter), expert_gate, expert_up, expert_down)
 
 
 def pack_kernel(
     arrived_ref, hidden_ref, gain_ref, ids_ref, weights_ref, parcels_ref, own_ref
 ):
     f32, bf16 = jnp.float32, jnp.bfloat16
-    seqs, width = hidden_ref.shape
-    quarter = own_ref.shape[1]
+    seqs, quarter = own_ref.shape
     top = ids_ref.shape[0]
+    at = pl.ds(pl.multiple_of(lax.axis_index("y") * quarter, quarter), quarter)
     attention = jnp.sum(arrived_ref[...].astype(f32), axis=0).astype(bf16)
-    residual = hidden_ref[...].astype(f32) + attention.astype(f32)
-    scale = lax.rsqrt(jnp.mean(residual * residual, axis=1, keepdims=True) + EPSILON)
-    at = pl.ds(pl.multiple_of(lax.axis_index("y") * quarter, quarter), quarter)
-    attention = jnp.sum(arrived_ref[:, :, at].astype(f32), axis=0).astype(bf16)
     residual = hidden_ref[:, at].astype(f32) + attention.astype(f32)
     own_ref[...] = residual
-    normed = (residual * scale * gain_ref[:, at]).astype(bf16)
+    gained = (residual * gain_ref[:, at]).astype(bf16)
 
     weights = weights_ref[...]
     routing = jnp.zeros((8, 128), f32)
@@ -297,15 +302,15 @@
     chunks = quarter // 128
     for z in range(parcels_ref.shape[0]):
         for chunk in range(chunks):
-            parcels_ref[z, chunk * seqs : (chunk + 1) * seqs, :] = normed[
+            parcels_ref[z, chunk * seqs : (chunk + 1) * seqs, :] = gained[
                 :, chunk * 128 : (chunk + 1) * 128
             ]
         parcels_ref[z, chunks * seqs : chunks * seqs + 8, :] = routing
 
 
 def pack(arrived, hidden_in, routed_gain, route_ids, route_weights, n_z):
-    n_y, seqs, width = arrived.shape
-    quarter = width // n_y
+    n_y, seqs, quarter = arrived.shape
+    width = n_y * quarter
     vmem = pl.BlockSpec(memory_space=pltpu.VMEM)
     return pl.pallas_call(
         pack_kernel,
@@ -468,7 +473,7 @@
     rows = exchange(parcels, "zq")
     chosen, place, weight = choose(rows, near, n_y, SLOTS, route_ids.shape[1], seqs)
     got = exchange(chosen.reshape(near * n_y, per_expert, quarter), NEAR_AXES)
-    back = experts(got.reshape(near, n_y, per_expert, quarter), expert_gate, expert_up, expert_down)
+    back = experts(got.reshape(near, n_y, per_expert, quarter), routed_gain, expert_gate, expert_up, expert_down)
     returned = exchange(back.reshape(near * n_y, per_expert, quarter), NEAR_AXES)
     combined = combine(returned.reshape(near, n_y, per_expert, quarter), place, weight, n_zq)
     routed = exchange(combined, "zq").astype(jnp.float32).sum(axis=0)

time: 121 us -> 120 us (level)
  no operation moved by 1% of the time
where the time goes in v7:
time: 120 us
  blocking collectives  112 us (93%)
  Pallas kernels  5.97 us (5%)
    all_to_all x6, blocking collectives, exchange(): return lax.all_to_all(pieces, axes, split_axis=0, concat_axis=0, tiled=True)  112 us
    pallas_call x1, Pallas kernels, heads_update(): pl.pallas_call(functools.partial(heads_kernel, owners), in_specs=[any_spa...  4.09 us

profile of v7, /device:TPU:1, one launch (start us, length us, event | category | flops | bytes accessed | tf_op | source)
XLA Modules:
  0.0 119.8 jit_solution(3283708875569431974)
XLA Ops:
  0.6 0.0 copy-start.6
  0.6 0.0 copy-start.5
  0.7 0.0 copy-start.4
  0.7 0.0 copy-start.3
  0.7 4.1 %shard_map.167 = (f32[16,4,64,64]{3,2,1,0:T(8,128)}, bf16[4,16,512]{2,1,0:T(8,128)(2,1)S(1)}) custom-call(f32[16,4,64,64]{3,2,1,0:T(8,128)} %state_ref.1, bf16[16,256]{1,0:T(8,128)(2,1)} %reading_ref.1, bf16[16,256]{1,0:T(8,128)(2,1)} %key_ref.1, bf16[16,256]{1,0:T(8,128)(2,1)} %value_ref.1, bf16[16,256]{1,0:T(8,128)(2,1)} %learn_ref.1, ...), custom_call_target="tpu_custom_call" | custom-call | flops 20000000 | bytes 5000000 | tf_op jit(solution)/shard_map/pallas_call | solution.py:196
  4.8 0.0 copy-start
  4.8 0.0 copy-start.1
  4.8 0.0 copy-start.2
  4.8 9.4 %all_to_all.30.arrived_ref = bf16[4,16,512]{2,1,0:T(8,128)(2,1)S(1)} all-to-all(bf16[4,16,512]{2,1,0:T(8,128)(2,1)S(1)} %get-tuple-element.9), channel_id=1, replica_groups=mesh['zq'=8,'zp'=2,'x'=4,'c'=2,'y'=4] {'y'}, dimensions={0} | all-to-all | bytes 131072 | tf_op jit(solution)/shard_map/all_to_all | solution.py:20
  14.2 0.0 copy-done.6
  14.2 0.0 copy-done.5
  14.2 0.0 copy-done.4
  14.2 0.0 copy-done.3
  14.2 0.1 shard_map.168
  14.3 28.4 %all_to_all.31.rows_ref = bf16[8,72,128]{2,1,0:T(8,128)(2,1)S(1)} all-to-all(bf16[8,72,128]{2,1,0:T(8,128)(2,1)S(1)} %get-tuple-element.11), channel_id=1, replica_groups=mesh['zq'=8,'zp'=2,'x'=4,'c'=2,'y'=4] {'zq'}, dimensions={0} | all-to-all | bytes 294912 | tf_op jit(solution)/shard_map/all_to_all | solution.py:20
  42.7 0.4 shard_map.169
  43.1 26.8 %all_to_all.32 = bf16[64,16,512]{2,1,0:T(8,128)(2,1)S(1)} all-to-all(bf16[64,16,512]{2,1,0:T(8,128)(2,1)S(1)} %bitcast.15), channel_id=1, replica_groups=mesh['zq'=8,'zp'=2,'x'=4,'c'=2,'y'=4] {'zp','x','c','y'}, dimensions={0} | all-to-all | bytes 2097152 | tf_op jit(solution)/shard_map/all_to_all | solution.py:20
  69.9 0.0 copy-done
  69.9 0.0 copy-done.1
  69.9 0.0 copy-done.2
  69.9 1.0 shard_map.170
  70.9 22.4 %all_to_all.33 = bf16[64,16,512]{2,1,0:T(8,128)(2,1)S(1)} all-to-all(bf16[64,16,512]{2,1,0:T(8,128)(2,1)S(1)} %bitcast.13), channel_id=1, replica_groups=mesh['zq'=8,'zp'=2,'x'=4,'c'=2,'y'=4] {'zp','x','c','y'}, dimensions={0} | all-to-all | bytes 2097152 | tf_op jit(solution)/shard_map/all_to_all | solution.py:20
  93.3 0.4 shard_map.171
  93.6 15.5 %all_to_all.34 = bf16[8,16,512]{2,1,0:T(8,128)(2,1)S(1)} all-to-all(bf16[8,16,512]{2,1,0:T(8,128)(2,1)S(1)} %shard_map.171), channel_id=1, replica_groups=mesh['zq'=8,'zp'=2,'x'=4,'c'=2,'y'=4] {'zq'}, dimensions={0} | all-to-all | bytes 262144 | tf_op jit(solution)/shard_map/all_to_all | solution.py:20
  109.2 10.0 %all_to_all.35 = bf16[4,16,512]{2,1,0:T(8,128)(2,1)S(1)} all-to-all(bf16[4,16,512]{2,1,0:T(8,128)(2,1)S(1)} %broadcast_in_dim.3), channel_id=1, replica_groups=mesh['zq'=8,'zp'=2,'x'=4,'c'=2,'y'=4] {'y'}, dimensions={0} | all-to-all | bytes 131072 | tf_op jit(solution)/shard_map/all_to_all | solution.py:20
  119.2 0.6 copy.19
  (3 shorter events, 0.0 us)
Async XLA Ops:
  0.6 13.6 %copy-start.6 = (f32[16,6]{0,1:T(8,128)S(1)}, f32[16,6]{0,1:T(8,128)}, u32[]{:S(2)}) copy-start(f32[16,6]{0,1:T(8,128)} %param.31) | copy-start | bytes 1156
  0.6 13.6 %copy-start.5 = (s32[16,6]{0,1:T(8,128)S(1)}, s32[16,6]{0,1:T(8,128)}, u32[]{:S(2)}) copy-start(s32[16,6]{0,1:T(8,128)} %param.30) | copy-start | bytes 1156
  0.7 13.6 %copy-start.4 = (f32[2048]{0:T(1024)S(1)}, f32[2048]{0:T(1024)}, u32[]{:S(2)}) copy-start(f32[2048]{0:T(1024)} %param.26) | copy-start | bytes 24580
  0.7 13.6 %copy-start.3 = (bf16[16,2048]{1,0:T(8,128)(2,1)S(1)}, bf16[16,2048]{1,0:T(8,128)(2,1)}, u32[]{:S(2)}) copy-start(bf16[16,2048]{1,0:T(8,128)(2,1)} %hidden_ref.1) | copy-start | bytes 196612
  4.8 65.1 %copy-start = (bf16[1,2048,128]{2,1,0:T(8,128)(2,1)S(1)}, bf16[1,2048,128]{2,1,0:T(8,128)(2,1)}, u32[]{:S(2)}) copy-start(bf16[1,2048,128]{2,1,0:T(8,128)(2,1)} %gate_ref.1) | copy-start | bytes 1572868
  4.8 65.1 %copy-start.1 = (bf16[1,2048,128]{2,1,0:T(8,128)(2,1)S(1)}, bf16[1,2048,128]{2,1,0:T(8,128)(2,1)}, u32[]{:S(2)}) copy-start(bf16[1,2048,128]{2,1,0:T(8,128)(2,1)} %up_ref.1) | copy-start | bytes 1572868
  4.8 65.1 %copy-start.2 = (bf16[1,128,2048]{2,1,0:T(8,128)(2,1)S(1)}, bf16[1,128,2048]{2,1,0:T(8,128)(2,1)}, u32[]{:S(2)}) copy-start(bf16[1,128,2048]{2,1,0:T(8,128)(2,1)} %down_ref.1) | copy-start | bytes 1572868

commit v8 on v7

--- a/solution.py
+++ b/solution.py
@@ -38,8 +38,9 @@
     weight_ref,
     new_state_ref,
     out_ref,
+    late_ref,
     state_here,
-    new_here,
+    early,
     inputs,
     decay_here,
     vectors,
@@ -57,15 +58,13 @@
     channels = heads * size
     pairs = heads // 2
     pair_width = 2 * size
-    steps = seqs // SEQ_STEP
+    steps = 2
 
     def state_load(step):
         at = pl.ds(step * SEQ_STEP, SEQ_STEP)
         return pltpu.make_async_copy(state_ref.at[at], state_here.at[at], arrived.at[step])
 
-    def state_store(step):
-        at = pl.ds(step * SEQ_STEP, SEQ_STEP)
-        return pltpu.make_async_copy(new_here.at[at], new_state_ref.at[at], stored.at[step])
+    store = pltpu.make_async_copy(early, new_state_ref.at[pl.ds(0, SEQ_STEP)], stored)
 
     small = [
         pltpu.make_async_copy(source, target, arrived.at[steps + number])
@@ -151,10 +150,12 @@
                 - sums[step, 0, at, :] * row(2, local, pair)
                 + sums[step, 1, at, :] * row(3, local, pair)
             )
-            new_here[first + local, 2 * pair] = new[:, 0:size]
-            new_here[first + local, 2 * pair + 1] = new[:, size:pair_width]
+            target = early if step == 0 else late_ref
+            target[local, 2 * pair] = new[:, 0:size]
+            target[local, 2 * pair + 1] = new[:, size:pair_width]
             parts[step, 0, at, :], parts[step, 1, at, :] = two_parts(new * row(4, local, pair))
-        state_store(step).start()
+        if step == 0:
+            store.start()
 
     dims = (((1,), (1,)), ((), ()))
     lines = [[], []]
@@ -182,28 +183,29 @@
     quarter = out_ref.shape[2]
     for owner in range(owners):
         out_ref[owner] = product[:, owner * quarter : (owner + 1) * quarter]
-    for step in range(steps):
-        state_store(step).wait()
+    store.wait()
 
 
 def heads_update(owners, state_in, receptance, key_in, value_in, learn_in, decay_in, decay_base, norm_gain, out_weight):
     seqs, heads, size, _ = state_in.shape
     width = out_weight.shape[1]
     channels = heads * size
-    steps = seqs // SEQ_STEP
+    steps = 2
     step_rows = SEQ_STEP * heads // 2 * size
     any_space = pl.BlockSpec(memory_space=pl.ANY)
-    new_state, product = pl.pallas_call(
+    half_shape = (SEQ_STEP, heads, size, size)
+    new_state, product, late = pl.pallas_call(
         functools.partial(heads_kernel, owners),
         in_specs=[any_space] * 9,
-        out_specs=[any_space, pl.BlockSpec(memory_space=pltpu.VMEM)],
+        out_specs=[any_space] + [pl.BlockSpec(memory_space=pltpu.VMEM)] * 2,
         out_shape=[
             jax.ShapeDtypeStruct(state_in.shape, jnp.float32),
             pltpu.VMEM((owners, seqs, width // owners), jnp.bfloat16),
+            pltpu.VMEM(half_shape, jnp.float32),
         ],
         scratch_shapes=[
             pltpu.VMEM(state_in.shape, jnp.float32),
-            pltpu.VMEM(state_in.shape, jnp.float32),
+            pltpu.VMEM(half_shape, jnp.float32),
             pltpu.VMEM((4, seqs, channels), jnp.bfloat16),
             pltpu.VMEM((seqs, channels), jnp.float32),
             pltpu.VMEM((2, 1, channels), jnp.float32),
@@ -214,7 +216,7 @@
             pltpu.VMEM((steps, 3, step_rows, 2 * size), jnp.bfloat16),
             pltpu.VMEM((steps, 2, step_rows, 2 * size), jnp.float32),
             pltpu.SemaphoreType.DMA((steps + 8,)),
-            pltpu.SemaphoreType.DMA((steps,)),
+            pltpu.SemaphoreType.DMA,
         ],
         compiler_params=pltpu.CompilerParams(vmem_limit_bytes=60 << 20),
         cost_estimate=pl.CostEstimate(flops=20_000_000, bytes_accessed=5_000_000, transcendentals=20_000),
@@ -229,11 +231,17 @@
         norm_gain.reshape(1, channels),
         out_weight,
     )
-    return product, new_state
-
-
-def expert_kernel(got_ref, gain_ref, gate_ref, up_ref, down_ref, out_ref, flat):
+    return product, new_state, late
+
+
+def expert_kernel(
+    got_ref, gain_ref, gate_ref, up_ref, down_ref, late_ref, state_ref, out_ref, new_state_ref, flat, stored
+):
     f32 = jnp.float32
+    store = pltpu.make_async_copy(
+        late_ref, new_state_ref.at[pl.ds(SEQ_STEP, SEQ_STEP)], stored
+    )
+    store.start()
     senders, n_y, rows, quarter = got_ref.shape
     power = jnp.zeros((senders * rows, 128), f32)
     for y in range(n_y):
@@ -259,20 +267,28 @@
             hidden, down_ref[0, :, y * quarter : (y + 1) * quarter], preferred_element_type=f32
         )
         out_ref[:, y] = partial.astype(jnp.bfloat16).reshape(senders, rows, quarter)
-
-
-def experts(got, routed_gain, expert_gate, expert_up, expert_down):
+    store.wait()
+
+
+def experts(got, routed_gain, expert_gate, expert_up, expert_down, late, new_state):
     senders, n_y, rows, quarter = got.shape
     vmem = pl.BlockSpec(memory_space=pltpu.VMEM)
     return pl.pallas_call(
         expert_kernel,
-        in_specs=[vmem] * 5,
-        out_specs=vmem,
-        out_shape=jax.ShapeDtypeStruct(got.shape, jnp.bfloat16),
-        scratch_shapes=[pltpu.VMEM((senders * rows, n_y * quarter), jnp.bfloat16)],
+        in_specs=[vmem] * 6 + [pl.BlockSpec(memory_space=pl.ANY)],
+        out_specs=[vmem, pl.BlockSpec(memory_space=pl.ANY)],
+        out_shape=[
+            jax.ShapeDtypeStruct(got.shape, jnp.bfloat16),
+            jax.ShapeDtypeStruct(new_state.shape, new_state.dtype),
+        ],
+        input_output_aliases={6: 1},
+        scratch_shapes=[
+            pltpu.VMEM((senders * rows, n_y * quarter), jnp.bfloat16),
+            pltpu.SemaphoreType.DMA,
+        ],
         compiler_params=pltpu.CompilerParams(vmem_limit_bytes=12 << 20),
         cost_estimate=pl.CostEstimate(flops=400_000_000, bytes_accessed=4_000_000, transcendentals=40_000),
-    )(got, routed_gain.reshape(1, n_y * quarter), expert_gate, expert_up, expert_down)
+    )(got, routed_gain.reshape(1, n_y * quarter), expert_gate, expert_up, expert_down, late, new_state)
 
 
 def pack_kernel(
@@ -465,7 +481,7 @@
     quarter = width // n_y
     per_expert = n_zq * SLOTS
 
-    product, new_state = heads_update(
+    product, new_state, late = heads_update(
         n_y, state_in, receptance, key_in, value_in, learn_in, decay_in, decay_base, norm_gain, out_weight
     )
     arrived = exchange(product, "y")
@@ -473,7 +489,8 @@
     rows = exchange(parcels, "zq")
     chosen, place, weight = choose(rows, near, n_y, SLOTS, route_ids.shape[1], seqs)
     got = exchange(chosen.reshape(near * n_y, per_expert, quarter), NEAR_AXES)
-    back = experts(got.reshape(near, n_y, per_expert, quarter), routed_gain, expert_gate, expert_up, expert_down)
+    got = got.reshape(near, n_y, per_expert, quarter)
+    back, new_state = experts(got, routed_gain, expert_gate, expert_up, expert_down, late, new_state)
     returned = exchange(back.reshape(near * n_y, per_expert, quarter), NEAR_AXES)
     combined = combine(returned.reshape(near, n_y, per_expert, quarter), place, weight, n_zq)
     routed = exchange(combined, "zq").astype(jnp.float32).sum(axis=0)

time: 120 us -> 120 us (level)
  no operation moved by 1% of the time
where the time goes in v8:
time: 120 us; the launch traced here: 119 us
  blocking collectives  112 us (93%)
  Pallas kernels  5.47 us (5%)
    all_to_all x6, blocking collectives, exchange(): return lax.all_to_all(pieces, axes, split_axis=0, concat_axis=0, tiled=True)  112 us
    pallas_call x1, Pallas kernels, heads_update(): pl.pallas_call(functools.partial(heads_kernel, owners), in_specs=[any_spa...  3.56 us

profile of v8, /device:TPU:1, one launch (start us, length us, event | category | flops | bytes accessed | tf_op | source)
XLA Modules:
  0.0 119.3 jit_solution(11244147113534823058)
XLA Ops:
  0.6 0.0 copy-start.6
  0.6 0.0 copy-start.5
  0.7 0.0 copy-start.4
  0.7 0.0 copy-start.3
  0.7 3.6 %shard_map.167 = (f32[16,4,64,64]{3,2,1,0:T(8,128)}, bf16[4,16,512]{2,1,0:T(8,128)(2,1)S(1)}, f32[8,4,64,64]{3,2,1,0:T(8,128)S(1)}) custom-call(f32[16,4,64,64]{3,2,1,0:T(8,128)} %state_ref.1, bf16[16,256]{1,0:T(8,128)(2,1)} %reading_ref.1, bf16[16,256]{1,0:T(8,128)(2,1)} %key_ref.1, bf16[16,256]{1,0:T(8,128)(2,1)} %value_ref.1, bf16[16,256]{1,0:T(8,128)(2,1)} %learn_ref.1, ...), custom_call_target="tpu_custom_call" | custom-call | flops 20000000 | bytes 5000000 | tf_op jit(solution)/shard_map/pallas_call | solution.py:197
  4.2 0.0 copy-start
  4.3 0.0 copy-start.1
  4.3 0.0 copy-start.2
  4.3 9.4 %all_to_all.30.arrived_ref = bf16[4,16,512]{2,1,0:T(8,128)(2,1)S(1)} all-to-all(bf16[4,16,512]{2,1,0:T(8,128)(2,1)S(1)} %get-tuple-element.12), channel_id=1, replica_groups=mesh['zq'=8,'zp'=2,'x'=4,'c'=2,'y'=4] {'y'}, dimensions={0} | all-to-all | bytes 131072 | tf_op jit(solution)/shard_map/all_to_all | solution.py:20
  13.7 0.0 copy-done.6
  13.7 0.0 copy-done.5
  13.7 0.0 copy-done.4
  13.7 0.0 copy-done.3
  13.7 0.1 shard_map.168
  13.8 28.4 %all_to_all.31.rows_ref = bf16[8,72,128]{2,1,0:T(8,128)(2,1)S(1)} all-to-all(bf16[8,72,128]{2,1,0:T(8,128)(2,1)S(1)} %get-tuple-element.14), channel_id=1, replica_groups=mesh['zq'=8,'zp'=2,'x'=4,'c'=2,'y'=4] {'zq'}, dimensions={0} | all-to-all | bytes 294912 | tf_op jit(solution)/shard_map/all_to_all | solution.py:20
  42.2 0.4 shard_map.169
  42.6 26.8 %all_to_all.32 = bf16[64,16,512]{2,1,0:T(8,128)(2,1)S(1)} all-to-all(bf16[64,16,512]{2,1,0:T(8,128)(2,1)S(1)} %bitcast.15), channel_id=1, replica_groups=mesh['zq'=8,'zp'=2,'x'=4,'c'=2,'y'=4] {'zp','x','c','y'}, dimensions={0} | all-to-all | bytes 2097152 | tf_op jit(solution)/shard_map/all_to_all | solution.py:20
  69.3 0.0 copy-done
  69.3 0.0 copy-done.1
  69.3 0.0 copy-done.2
  69.4 1.0 shard_map.170
  70.4 22.3 %all_to_all.33 = bf16[64,16,512]{2,1,0:T(8,128)(2,1)S(1)} all-to-all(bf16[64,16,512]{2,1,0:T(8,128)(2,1)S(1)} %bitcast.14), channel_id=1, replica_groups=mesh['zq'=8,'zp'=2,'x'=4,'c'=2,'y'=4] {'zp','x','c','y'}, dimensions={0} | all-to-all | bytes 2097152 | tf_op jit(solution)/shard_map/all_to_all | solution.py:20
  92.7 0.4 shard_map.171
  93.1 15.5 %all_to_all.34 = bf16[8,16,512]{2,1,0:T(8,128)(2,1)S(1)} all-to-all(bf16[8,16,512]{2,1,0:T(8,128)(2,1)S(1)} %shard_map.171), channel_id=1, replica_groups=mesh['zq'=8,'zp'=2,'x'=4,'c'=2,'y'=4] {'zq'}, dimensions={0} | all-to-all | bytes 262144 | tf_op jit(solution)/shard_map/all_to_all | solution.py:20
  108.7 10.0 %all_to_all.35 = bf16[4,16,512]{2,1,0:T(8,128)(2,1)S(1)} all-to-all(bf16[4,16,512]{2,1,0:T(8,128)(2,1)S(1)} %broadcast_in_dim.3), channel_id=1, replica_groups=mesh['zq'=8,'zp'=2,'x'=4,'c'=2,'y'=4] {'y'}, dimensions={0} | all-to-all | bytes 131072 | tf_op jit(solution)/shard_map/all_to_all | solution.py:20
  118.7 0.6 copy.20
  (3 shorter events, 0.0 us)
Async XLA Ops:
  0.6 13.1 %copy-start.6 = (f32[16,6]{0,1:T(8,128)S(1)}, f32[16,6]{0,1:T(8,128)}, u32[]{:S(2)}) copy-start(f32[16,6]{0,1:T(8,128)} %param.31) | copy-start | bytes 1156
  0.6 13.0 %copy-start.5 = (s32[16,6]{0,1:T(8,128)S(1)}, s32[16,6]{0,1:T(8,128)}, u32[]{:S(2)}) copy-start(s32[16,6]{0,1:T(8,128)} %param.30) | copy-start | bytes 1156
  0.7 13.0 %copy-start.4 = (f32[2048]{0:T(1024)S(1)}, f32[2048]{0:T(1024)}, u32[]{:S(2)}) copy-start(f32[2048]{0:T(1024)} %param.26) | copy-start | bytes 24580
  0.7 13.0 %copy-start.3 = (bf16[16,2048]{1,0:T(8,128)(2,1)S(1)}, bf16[16,2048]{1,0:T(8,128)(2,1)}, u32[]{:S(2)}) copy-start(bf16[16,2048]{1,0:T(8,128)(2,1)} %hidden_ref.1) | copy-start | bytes 196612
  4.2 65.1 %copy-start = (bf16[1,2048,128]{2,1,0:T(8,128)(2,1)S(1)}, bf16[1,2048,128]{2,1,0:T(8,128)(2,1)}, u32[]{:S(2)}) copy-start(bf16[1,2048,128]{2,1,0:T(8,128)(2,1)} %gate_ref.1) | copy-start | bytes 1572868
  4.3 65.1 %copy-start.1 = (bf16[1,2048,128]{2,1,0:T(8,128)(2,1)S(1)}, bf16[1,2048,128]{2,1,0:T(8,128)(2,1)}, u32[]{:S(2)}) copy-start(bf16[1,2048,128]{2,1,0:T(8,128)(2,1)} %up_ref.1) | copy-start | bytes 1572868
  4.3 65.1 %copy-start.2 = (bf16[1,128,2048]{2,1,0:T(8,128)(2,1)S(1)}, bf16[1,128,2048]{2,1,0:T(8,128)(2,1)}, u32[]{:S(2)}) copy-start(bf16[1,128,2048]{2,1,0:T(8,128)(2,1)} %down_ref.1) | copy-start | bytes 1572868

commit v9 on v8

--- a/solution.py
+++ b/solution.py
@@ -23,6 +23,27 @@
 def two_parts(values):
     high = values.astype(jnp.bfloat16)
     return high, (values - high.astype(jnp.float32)).astype(jnp.bfloat16)
+
+
+def routing_rows(ids, shares):
+    f32, bf16 = jnp.float32, jnp.bfloat16
+    top, seqs = ids.shape
+    lane = lax.broadcasted_iota(jnp.int32, (8, 128), 1)
+    ids = jnp.pad(ids, ((0, 8 - top), (0, 128 - seqs)))
+    again = jnp.zeros((8, 128), jnp.int32)
+    for k in range(top):
+        line = jnp.broadcast_to(ids[k : k + 1], (8, 128))
+        for back in range(1, seqs):
+            same = (pltpu.roll(line, back, 1) == ids) & (lane >= back)
+            again = jnp.where(same, 128, again)
+    parts = [(ids + again)[:, :seqs].astype(f32)]
+    shares = jnp.pad(shares, ((0, 8 - top), (0, 0)))
+    for _ in range(3):
+        part = shares.astype(bf16).astype(f32)
+        parts.append(part)
+        shares = shares - part
+    parts.append(jnp.zeros((8, 128 - len(parts) * seqs), f32))
+    return jnp.concatenate(parts, axis=1).astype(bf16)
 
 
 def heads_kernel(
@@ -36,14 +57,19 @@
     base_ref,
     gain_ref,
     weight_ref,
+    ids_ref,
+    shares_ref,
     new_state_ref,
     out_ref,
     late_ref,
+    routing_ref,
     state_here,
     early,
     inputs,
     decay_here,
     vectors,
+    ids_here,
+    shares_here,
     weight_here,
     rows,
     read,
@@ -77,6 +103,8 @@
                 (reading_ref, inputs.at[2]),
                 (value_ref, inputs.at[3]),
                 (gain_ref, vectors.at[1]),
+                (ids_ref, ids_here),
+                (shares_ref, shares_here),
             )
         )
     ]
@@ -112,6 +140,8 @@
         rows[3, pair] = key
         rows[4, pair] = inputs[2, :, at].astype(f32)
         rows[5, pair] = inputs[3, :, at].astype(f32)
+
+    routing_ref[...] = routing_rows(ids_here[...], shares_here[...])
 
     blocks = [
         (local, pair, slice((local * pairs + pair) * size, (local * pairs + pair + 1) * size))
@@ -186,7 +216,7 @@
     store.wait()
 
 
-def heads_update(owners, state_in, receptance, key_in, value_in, learn_in, decay_in, decay_base, norm_gain, out_weight):
+def heads_update(owners, state_in, receptance, key_in, value_in, learn_in, decay_in, decay_base, norm_gain, out_weight, route_ids, route_weights):
     seqs, heads, size, _ = state_in.shape
     width = out_weight.shape[1]
     channels = heads * size
@@ -194,14 +224,16 @@
     step_rows = SEQ_STEP * heads // 2 * size
     any_space = pl.BlockSpec(memory_space=pl.ANY)
     half_shape = (SEQ_STEP, heads, size, size)
-    new_state, product, late = pl.pallas_call(
+    top = route_ids.shape[1]
+    new_state, product, late, routing = pl.pallas_call(
         functools.partial(heads_kernel, owners),
-        in_specs=[any_space] * 9,
-        out_specs=[any_space] + [pl.BlockSpec(memory_space=pltpu.VMEM)] * 2,
+        in_specs=[any_space] * 11,
+        out_specs=[any_space] + [pl.BlockSpec(memory_space=pltpu.VMEM)] * 3,
         out_shape=[
             jax.ShapeDtypeStruct(state_in.shape, jnp.float32),
             pltpu.VMEM((owners, seqs, width // owners), jnp.bfloat16),
             pltpu.VMEM(half_shape, jnp.float32),
+            pltpu.VMEM((8, 128), jnp.bfloat16),
         ],
         scratch_shapes=[
             pltpu.VMEM(state_in.shape, jnp.float32),
@@ -209,13 +241,15 @@
             pltpu.VMEM((4, seqs, channels), jnp.bfloat16),
             pltpu.VMEM((seqs, channels), jnp.float32),
             pltpu.VMEM((2, 1, channels), jnp.float32),
+            pltpu.VMEM((top, seqs), jnp.int32),
+            pltpu.VMEM((top, seqs), jnp.float32),
             pltpu.VMEM((channels, width), jnp.bfloat16),
             pltpu.VMEM((6, heads // 2, seqs, 2 * size), jnp.float32),
             pltpu.VMEM((2, seqs, channels // 2), jnp.float32),
             pltpu.VMEM((steps, step_rows, 2 * size), jnp.float32),
             pltpu.VMEM((steps, 3, step_rows, 2 * size), jnp.bfloat16),
             pltpu.VMEM((steps, 2, step_rows, 2 * size), jnp.float32),
-            pltpu.SemaphoreType.DMA((steps + 8,)),
+            pltpu.SemaphoreType.DMA((steps + 10,)),
             pltpu.SemaphoreType.DMA,
         ],
         compiler_params=pltpu.CompilerParams(vmem_limit_bytes=60 << 20),
@@ -230,8 +264,10 @@
         decay_base.reshape(1, channels),
         norm_gain.reshape(1, channels),
         out_weight,
-    )
-    return product, new_state, late
+        route_ids.T,
+        route_weights.T,
+    )
+    return product, new_state, late, routing
 
 
 def expert_kernel(
@@ -292,52 +328,39 @@
 
 
 def pack_kernel(
-    arrived_ref, hidden_ref, gain_ref, ids_ref, weights_ref, parcels_ref, own_ref
+    arrived_ref, hidden_ref, gain_ref, routing_ref, parcels_ref, own_ref
 ):
     f32, bf16 = jnp.float32, jnp.bfloat16
     seqs, quarter = own_ref.shape
-    top = ids_ref.shape[0]
     at = pl.ds(pl.multiple_of(lax.axis_index("y") * quarter, quarter), quarter)
     attention = jnp.sum(arrived_ref[...].astype(f32), axis=0).astype(bf16)
     residual = hidden_ref[:, at].astype(f32) + attention.astype(f32)
     own_ref[...] = residual
     gained = (residual * gain_ref[:, at]).astype(bf16)
 
-    weights = weights_ref[...]
-    routing = jnp.zeros((8, 128), f32)
-    parts = [ids_ref[...].astype(f32)]
-    for _ in range(3):
-        part = weights.astype(bf16).astype(f32)
-        parts.append(part)
-        weights = weights - part
-    routing = jnp.concatenate(
-        [jnp.pad(part, ((0, 8 - top), (0, 0))) for part in parts]
-        + [jnp.zeros((8, 128 - len(parts) * seqs), f32)],
-        axis=1,
-    ).astype(bf16)
     chunks = quarter // 128
     for z in range(parcels_ref.shape[0]):
         for chunk in range(chunks):
             parcels_ref[z, chunk * seqs : (chunk + 1) * seqs, :] = gained[
                 :, chunk * 128 : (chunk + 1) * 128
             ]
-        parcels_ref[z, chunks * seqs : chunks * seqs + 8, :] = routing
-
-
-def pack(arrived, hidden_in, routed_gain, route_ids, route_weights, n_z):
+        parcels_ref[z, chunks * seqs : chunks * seqs + 8, :] = routing_ref[...]
+
+
+def pack(arrived, hidden_in, routed_gain, routing, n_z):
     n_y, seqs, quarter = arrived.shape
     width = n_y * quarter
     vmem = pl.BlockSpec(memory_space=pltpu.VMEM)
     return pl.pallas_call(
         pack_kernel,
-        in_specs=[vmem] * 5,
+        in_specs=[vmem] * 4,
         out_specs=[vmem] * 2,
         out_shape=[
             jax.ShapeDtypeStruct((n_z, quarter // 128 * seqs + 8, 128), jnp.bfloat16),
             jax.ShapeDtypeStruct((seqs, quarter), jnp.float32),
         ],
         compiler_params=pltpu.CompilerParams(vmem_limit_bytes=8 << 20),
-    )(arrived, hidden_in, routed_gain.reshape(1, width), route_ids.T, route_weights.T)
+    )(arrived, hidden_in, routed_gain.reshape(1, width), routing)
 
 
 def choose_kernel(top, slots, rows_ref, chosen_ref, place_ref, weight_ref, flat, choice):
@@ -367,18 +390,14 @@
     named = (
         lax.axis_index("zq") * near + lax.broadcasted_iota(jnp.int32, (near, tokens), 0)
     ).astype(f32)
-    member = jnp.zeros((near, tokens), f32)
+    sender = (lax.broadcasted_iota(jnp.int32, (near, tokens), 1) // seqs * slots).astype(f32)
+    place = jnp.full((near, tokens), -1.0, f32)
     weight = jnp.zeros((near, tokens), f32)
     for k in range(top):
-        hit = named == ids[k : k + 1, :]
-        member = jnp.where(hit, 1.0, member)
-        weight = jnp.where(hit, weights[k : k + 1, :], weight)
-    token = lax.broadcasted_iota(jnp.int32, (tokens, tokens), 0)
-    other = lax.broadcasted_iota(jnp.int32, (tokens, tokens), 1)
-    earlier = (token // seqs == other // seqs) & (token < other)
-    rank = jnp.dot(member.astype(bf16), jnp.where(earlier, 1.0, 0.0).astype(bf16), preferred_element_type=f32)
-    sender = (lax.broadcasted_iota(jnp.int32, (near, tokens), 1) // seqs * slots).astype(f32)
-    place = jnp.where(member > 0, sender + rank, -1.0)
+        for slot in range(slots):
+            hit = named + 128.0 * slot == ids[k : k + 1, :]
+            place = jnp.where(hit, sender + slot, place)
+            weight = jnp.where(hit, weights[k : k + 1, :], weight)
     place_ref[...] = place
     weight_ref[...] = weight
     row = lax.broadcasted_iota(jnp.int32, (per_expert, tokens), 0).astype(f32)
@@ -481,11 +500,12 @@
     quarter = width // n_y
     per_expert = n_zq * SLOTS
 
-    product, new_state, late = heads_update(
-        n_y, state_in, receptance, key_in, value_in, learn_in, decay_in, decay_base, norm_gain, out_weight
+    product, new_state, late, routing = heads_update(
+        n_y, state_in, receptance, key_in, value_in, learn_in, decay_in, decay_base, norm_gain, out_weight,
+        route_ids, route_weights,
     )
     arrived = exchange(product, "y")
-    parcels, own_residual = pack(arrived, hidden_in, routed_gain, route_ids, route_weights, n_zq)
+    parcels, own_residual = pack(arrived, hidden_in, routed_gain, routing, n_zq)
     rows = exchange(parcels, "zq")
     chosen, place, weight = choose(rows, near, n_y, SLOTS, route_ids.shape[1], seqs)
     got = exchange(chosen.reshape(near * n_y, per_expert, quarter), NEAR_AXES)

time: 120 us -> 119 us (level)
  no operation moved by 1% of the time
where the time goes in v9:
time: 119 us
  blocking collectives  112 us (94%)
  Pallas kernels  5.31 us (4%)
    all_to_all x6, blocking collectives, exchange(): return lax.all_to_all(pieces, axes, split_axis=0, concat_axis=0, tiled=True)  112 us
    pallas_call x1, Pallas kernels, heads_update(): pl.pallas_call(functools.partial(heads_kernel, owners), in_specs=[any_spa...  3.58 us

profile of v9, /device:TPU:1, one launch (start us, length us, event | category | flops | bytes accessed | tf_op | source)
XLA Modules:
  0.0 119.2 jit_solution(14327179047973123202)
XLA Ops:
  0.6 0.0 copy-start.4
  0.6 0.0 copy-start.3
  0.7 3.6 %shard_map.167 = (f32[16,4,64,64]{3,2,1,0:T(8,128)}, bf16[4,16,512]{2,1,0:T(8,128)(2,1)S(1)}, f32[8,4,64,64]{3,2,1,0:T(8,128)S(1)}, bf16[8,128]{1,0:T(8,128)(2,1)S(1)}) custom-call(f32[16,4,64,64]{3,2,1,0:T(8,128)} %state_ref.1, bf16[16,256]{1,0:T(8,128)(2,1)} %reading_ref.1, bf16[16,256]{1,0:T(8,128)(2,1)} %key_ref.1, bf16[16,256]{1,0:T(8,128)(2,1)} %value_ref.1, ...), custom_call_target="tpu_custom_call" | custom-call | flops 20000000 | bytes 5000000 | tf_op jit(solution)/shard_map/pallas_call | solution.py:228
  4.2 0.0 copy-start
  4.3 0.0 copy-start.1
  4.3 0.0 copy-start.2
  4.3 9.4 %all_to_all.30.arrived_ref = bf16[4,16,512]{2,1,0:T(8,128)(2,1)S(1)} all-to-all(bf16[4,16,512]{2,1,0:T(8,128)(2,1)S(1)} %get-tuple-element.13), channel_id=1, replica_groups=mesh['zq'=8,'zp'=2,'x'=4,'c'=2,'y'=4] {'y'}, dimensions={0} | all-to-all | bytes 131072 | tf_op jit(solution)/shard_map/all_to_all | solution.py:20
  13.7 0.0 copy-done.4
  13.7 0.0 copy-done.3
  13.7 28.4 %all_to_all.31.rows_ref = bf16[8,72,128]{2,1,0:T(8,128)(2,1)S(1)} all-to-all(bf16[8,72,128]{2,1,0:T(8,128)(2,1)S(1)} %get-tuple-element.16), channel_id=1, replica_groups=mesh['zq'=8,'zp'=2,'x'=4,'c'=2,'y'=4] {'zq'}, dimensions={0} | all-to-all | bytes 294912 | tf_op jit(solution)/shard_map/all_to_all | solution.py:20
  42.1 0.3 shard_map.169
  42.4 26.8 %all_to_all.32 = bf16[64,16,512]{2,1,0:T(8,128)(2,1)S(1)} all-to-all(bf16[64,16,512]{2,1,0:T(8,128)(2,1)S(1)} %bitcast.15), channel_id=1, replica_groups=mesh['zq'=8,'zp'=2,'x'=4,'c'=2,'y'=4] {'zp','x','c','y'}, dimensions={0} | all-to-all | bytes 2097152 | tf_op jit(solution)/shard_map/all_to_all | solution.py:20
  69.2 0.0 copy-done
  69.2 0.0 copy-done.1
  69.2 0.0 copy-done.2
  69.2 1.0 shard_map.170
  70.2 22.4 %all_to_all.33 = bf16[64,16,512]{2,1,0:T(8,128)(2,1)S(1)} all-to-all(bf16[64,16,512]{2,1,0:T(8,128)(2,1)S(1)} %bitcast.14), channel_id=1, replica_groups=mesh['zq'=8,'zp'=2,'x'=4,'c'=2,'y'=4] {'zp','x','c','y'}, dimensions={0} | all-to-all | bytes 2097152 | tf_op jit(solution)/shard_map/all_to_all | solution.py:20
  92.6 0.4 shard_map.171
  93.0 15.5 %all_to_all.34 = bf16[8,16,512]{2,1,0:T(8,128)(2,1)S(1)} all-to-all(bf16[8,16,512]{2,1,0:T(8,128)(2,1)S(1)} %shard_map.171), channel_id=1, replica_groups=mesh['zq'=8,'zp'=2,'x'=4,'c'=2,'y'=4] {'zq'}, dimensions={0} | all-to-all | bytes 262144 | tf_op jit(solution)/shard_map/all_to_all | solution.py:20
  108.5 10.0 %all_to_all.35 = bf16[4,16,512]{2,1,0:T(8,128)(2,1)S(1)} all-to-all(bf16[4,16,512]{2,1,0:T(8,128)(2,1)S(1)} %broadcast_in_dim.3), channel_id=1, replica_groups=mesh['zq'=8,'zp'=2,'x'=4,'c'=2,'y'=4] {'y'}, dimensions={0} | all-to-all | bytes 131072 | tf_op jit(solution)/shard_map/all_to_all | solution.py:20
  118.5 0.6 copy.20
  (4 shorter events, 0.1 us)
Async XLA Ops:
  0.6 13.1 %copy-start.4 = (f32[2048]{0:T(1024)S(1)}, f32[2048]{0:T(1024)}, u32[]{:S(2)}) copy-start(f32[2048]{0:T(1024)} %param.26) | copy-start | bytes 24580
  0.6 13.0 %copy-start.3 = (bf16[16,2048]{1,0:T(8,128)(2,1)S(1)}, bf16[16,2048]{1,0:T(8,128)(2,1)}, u32[]{:S(2)}) copy-start(bf16[16,2048]{1,0:T(8,128)(2,1)} %hidden_ref.1) | copy-start | bytes 196612
  4.2 64.9 %copy-start = (bf16[1,2048,128]{2,1,0:T(8,128)(2,1)S(1)}, bf16[1,2048,128]{2,1,0:T(8,128)(2,1)}, u32[]{:S(2)}) copy-start(bf16[1,2048,128]{2,1,0:T(8,128)(2,1)} %gate_ref.1) | copy-start | bytes 1572868
  4.3 64.9 %copy-start.1 = (bf16[1,2048,128]{2,1,0:T(8,128)(2,1)S(1)}, bf16[1,2048,128]{2,1,0:T(8,128)(2,1)}, u32[]{:S(2)}) copy-start(bf16[1,2048,128]{2,1,0:T(8,128)(2,1)} %up_ref.1) | copy-start | bytes 1572868
  4.3 64.9 %copy-start.2 = (bf16[1,128,2048]{2,1,0:T(8,128)(2,1)S(1)}, bf16[1,128,2048]{2,1,0:T(8,128)(2,1)}, u32[]{:S(2)}) copy-start(bf16[1,128,2048]{2,1,0:T(8,128)(2,1)} %down_ref.1) | copy-start | bytes 1572868

commit v10 on v9

--- a/solution.py
+++ b/solution.py
@@ -202,8 +202,13 @@
     mixed = []
     for pair in range(pairs):
         at = slice(pair * size, (pair + 1) * size)
-        live = jnp.concatenate([read[0, :, at], read[1, :, at]], axis=1)
-        live = live - head_sums(live) * (1.0 / size)
+        live = jnp.concatenate(
+            [
+                read[which, :, at] - jnp.mean(read[which, :, at], axis=1, keepdims=True)
+                for which in range(2)
+            ],
+            axis=1,
+        )
         spread = head_sums(jnp.square(live)) * (1.0 / size)
         gain = vectors[1, :, pair * pair_width : (pair + 1) * pair_width]
         mixed.append(live * lax.rsqrt(spread + GROUP_EPSILON) * gain)

time: 119 us -> 119 us (level)
  no operation moved by 1% of the time
where the time goes in v10:
time: 119 us
  blocking collectives  112 us (94%)
  Pallas kernels  5.3 us (4%)
    all_to_all x6, blocking collectives, exchange(): return lax.all_to_all(pieces, axes, split_axis=0, concat_axis=0, tiled=True)  112 us
    pallas_call x1, Pallas kernels, heads_update(): pl.pallas_call(functools.partial(heads_kernel, owners), in_specs=[any_spa...  3.55 us

profile of v10, /device:TPU:1, one launch (start us, length us, event | category | flops | bytes accessed | tf_op | source)
XLA Modules:
  0.0 119.1 jit_solution(2208481889422354141)
XLA Ops:
  0.6 0.0 copy-start.4
  0.6 0.0 copy-start.3
  0.7 3.6 %shard_map.167 = (f32[16,4,64,64]{3,2,1,0:T(8,128)}, bf16[4,16,512]{2,1,0:T(8,128)(2,1)S(1)}, f32[8,4,64,64]{3,2,1,0:T(8,128)S(1)}, bf16[8,128]{1,0:T(8,128)(2,1)S(1)}) custom-call(f32[16,4,64,64]{3,2,1,0:T(8,128)} %state_ref.1, bf16[16,256]{1,0:T(8,128)(2,1)} %reading_ref.1, bf16[16,256]{1,0:T(8,128)(2,1)} %key_ref.1, bf16[16,256]{1,0:T(8,128)(2,1)} %value_ref.1, ...), custom_call_target="tpu_custom_call" | custom-call | flops 20000000 | bytes 5000000 | tf_op jit(solution)/shard_map/pallas_call | solution.py:233
  4.2 0.0 copy-start
  4.2 0.0 copy-start.1
  4.2 0.0 copy-start.2
  4.3 9.4 %all_to_all.30.arrived_ref = bf16[4,16,512]{2,1,0:T(8,128)(2,1)S(1)} all-to-all(bf16[4,16,512]{2,1,0:T(8,128)(2,1)S(1)} %get-tuple-element.13), channel_id=1, replica_groups=mesh['zq'=8,'zp'=2,'x'=4,'c'=2,'y'=4] {'y'}, dimensions={0} | all-to-all | bytes 131072 | tf_op jit(solution)/shard_map/all_to_all | solution.py:20
  13.7 0.0 copy-done.4
  13.7 0.0 copy-done.3
  13.7 28.4 %all_to_all.31.rows_ref = bf16[8,72,128]{2,1,0:T(8,128)(2,1)S(1)} all-to-all(bf16[8,72,128]{2,1,0:T(8,128)(2,1)S(1)} %get-tuple-element.16), channel_id=1, replica_groups=mesh['zq'=8,'zp'=2,'x'=4,'c'=2,'y'=4] {'zq'}, dimensions={0} | all-to-all | bytes 294912 | tf_op jit(solution)/shard_map/all_to_all | solution.py:20
  42.1 0.3 shard_map.169
  42.4 26.8 %all_to_all.32 = bf16[64,16,512]{2,1,0:T(8,128)(2,1)S(1)} all-to-all(bf16[64,16,512]{2,1,0:T(8,128)(2,1)S(1)} %bitcast.15), channel_id=1, replica_groups=mesh['zq'=8,'zp'=2,'x'=4,'c'=2,'y'=4] {'zp','x','c','y'}, dimensions={0} | all-to-all | bytes 2097152 | tf_op jit(solution)/shard_map/all_to_all | solution.py:20
  69.2 0.0 copy-done
  69.2 0.0 copy-done.1
  69.2 0.0 copy-done.2
  69.2 1.0 shard_map.170
  70.2 22.3 %all_to_all.33 = bf16[64,16,512]{2,1,0:T(8,128)(2,1)S(1)} all-to-all(bf16[64,16,512]{2,1,0:T(8,128)(2,1)S(1)} %bitcast.14), channel_id=1, replica_groups=mesh['zq'=8,'zp'=2,'x'=4,'c'=2,'y'=4] {'zp','x','c','y'}, dimensions={0} | all-to-all | bytes 2097152 | tf_op jit(solution)/shard_map/all_to_all | solution.py:20
  92.5 0.4 shard_map.171
  92.9 15.5 %all_to_all.34 = bf16[8,16,512]{2,1,0:T(8,128)(2,1)S(1)} all-to-all(bf16[8,16,512]{2,1,0:T(8,128)(2,1)S(1)} %shard_map.171), channel_id=1, replica_groups=mesh['zq'=8,'zp'=2,'x'=4,'c'=2,'y'=4] {'zq'}, dimensions={0} | all-to-all | bytes 262144 | tf_op jit(solution)/shard_map/all_to_all | solution.py:20
  108.5 10.0 %all_to_all.35 = bf16[4,16,512]{2,1,0:T(8,128)(2,1)S(1)} all-to-all(bf16[4,16,512]{2,1,0:T(8,128)(2,1)S(1)} %broadcast_in_dim.3), channel_id=1, replica_groups=mesh['zq'=8,'zp'=2,'x'=4,'c'=2,'y'=4] {'y'}, dimensions={0} | all-to-all | bytes 131072 | tf_op jit(solution)/shard_map/all_to_all | solution.py:20
  118.5 0.6 copy.20
  (4 shorter events, 0.1 us)
Async XLA Ops:
  0.6 13.0 %copy-start.4 = (f32[2048]{0:T(1024)S(1)}, f32[2048]{0:T(1024)}, u32[]{:S(2)}) copy-start(f32[2048]{0:T(1024)} %param.26) | copy-start | bytes 24580
  0.6 13.0 %copy-start.3 = (bf16[16,2048]{1,0:T(8,128)(2,1)S(1)}, bf16[16,2048]{1,0:T(8,128)(2,1)}, u32[]{:S(2)}) copy-start(bf16[16,2048]{1,0:T(8,128)(2,1)} %hidden_ref.1) | copy-start | bytes 196612
  4.2 64.9 %copy-start = (bf16[1,2048,128]{2,1,0:T(8,128)(2,1)S(1)}, bf16[1,2048,128]{2,1,0:T(8,128)(2,1)}, u32[]{:S(2)}) copy-start(bf16[1,2048,128]{2,1,0:T(8,128)(2,1)} %gate_ref.1) | copy-start | bytes 1572868
  4.2 64.9 %copy-start.1 = (bf16[1,2048,128]{2,1,0:T(8,128)(2,1)S(1)}, bf16[1,2048,128]{2,1,0:T(8,128)(2,1)}, u32[]{:S(2)}) copy-start(bf16[1,2048,128]{2,1,0:T(8,128)(2,1)} %up_ref.1) | copy-start | bytes 1572868
  4.2 64.9 %copy-start.2 = (bf16[1,128,2048]{2,1,0:T(8,128)(2,1)S(1)}, bf16[1,128,2048]{2,1,0:T(8,128)(2,1)}, u32[]{:S(2)}) copy-start(bf16[1,128,2048]{2,1,0:T(8,128)(2,1)} %down_ref.1) | copy-start | bytes 1572868

commit v11 on v10

--- a/solution.py
+++ b/solution.py
@@ -11,6 +11,7 @@
 EPSILON = 1e-06
 GROUP_EPSILON = 0.00064
 SEQ_STEP = 8
+SEQ_COPY = 4
 SLOTS = 2
 NEAR_AXES = ("zp", "x", "c", "y")
 EP = ("zq", "zp", "x", "c")
@@ -86,14 +87,16 @@
     pair_width = 2 * size
     steps = 2
 
-    def state_load(step):
-        at = pl.ds(step * SEQ_STEP, SEQ_STEP)
-        return pltpu.make_async_copy(state_ref.at[at], state_here.at[at], arrived.at[step])
+    chunks = seqs // SEQ_COPY
+
+    def state_load(chunk):
+        at = pl.ds(chunk * SEQ_COPY, SEQ_COPY)
+        return pltpu.make_async_copy(state_ref.at[at], state_here.at[at], arrived.at[chunk])
 
     store = pltpu.make_async_copy(early, new_state_ref.at[pl.ds(0, SEQ_STEP)], stored)
 
     small = [
-        pltpu.make_async_copy(source, target, arrived.at[steps + number])
+        pltpu.make_async_copy(source, target, arrived.at[chunks + number])
         for number, (source, target) in enumerate(
             (
                 (key_ref, inputs.at[0]),
@@ -108,11 +111,11 @@
             )
         )
     ]
-    weight_load = pltpu.make_async_copy(weight_ref, weight_here, arrived.at[steps + len(small)])
+    weight_load = pltpu.make_async_copy(weight_ref, weight_here, arrived.at[chunks + len(small)])
     for load in small:
         load.start()
-    for step in range(steps):
-        state_load(step).start()
+    for chunk in range(chunks):
+        state_load(chunk).start()
     weight_load.start()
 
     square = (pair_width, pair_width)
@@ -162,8 +165,9 @@
         def row(which, local, pair):
             return rows[which, pair, first + local : first + local + 1, :]
 
-        state_load(step).wait()
         for local, pair, at in blocks:
+            if pair == 0 and local % SEQ_COPY == 0:
+                state_load((first + local) // SEQ_COPY).wait()
             parts[step, 2, at, :] = jnp.where(on_diagonal, row(5, local, pair), 0.0).astype(bf16)
             state = jnp.concatenate(
                 [state_here[first + local, 2 * pair], state_here[first + local, 2 * pair + 1]], axis=1
@@ -254,7 +258,7 @@
             pltpu.VMEM((steps, step_rows, 2 * size), jnp.float32),
             pltpu.VMEM((steps, 3, step_rows, 2 * size), jnp.bfloat16),
             pltpu.VMEM((steps, 2, step_rows, 2 * size), jnp.float32),
-            pltpu.SemaphoreType.DMA((steps + 10,)),
+            pltpu.SemaphoreType.DMA((seqs // SEQ_COPY + 10,)),
             pltpu.SemaphoreType.DMA,
         ],
         compiler_params=pltpu.CompilerParams(vmem_limit_bytes=60 << 20),

time: 119 us -> 119 us (level)
  no operation moved by 1% of the time
where the time goes in v11:
time: 119 us
  blocking collectives  112 us (94%)
  Pallas kernels  5.24 us (4%)
    all_to_all x6, blocking collectives, exchange(): return lax.all_to_all(pieces, axes, split_axis=0, concat_axis=0, tiled=True)  112 us
    pallas_call x1, Pallas kernels, heads_update(): pl.pallas_call(functools.partial(heads_kernel, owners), in_specs=[any_spa...  3.5 us

profile of v11, /device:TPU:1, one launch (start us, length us, event | category | flops | bytes accessed | tf_op | source)
XLA Modules:
  0.0 119.1 jit_solution(14338617403689590365)
XLA Ops:
  0.6 0.0 copy-start.4
  0.6 0.0 copy-start.3
  0.7 3.5 %shard_map.167 = (f32[16,4,64,64]{3,2,1,0:T(8,128)}, bf16[4,16,512]{2,1,0:T(8,128)(2,1)S(1)}, f32[8,4,64,64]{3,2,1,0:T(8,128)S(1)}, bf16[8,128]{1,0:T(8,128)(2,1)S(1)}) custom-call(f32[16,4,64,64]{3,2,1,0:T(8,128)} %state_ref.1, bf16[16,256]{1,0:T(8,128)(2,1)} %reading_ref.1, bf16[16,256]{1,0:T(8,128)(2,1)} %key_ref.1, bf16[16,256]{1,0:T(8,128)(2,1)} %value_ref.1, ...), custom_call_target="tpu_custom_call" | custom-call | flops 20000000 | bytes 5000000 | tf_op jit(solution)/shard_map/pallas_call | solution.py:237
  4.2 0.0 copy-start
  4.2 0.0 copy-start.1
  4.2 0.0 copy-start.2
  4.2 9.4 %all_to_all.30.arrived_ref = bf16[4,16,512]{2,1,0:T(8,128)(2,1)S(1)} all-to-all(bf16[4,16,512]{2,1,0:T(8,128)(2,1)S(1)} %get-tuple-element.13), channel_id=1, replica_groups=mesh['zq'=8,'zp'=2,'x'=4,'c'=2,'y'=4] {'y'}, dimensions={0} | all-to-all | bytes 131072 | tf_op jit(solution)/shard_map/all_to_all | solution.py:21
  13.6 0.0 copy-done.4
  13.6 0.0 copy-done.3
  13.6 28.4 %all_to_all.31.rows_ref = bf16[8,72,128]{2,1,0:T(8,128)(2,1)S(1)} all-to-all(bf16[8,72,128]{2,1,0:T(8,128)(2,1)S(1)} %get-tuple-element.16), channel_id=1, replica_groups=mesh['zq'=8,'zp'=2,'x'=4,'c'=2,'y'=4] {'zq'}, dimensions={0} | all-to-all | bytes 294912 | tf_op jit(solution)/shard_map/all_to_all | solution.py:21
  42.0 0.3 shard_map.169
  42.3 26.8 %all_to_all.32 = bf16[64,16,512]{2,1,0:T(8,128)(2,1)S(1)} all-to-all(bf16[64,16,512]{2,1,0:T(8,128)(2,1)S(1)} %bitcast.15), channel_id=1, replica_groups=mesh['zq'=8,'zp'=2,'x'=4,'c'=2,'y'=4] {'zp','x','c','y'}, dimensions={0} | all-to-all | bytes 2097152 | tf_op jit(solution)/shard_map/all_to_all | solution.py:21
  69.1 0.0 copy-done
  69.1 0.0 copy-done.1
  69.1 0.0 copy-done.2
  69.1 1.0 shard_map.170
  70.1 22.4 %all_to_all.33 = bf16[64,16,512]{2,1,0:T(8,128)(2,1)S(1)} all-to-all(bf16[64,16,512]{2,1,0:T(8,128)(2,1)S(1)} %bitcast.14), channel_id=1, replica_groups=mesh['zq'=8,'zp'=2,'x'=4,'c'=2,'y'=4] {'zp','x','c','y'}, dimensions={0} | all-to-all | bytes 2097152 | tf_op jit(solution)/shard_map/all_to_all | solution.py:21
  92.5 0.4 shard_map.171
  92.9 15.5 %all_to_all.34 = bf16[8,16,512]{2,1,0:T(8,128)(2,1)S(1)} all-to-all(bf16[8,16,512]{2,1,0:T(8,128)(2,1)S(1)} %shard_map.171), channel_id=1, replica_groups=mesh['zq'=8,'zp'=2,'x'=4,'c'=2,'y'=4] {'zq'}, dimensions={0} | all-to-all | bytes 262144 | tf_op jit(solution)/shard_map/all_to_all | solution.py:21
  108.4 10.0 %all_to_all.35 = bf16[4,16,512]{2,1,0:T(8,128)(2,1)S(1)} all-to-all(bf16[4,16,512]{2,1,0:T(8,128)(2,1)S(1)} %broadcast_in_dim.3), channel_id=1, replica_groups=mesh['zq'=8,'zp'=2,'x'=4,'c'=2,'y'=4] {'y'}, dimensions={0} | all-to-all | bytes 131072 | tf_op jit(solution)/shard_map/all_to_all | solution.py:21
  118.4 0.6 copy.20
  (4 shorter events, 0.1 us)
Async XLA Ops:
  0.6 13.0 %copy-start.4 = (f32[2048]{0:T(1024)S(1)}, f32[2048]{0:T(1024)}, u32[]{:S(2)}) copy-start(f32[2048]{0:T(1024)} %param.26) | copy-start | bytes 24580
  0.6 13.0 %copy-start.3 = (bf16[16,2048]{1,0:T(8,128)(2,1)S(1)}, bf16[16,2048]{1,0:T(8,128)(2,1)}, u32[]{:S(2)}) copy-start(bf16[16,2048]{1,0:T(8,128)(2,1)} %hidden_ref.1) | copy-start | bytes 196612
  4.2 64.9 %copy-start = (bf16[1,2048,128]{2,1,0:T(8,128)(2,1)S(1)}, bf16[1,2048,128]{2,1,0:T(8,128)(2,1)}, u32[]{:S(2)}) copy-start(bf16[1,2048,128]{2,1,0:T(8,128)(2,1)} %gate_ref.1) | copy-start | bytes 1572868
  4.2 64.9 %copy-start.1 = (bf16[1,2048,128]{2,1,0:T(8,128)(2,1)S(1)}, bf16[1,2048,128]{2,1,0:T(8,128)(2,1)}, u32[]{:S(2)}) copy-start(bf16[1,2048,128]{2,1,0:T(8,128)(2,1)} %up_ref.1) | copy-start | bytes 1572868
  4.2 64.9 %copy-start.2 = (bf16[1,128,2048]{2,1,0:T(8,128)(2,1)S(1)}, bf16[1,128,2048]{2,1,0:T(8,128)(2,1)}, u32[]{:S(2)}) copy-start(bf16[1,128,2048]{2,1,0:T(8,128)(2,1)} %down_ref.1) | copy-start | bytes 1572868

commit v12 on v11

--- a/solution.py
+++ b/solution.py
@@ -112,9 +112,10 @@
         )
     ]
     weight_load = pltpu.make_async_copy(weight_ref, weight_here, arrived.at[chunks + len(small)])
+    state_load(0).start()
     for load in small:
         load.start()
-    for chunk in range(chunks):
+    for chunk in range(1, chunks):
         state_load(chunk).start()
     weight_load.start()
 

time: 119 us -> 119 us (level)
  no operation moved by 1% of the time
where the time goes in v12:
time: 119 us
  blocking collectives  112 us (94%)
  Pallas kernels  5.23 us (4%)
    all_to_all x6, blocking collectives, exchange(): return lax.all_to_all(pieces, axes, split_axis=0, concat_axis=0, tiled=True)  112 us
    pallas_call x1, Pallas kernels, heads_update(): pl.pallas_call(functools.partial(heads_kernel, owners), in_specs=[any_spa...  3.48 us

profile of v12, /device:TPU:1, one launch (start us, length us, event | category | flops | bytes accessed | tf_op | source)
XLA Modules:
  0.0 119.1 jit_solution(18147072406260256902)
XLA Ops:
  0.6 0.0 copy-start.4
  0.6 0.0 copy-start.3
  0.7 3.5 %shard_map.167 = (f32[16,4,64,64]{3,2,1,0:T(8,128)}, bf16[4,16,512]{2,1,0:T(8,128)(2,1)S(1)}, f32[8,4,64,64]{3,2,1,0:T(8,128)S(1)}, bf16[8,128]{1,0:T(8,128)(2,1)S(1)}) custom-call(f32[16,4,64,64]{3,2,1,0:T(8,128)} %state_ref.1, bf16[16,256]{1,0:T(8,128)(2,1)} %reading_ref.1, bf16[16,256]{1,0:T(8,128)(2,1)} %key_ref.1, bf16[16,256]{1,0:T(8,128)(2,1)} %value_ref.1, ...), custom_call_target="tpu_custom_call" | custom-call | flops 20000000 | bytes 5000000 | tf_op jit(solution)/shard_map/pallas_call | solution.py:238
  4.1 0.0 copy-start
  4.2 0.0 copy-start.1
  4.2 0.0 copy-start.2
  4.2 9.4 %all_to_all.30.arrived_ref = bf16[4,16,512]{2,1,0:T(8,128)(2,1)S(1)} all-to-all(bf16[4,16,512]{2,1,0:T(8,128)(2,1)S(1)} %get-tuple-element.13), channel_id=1, replica_groups=mesh['zq'=8,'zp'=2,'x'=4,'c'=2,'y'=4] {'y'}, dimensions={0} | all-to-all | bytes 131072 | tf_op jit(solution)/shard_map/all_to_all | solution.py:21
  13.6 0.0 copy-done.4
  13.6 0.0 copy-done.3
  13.6 28.4 %all_to_all.31.rows_ref = bf16[8,72,128]{2,1,0:T(8,128)(2,1)S(1)} all-to-all(bf16[8,72,128]{2,1,0:T(8,128)(2,1)S(1)} %get-tuple-element.16), channel_id=1, replica_groups=mesh['zq'=8,'zp'=2,'x'=4,'c'=2,'y'=4] {'zq'}, dimensions={0} | all-to-all | bytes 294912 | tf_op jit(solution)/shard_map/all_to_all | solution.py:21
  42.0 0.3 shard_map.169
  42.3 26.8 %all_to_all.32 = bf16[64,16,512]{2,1,0:T(8,128)(2,1)S(1)} all-to-all(bf16[64,16,512]{2,1,0:T(8,128)(2,1)S(1)} %bitcast.15), channel_id=1, replica_groups=mesh['zq'=8,'zp'=2,'x'=4,'c'=2,'y'=4] {'zp','x','c','y'}, dimensions={0} | all-to-all | bytes 2097152 | tf_op jit(solution)/shard_map/all_to_all | solution.py:21
  69.1 0.0 copy-done
  69.1 0.0 copy-done.1
  69.1 0.0 copy-done.2
  69.1 1.0 shard_map.170
  70.1 22.4 %all_to_all.33 = bf16[64,16,512]{2,1,0:T(8,128)(2,1)S(1)} all-to-all(bf16[64,16,512]{2,1,0:T(8,128)(2,1)S(1)} %bitcast.14), channel_id=1, replica_groups=mesh['zq'=8,'zp'=2,'x'=4,'c'=2,'y'=4] {'zp','x','c','y'}, dimensions={0} | all-to-all | bytes 2097152 | tf_op jit(solution)/shard_map/all_to_all | solution.py:21
  92.5 0.4 shard_map.171
  92.9 15.5 %all_to_all.34 = bf16[8,16,512]{2,1,0:T(8,128)(2,1)S(1)} all-to-all(bf16[8,16,512]{2,1,0:T(8,128)(2,1)S(1)} %shard_map.171), channel_id=1, replica_groups=mesh['zq'=8,'zp'=2,'x'=4,'c'=2,'y'=4] {'zq'}, dimensions={0} | all-to-all | bytes 262144 | tf_op jit(solution)/shard_map/all_to_all | solution.py:21
  108.4 10.0 %all_to_all.35 = bf16[4,16,512]{2,1,0:T(8,128)(2,1)S(1)} all-to-all(bf16[4,16,512]{2,1,0:T(8,128)(2,1)S(1)} %broadcast_in_dim.3), channel_id=1, replica_groups=mesh['zq'=8,'zp'=2,'x'=4,'c'=2,'y'=4] {'y'}, dimensions={0} | all-to-all | bytes 131072 | tf_op jit(solution)/shard_map/all_to_all | solution.py:21
  118.4 0.6 copy.20
  (4 shorter events, 0.1 us)
Async XLA Ops:
  0.6 13.0 %copy-start.4 = (f32[2048]{0:T(1024)S(1)}, f32[2048]{0:T(1024)}, u32[]{:S(2)}) copy-start(f32[2048]{0:T(1024)} %param.26) | copy-start | bytes 24580
  0.6 13.0 %copy-start.3 = (bf16[16,2048]{1,0:T(8,128)(2,1)S(1)}, bf16[16,2048]{1,0:T(8,128)(2,1)}, u32[]{:S(2)}) copy-start(bf16[16,2048]{1,0:T(8,128)(2,1)} %hidden_ref.1) | copy-start | bytes 196612
  4.1 64.9 %copy-start = (bf16[1,2048,128]{2,1,0:T(8,128)(2,1)S(1)}, bf16[1,2048,128]{2,1,0:T(8,128)(2,1)}, u32[]{:S(2)}) copy-start(bf16[1,2048,128]{2,1,0:T(8,128)(2,1)} %gate_ref.1) | copy-start | bytes 1572868
  4.2 64.9 %copy-start.1 = (bf16[1,2048,128]{2,1,0:T(8,128)(2,1)S(1)}, bf16[1,2048,128]{2,1,0:T(8,128)(2,1)}, u32[]{:S(2)}) copy-start(bf16[1,2048,128]{2,1,0:T(8,128)(2,1)} %up_ref.1) | copy-start | bytes 1572868
  4.2 64.9 %copy-start.2 = (bf16[1,128,2048]{2,1,0:T(8,128)(2,1)S(1)}, bf16[1,128,2048]{2,1,0:T(8,128)(2,1)}, u32[]{:S(2)}) copy-start(bf16[1,128,2048]{2,1,0:T(8,128)(2,1)} %down_ref.1) | copy-start | bytes 1572868
